TPU v7x, 128 devices: a whole 4x4x4 slice. The times are simulated.
128 devices in a mesh: fs: 16 (over z, x), tp: 8 (over y, core).
Axes of the slice: x: 4, y: 4, z: 4, core: 2. Of those that a mesh axis runs over, the one named last changes fastest.
Arguments:
- later_in: bfloat16 [16384, 2048], P('fs'), may hold values from -3 to 3
- earlier_in: bfloat16 [16384, 2048], P('fs'), may hold values from -3 to 3
- cotangent: bfloat16 [16384, 2048], P('fs'), may hold values from -6 to 6
- gate_weight: bfloat16 [2048, 5632], P('fs', 'tp'), may hold values from -0.125 to 0.125
- up_weight: bfloat16 [2048, 5632], P('fs', 'tp'), may hold values from -0.125 to 0.125
- down_weight: bfloat16 [2048, 5632], P('fs', 'tp'), may hold values from -0.078125 to 0.078125
- norm_gain: bfloat16 [2048], replicated, may hold values from 0.099609375 to 1.8984375
- gate_sum: float32 [2048, 5632], P('fs', 'tp'), may hold values from -96 to 96
- up_sum: float32 [2048, 5632], P('fs', 'tp'), may hold values from -96 to 96
- down_sum: float32 [2048, 5632], P('fs', 'tp'), may hold values from -96 to 96
- gain_sum: float32 [2048], replicated, may hold values from -192 to 192
Outputs:
- later_out: bfloat16 [16384, 2048], P(('fs', 'tp'))
- later_hidden: bfloat16 [16384, 5632], P('fs', 'tp')
- earlier_grad: bfloat16 [16384, 2048], P(('fs', 'tp'))
- gate_sum_new: float32 [2048, 5632], P('fs', 'tp')
- up_sum_new: float32 [2048, 5632], P('fs', 'tp')
- down_sum_new: float32 [2048, 5632], P('fs', 'tp')
- gain_sum_new: float32 [2048], replicated
All inputs are finite; a program needn't handle non-finite values.
Results may differ from a plain program's by a relative error of at most 0.013.
Values may be sent and summed in bfloat16 or wider, within the bound.
A program may use at most 128 MiB of HBM per device.

v0:
```python
import jax
import jax.numpy as jnp
from jax import lax
from jax.sharding import Mesh
from jax.sharding import PartitionSpec as P

TP = ("tp_0", "tp_1")
FS = ("fs_0", "fs_1")
FS_TP = ("fs_0", "fs_1", "tp_0", "tp_1")


norm_floor = 0.05


def split_up(array, dim, count):
    dims = array.shape
    parts = array.reshape(*dims[:dim], count, dims[dim] // count, *dims[dim + 1 :])
    return jnp.moveaxis(parts, dim, 0)


def sum_at_owner(array, axis, dim):
    parts = split_up(array, dim, lax.axis_size(axis))
    arrived = lax.all_to_all(parts, axis, split_axis=0, concat_axis=0, tiled=True)
    return arrived.astype(jnp.float32).sum(axis=0)


def by_axis(array, axes):
    for axis in axes:
        array = lax.psum(array, axis)
    return array


def side_by_side(arrays, axis, dim, along):
    ends, at = ([], 0)
    for a in arrays[:-1]:
        at += a.shape[along]
        ends.append(at)
    both = jnp.concatenate(arrays, axis=along)
    return tuple(jnp.split(lax.all_gather(both, axis, axis=dim, tiled=True), ends, axis=along))


def normalize(tokens_in, norm_gain):
    values = tokens_in.astype(jnp.float32)
    row_scale = lax.rsqrt(jnp.mean(values * values, axis=1, keepdims=True) + norm_floor)
    unit_rows = values * row_scale
    normed = (unit_rows * norm_gain.astype(jnp.float32)).astype(jnp.bfloat16)
    return (row_scale, unit_rows, normed)


def transposed(matrix_a, matrix_b):
    return lax.dot_general(
        matrix_a, matrix_b, (((1,), (1,)), ((), ())), preferred_element_type=jnp.float32
    )


def outer_sum(matrix_a, matrix_b):
    return lax.dot_general(
        matrix_a, matrix_b, (((0,), (0,)), ((), ())), preferred_element_type=jnp.float32
    )


def own_rows(tokens_in, own_count):
    return lax.dynamic_slice_in_dim(tokens_in, lax.axis_index(TP) * own_count, own_count, 0)


def forward(later_in, norm_gain, weights):
    w_gate, w_up, w_down = weights
    normed = normalize(later_in, norm_gain)[2]
    gate_pre = jnp.dot(normed, w_gate, preferred_element_type=jnp.float32)
    up_pre = jnp.dot(normed, w_up, preferred_element_type=jnp.float32)
    hidden = (jax.nn.silu(gate_pre) * up_pre).astype(jnp.bfloat16)
    own_count = later_in.shape[0] // lax.axis_size(TP)
    summed = lax.psum_scatter(
        transposed(hidden, w_down).astype(jnp.bfloat16), TP, scatter_dimension=0, tiled=True
    ).astype(jnp.float32)
    later_out = (own_rows(later_in, own_count).astype(jnp.float32) + 0.5 * summed).astype(
        jnp.bfloat16
    )
    return (later_out, hidden)


def backward(earlier_in, cotangent, norm_gain, weights):
    w_gate, w_up, w_down = weights
    row_scale, unit_rows, normed = normalize(earlier_in, norm_gain)
    gate_pre = jnp.dot(normed, w_gate, preferred_element_type=jnp.float32)
    up_pre = jnp.dot(normed, w_up, preferred_element_type=jnp.float32)
    sigmoid_gate = jax.nn.sigmoid(gate_pre)
    activated = gate_pre * sigmoid_gate
    hidden = (activated * up_pre).astype(jnp.bfloat16)
    col_width = hidden.shape[1]
    dhidden = jnp.dot(cotangent, w_down, preferred_element_type=jnp.float32)
    dgate = (
        0.5 * dhidden * up_pre * sigmoid_gate * (1.0 + gate_pre * (1.0 - sigmoid_gate))
    ).astype(jnp.bfloat16)
    dupper = (0.5 * dhidden * activated).astype(jnp.bfloat16)
    gate_and_up = jnp.concatenate([dgate, dupper], axis=1)
    dnormed = transposed(dgate, w_gate) + transposed(dupper, w_up)
    gain_part = jnp.sum(dnormed * unit_rows, axis=0)
    weighted = dnormed * norm_gain.astype(jnp.float32)
    branch = row_scale * (
        weighted - unit_rows * jnp.mean(weighted * unit_rows, axis=1, keepdims=True)
    )
    own_count = earlier_in.shape[0] // lax.axis_size(TP)
    summed = sum_at_owner(branch.astype(jnp.bfloat16), TP, 0)
    earlier_grad = (own_rows(cotangent, own_count).astype(jnp.float32) + summed).astype(
        jnp.bfloat16
    )
    grads_total = lax.psum_scatter(
        jnp.concatenate(
            [outer_sum(normed, gate_and_up), 0.5 * outer_sum(cotangent, hidden)], axis=1
        ).astype(jnp.bfloat16),
        FS,
        scatter_dimension=0,
        tiled=True,
    ).astype(jnp.float32)
    grad_gate = grads_total[:, :col_width]
    grad_up = grads_total[:, col_width : 2 * col_width]
    grad_down = grads_total[:, 2 * col_width :]
    gain_total = by_axis(gain_part, FS_TP)
    return (earlier_grad, grad_gate, grad_up, grad_down, gain_total)


def local(
    later_in,
    earlier_in,
    cotangent,
    gate_weight,
    up_weight,
    down_weight,
    norm_gain,
    gate_sum,
    up_sum,
    down_sum,
    gain_sum,
):
    pieces = (gate_weight, up_weight, down_weight)
    shared = side_by_side((pieces[0], pieces[1], pieces[2]), FS, 0, 1)
    later_out, later_hidden = forward(later_in, norm_gain, shared)
    earlier = backward(earlier_in, cotangent, norm_gain, shared)
    earlier_grad, grad_gate, grad_up, grad_down, gain_total = earlier
    return (
        later_out,
        later_hidden,
        earlier_grad,
        gate_sum + grad_gate,
        up_sum + grad_up,
        down_sum + grad_down,
        gain_sum + gain_total,
    )


def solution(mesh):
    torus = Mesh(mesh.devices.reshape(4, 4, 4, 2), ("fs_0", "fs_1", "tp_0", "tp_1"))
    return jax.shard_map(
        local,
        mesh=torus,
        in_specs=(
            P(FS, None),
            P(FS, None),
            P(FS, None),
            P(FS, TP),
            P(FS, TP),
            P(FS, TP),
            P(),
            P(FS, TP),
            P(FS, TP),
            P(FS, TP),
            P(),
        ),
        out_specs=(P(FS_TP, None), P(FS, TP), P(FS_TP, None), P(FS, TP), P(FS, TP), P(FS, TP), P()),
        check_vma=False,
    )
```

profile of v0, /device:TPU:0, one launch (start us, length us, event | category | flops | bytes accessed | tf_op | source)
XLA Modules:
  0.0 251.8 jit_solution(18048430084781595478)
XLA Ops:
  7.2 0.0 all-gather.2.cloned.1.call-start
  7.2 1.9 pad_maximum_fusion.1
  9.1 0.0 all-gather.2.cloned.1.call-update
  9.2 0.0 reduce-scatter.5.cloned.1.call-start
  9.2 0.7 convert_element_type.59
  9.9 3.1 %fusion.4 = f32[1024]{0:T(1024)S(1)} fusion(bf16[1024,2048]{1,0:T(8,128)(2,1)} %param.11), kind=kLoop, calls=%fused_computation.9 | loop fusion | flops 6290432 | bytes 4198400 | tf_op jit(solution)/shard_map/reduce_sum | solution.py:44
  13.0 78.8 %all-gather.2.cloned.1.call-done = bf16[2048,2112]{0,1:T(8,128)(2,1)} async-done(((bf16[128,2112]{0,1:T(8,128)(2,1)}), bf16[2048,2112]{0,1:T(8,128)(2,1)}) %all-gather.2.cloned.1.call-update) | async-done | bytes 8650768 | tf_op jit(solution)/shard_map/all_gather | solution.py:39
  91.8 0.0 copy-start.2
  91.8 6.4 %fusion.29 = f32[1024,704]{0,1:T(8,128)S(1)} fusion(bf16[2048,2112]{0,1:T(8,128)(2,1)} %all-gather.2.cloned.1.call-done, bf16[1024,2048]{1,0:T(8,128)(2,1)} %param.11, f32[2048]{0:T(1024)S(1)} %convert_element_type.59, f32[1024]{0:T(1024)S(1)} %add_rsqrt_fusion.1), kind=kOutput, calls=%fused_computation.44 | convolution fusion | flops 2961178624 | bytes 9973760 | tf_op jit(solution)/shard_map/dot_general | solution.py:70
  98.3 0.0 copy-done.2
  98.3 0.4 copy-done.8
  98.7 3.6 %multiply_convert_fusion.2 = bf16[1024,704]{0,1:T(8,128)(2,1)S(1)} fusion(f32[1024,704]{0,1:T(8,128)S(1)} %fusion.29, bf16[2048,2112]{0,1:T(8,128)(2,1)S(1)} %copy-done.8, bf16[1024,2048]{1,0:T(8,128)(2,1)S(1)} %copy-done.2, f32[2048]{0:T(1024)S(1)} %convert_element_type.59, f32[1024]{0:T(1024)S(1)} %add_rsqrt_fusion.1), kind=kOutput, calls=%fused_computation.37 | convolution fusion | flops 2965504000 | bytes 11415552 | tf_op jit(solution)/shard_map/dot_general | solution.py:69
  102.3 0.0 copy-start.9
  102.3 5.1 %convolution_convert_fusion.1 = bf16[1024,2048]{1,0:T(8,128)(2,1)} fusion(bf16[1024,704]{0,1:T(8,128)(2,1)S(1)} %multiply_convert_fusion.2, bf16[2048,2112]{0,1:T(8,128)(2,1)S(1)} %copy-done.8), kind=kOutput, calls=%fused_computation.23 | convolution fusion | flops 2954887168 | bytes 8519680 | tf_op jit(solution)/shard_map/dot_general | solution.py:51
  107.4 0.0 copy-done.9
  107.4 0.0 reduce-scatter.5.cloned.1.call-update
  107.4 0.2 reduce-scatter.7.cloned.1.call-start
  107.7 0.0 copy-start
  107.7 0.0 slice-start
  107.7 3.2 %fusion.13 = f32[1024]{0:T(1024)S(1)} fusion(bf16[1024,2048]{1,0:T(8,128)(2,1)} %param.12), kind=kLoop, calls=%fused_computation.18 | loop fusion | flops 6290432 | bytes 4198400 | tf_op jit(solution)/shard_map/reduce_sum | solution.py:44
  110.9 0.2 copy-done
  111.1 5.3 %fusion.33 = f32[1024,704]{0,1:T(8,128)S(1)} fusion(bf16[2048,2112]{0,1:T(8,128)(2,1)} %all-gather.2.cloned.1.call-done, bf16[1024,2048]{1,0:T(8,128)(2,1)S(1)} %copy-done, f32[1024]{0:T(1024)S(1)} %add_rsqrt_fusion, f32[2048]{0:T(1024)S(1)} %convert_element_type.59), kind=kOutput, calls=%fused_computation.48 | convolution fusion | flops 2961178624 | bytes 9973760 | tf_op jit(solution)/shard_map/dot_general | solution.py:85
  116.4 0.0 slice-done
  116.5 0.0 slice-done.1
  116.5 0.0 slice-done.2
  116.5 0.0 copy-start.6
  116.5 3.2 %fusion.27 = f32[1024,704]{0,1:T(8,128)S(1)} fusion(bf16[2048,2112]{0,1:T(8,128)(2,1)S(1)} %bitcast.22, bf16[1024,2048]{1,0:T(8,128)(2,1)S(1)} %copy-done, f32[1024]{0:T(1024)S(1)} %add_rsqrt_fusion, f32[2048]{0:T(1024)S(1)} %convert_element_type.59), kind=kOutput, calls=%fused_computation.42 | convolution fusion | flops 2961178624 | bytes 9973760 | tf_op jit(solution)/shard_map/dot_general | solution.py:86
  119.7 0.0 copy-start.10
  119.8 1.5 copy-done.10
  121.3 0.0 copy-done.6
  121.3 3.5 %fusion.14 = bf16[2048,704]{0,1:T(8,128)(2,1)S(1)} fusion(bf16[1024,2048]{1,0:T(8,128)(2,1)S(1)} %copy-done.6, f32[1024,704]{0,1:T(8,128)S(1)} %fusion.27, f32[1024,704]{0,1:T(8,128)S(1)} %fusion.33), kind=kOutput, calls=%fused_computation.24 | convolution fusion | flops 2959998976 | bytes 12845056 | tf_op jit(solution)/shard_map/dot_general | solution.py:57
  124.8 6.7 %fusion.21 = (bf16[1024,704]{0,1:T(8,128)(2,1)S(1)}, bf16[1024,704]{0,1:T(8,128)(2,1)}) fusion(f32[1024,704]{0,1:T(8,128)S(1)} %fusion.33, f32[1024,704]{0,1:T(8,128)} %copy-done.10, bf16[1024,2048]{1,0:T(8,128)(2,1)S(1)} %copy-done.6, bf16[2048,2112]{0,1:T(8,128)(2,1)S(1)} %bitcast.22), kind=kOutput, calls=%fused_computation.33 | convolution fusion | flops 2962882560 | bytes 15728640 | tf_op jit(solution)/shard_map/dot_general | solution.py:91
  131.5 8.5 %convolution_convert_fusion = bf16[2048,1408]{0,1:T(8,128)(2,1)S(1)} fusion(bf16[1024,704]{0,1:T(8,128)(2,1)S(1)} %get-tuple-element.9, bf16[1024,704]{0,1:T(8,128)(2,1)} %get-tuple-element.10, bf16[1024,2048]{1,0:T(8,128)(2,1)S(1)} %copy-done, f32[1024]{0:T(1024)S(1)} %add_rsqrt_fusion, f32[2048]{0:T(1024)S(1)} %convert_element_type.59), kind=kOutput, calls=%fused_computation.20 | convolution fusion | flops 5922619392 | bytes 12857344 | tf_op jit(solution)/shard_map/dot_general | solution.py:57
  140.0 0.0 copy-done.11
  140.0 4.3 %pad_maximum_fusion = bf16[2048,2112]{0,1:T(8,128)(2,1)} fusion(bf16[2048,704]{0,1:T(8,128)(2,1)S(1)} %fusion.14, bf16[2048,1408]{0,1:T(8,128)(2,1)S(1)} %convolution_convert_fusion), kind=kLoop, calls=%fused_computation.8 | loop fusion | flops 17301504 | bytes 17301504 | tf_op jit(solution)/shard_map/concatenate | solution.py:109
  144.3 11.8 %copy.18 = bf16[2048,2112]{1,0:T(8,128)(2,1)} copy(bf16[2048,2112]{0,1:T(8,128)(2,1)} %pad_maximum_fusion) | data formatting | bytes 17301504
  156.1 0.0 reduce-scatter.7.cloned.1.call-update
  156.1 1.3 copy-done.13
  157.5 5.5 %fusion.31 = f32[1024,2048]{1,0:T(8,128)S(1)} fusion(bf16[1024,704]{0,1:T(8,128)(2,1)S(1)} %copy-done.13, bf16[2048,2112]{0,1:T(8,128)(2,1)} %all-gather.2.cloned.1.call-done), kind=kOutput, calls=%fused_computation.46 | convolution fusion | flops 2952790016 | bytes 12713984 | tf_op jit(solution)/shard_map/dot_general | solution.py:51
  163.0 0.0 copy-done.1
  163.0 0.0 copy-done.12
  163.0 7.3 %fusion.12 = (f32[2048]{0:T(1024)S(1)}, f32[1024]{0:T(1024)S(1)}, f32[1024,2048]{1,0:T(8,128)S(1)}) fusion(bf16[1024,2048]{1,0:T(8,128)(2,1)S(1)} %copy-done.1, f32[1024]{0:T(1024)S(1)} %add_rsqrt_fusion, f32[2048]{0:T(1024)S(1)} %convert_element_type.59, f32[1024,2048]{1,0:T(8,128)S(1)} %fusion.31, bf16[1024,704]{0,1:T(8,128)(2,1)S(1)} %copy-done.12, ...), kind=kOutput, calls=%fused_computation.17 | convolution fusion | flops 2969564160 | bytes 25321472 | tf_op jit(solution)/shard_map/dot_general | solution.py:51
  170.3 3.4 %fusion.11 = bf16[1024,2048]{1,0:T(8,128)(2,1)} fusion(bf16[1024,2048]{1,0:T(8,128)(2,1)S(1)} %copy-done.1, f32[1024,2048]{1,0:T(8,128)S(1)} %get-tuple-element.14, f32[1024]{0:T(1024)S(1)} %broadcast_multiply_fusion, f32[1024]{0:T(1024)S(1)} %add_rsqrt_fusion, f32[2048]{0:T(1024)S(1)} %convert_element_type.59), kind=kLoop, calls=%fused_computation.16 | loop fusion | flops 14680064 | bytes 16793600 | tf_op jit(solution)/shard_map/convert_element_type | solution.py:104
  173.6 4.7 %all-to-all-start = ((bf16[8,128,2048]{2,1,0:T(8,128)(2,1)}), bf16[8,128,2048]{2,1,0:T(8,128)(2,1)}, u32[]{:S(2)}, u32[]{:S(2)}) async-start(bf16[8,128,2048]{2,1,0:T(8,128)(2,1)} %bitcast.20), calls=%async_computation.1 | async-start | bytes 8388608 | tf_op jit(solution)/shard_map/all_to_all | solution.py:23
  178.4 10.4 %psum.28 = f32[2048]{0:T(1024)S(1)} all-reduce(f32[2048]{0:T(1024)S(1)} %get-tuple-element.7), channel_id=1, replica_groups=mesh['fs_0'=4,'fs_1'=4,'tp_0'=4,'tp_1'=2] {'fs_0'}, use_global_device_ids=true, to_apply=%region_7.8 | all-reduce | flops 2048 | bytes 16384 | tf_op jit(solution)/shard_map/psum | solution.py:29
  188.8 8.8 %psum.29 = f32[2048]{0:T(1024)S(1)} all-reduce(f32[2048]{0:T(1024)S(1)} %psum.28), channel_id=1, replica_groups=mesh['fs_0'=4,'fs_1'=4,'tp_0'=4,'tp_1'=2] {'fs_1'}, use_global_device_ids=true, to_apply=%region_8.9 | all-reduce | flops 2048 | bytes 16384 | tf_op jit(solution)/shard_map/psum | solution.py:29
  197.6 32.8 %psum.30 = f32[2048]{0:T(1024)S(1)} all-reduce(f32[2048]{0:T(1024)S(1)} %psum.29), channel_id=1, replica_groups=mesh['fs_0'=4,'fs_1'=4,'tp_0'=4,'tp_1'=2] {'tp_0'}, use_global_device_ids=true, to_apply=%region_9.10 | all-reduce | flops 2048 | bytes 16384 | tf_op jit(solution)/shard_map/psum | solution.py:29
  230.3 2.5 psum.31
  232.8 0.0 copy-done.7
  232.8 0.6 add.80
  233.5 0.0 all-to-all-done
  233.5 3.1 %convert_reduce_fusion = f32[128,2048]{1,0:T(8,128)S(1)} fusion(bf16[8,128,2048]{2,1,0:T(8,128)(2,1)} %all-to-all-done), kind=kLoop, calls=%fused_computation.19 | loop fusion | flops 3932160 | bytes 5242880 | tf_op jit(solution)/shard_map/reduce_sum | solution.py:24
  236.5 0.0 copy-start.3
  236.6 0.0 copy-start.4
  236.6 0.0 copy-start.5
  236.6 2.0 add_convert_fusion
  238.6 2.2 add_convert_fusion.1
  240.8 2.0 reduce-scatter.7.cloned.1.call-done
  242.8 1.3 copy.19
  244.2 0.1 convert_element_type.74
  244.2 0.0 copy-done.3
  244.3 0.0 copy-done.4
  244.3 0.0 copy-done.5
  244.3 1.0 slice_add_fusion
  (13 shorter events, 0.0 us)
Async XLA Ops:
  7.2 84.7 %all-gather.2.cloned.1.call-start = ((), (), s32[]{:S(2)}) async-start(), calls=%async_computation.3 | async-start | bytes 9191424 | tf_op jit(solution)/shard_map/all_gather | solution.py:39
  9.2 229.4 %reduce-scatter.5.cloned.1.call-start = ((), (), s32[]{:S(2)}) async-start(), calls=%async_computation.4 | async-start | bytes 4718592 | tf_op jit(solution)/shard_map/reduce_scatter | solution.py:73
  91.8 6.4 %copy-start.2 = (bf16[1024,2048]{1,0:T(8,128)(2,1)S(1)}, bf16[1024,2048]{1,0:T(8,128)(2,1)}, u32[]{:S(2)}) copy-start(bf16[1024,2048]{1,0:T(8,128)(2,1)} %param.11) | copy-start | bytes 12582916
  91.8 6.8 %copy-start.8 = (bf16[2048,2112]{0,1:T(8,128)(2,1)S(1)}, bf16[2048,2112]{0,1:T(8,128)(2,1)}, u32[]{:S(2)}) copy-start(bf16[2048,2112]{0,1:T(8,128)(2,1)} %all-gather.2.cloned.1.call-done) | copy-start | bytes 25952260
  102.3 5.1 %copy-start.9 = (bf16[1024,704]{0,1:T(8,128)(2,1)}, bf16[1024,704]{0,1:T(8,128)(2,1)S(1)}, u32[]{:S(2)}) copy-start(bf16[1024,704]{0,1:T(8,128)(2,1)S(1)} %multiply_convert_fusion.2) | copy-start | bytes 4325380
  107.4 135.4 %reduce-scatter.7.cloned.1.call-start = ((), (), s32[]{:S(2)}) async-start(), calls=%async_computation.5 | async-start | bytes 9469952
  107.7 3.5 %copy-start = (bf16[1024,2048]{1,0:T(8,128)(2,1)S(1)}, bf16[1024,2048]{1,0:T(8,128)(2,1)}, u32[]{:S(2)}) copy-start(bf16[1024,2048]{1,0:T(8,128)(2,1)} %param.12) | copy-start | bytes 12582916
  107.7 8.8 %slice-start = ((s8[8650752]{0:T(1024)(128)(4,1)}), s8[4194304]{0:T(1024)(128)(4,1)S(1)}, s32[]{:S(2)}) async-start(s8[8650752]{0:T(1024)(128)(4,1)} %bitcast.21), calls=%async_computation.6 | async-start | bytes 8388608
  111.1 5.3 %slice-start.1 = ((s8[8650752]{0:T(1024)(128)(4,1)}), s8[4194304]{0:T(1024)(128)(4,1)S(1)}, s32[]{:S(2)}) async-start(s8[8650752]{0:T(1024)(128)(4,1)} %bitcast.21), calls=%async_computation.7 | async-start | bytes 8388608
  111.1 5.4 %slice-start.2 = ((s8[8650752]{0:T(1024)(128)(4,1)}), s8[262144]{0:T(1024)(128)(4,1)S(1)}, s32[]{:S(2)}) async-start(s8[8650752]{0:T(1024)(128)(4,1)} %bitcast.21), calls=%async_computation.8 | async-start | bytes 524288
  116.5 4.8 %copy-start.6 = (bf16[1024,2048]{1,0:T(8,128)(2,1)S(1)}, bf16[1024,2048]{1,0:T(8,128)(2,1)}, u32[]{:S(2)}) copy-start(bf16[1024,2048]{1,0:T(8,128)(2,1)} %param.13) | copy-start | bytes 12582916
  119.7 1.6 copy-start.10
  131.5 8.5 %copy-start.11 = (bf16[1024,704]{0,1:T(8,128)(2,1)}, bf16[1024,704]{0,1:T(8,128)(2,1)S(1)}, u32[]{:S(2)}) copy-start(bf16[1024,704]{0,1:T(8,128)(2,1)S(1)} %get-tuple-element.9) | copy-start | bytes 4325380
  156.1 1.4 copy-start.13
  157.5 5.5 %copy-start.1 = (bf16[1024,2048]{1,0:T(8,128)(2,1)S(1)}, bf16[1024,2048]{1,0:T(8,128)(2,1)}, u32[]{:S(2)}) copy-start(bf16[1024,2048]{1,0:T(8,128)(2,1)} %param.12) | copy-start | bytes 12582916
  157.5 5.5 %copy-start.12 = (bf16[1024,704]{0,1:T(8,128)(2,1)S(1)}, bf16[1024,704]{0,1:T(8,128)(2,1)}, u32[]{:S(2)}) copy-start(bf16[1024,704]{0,1:T(8,128)(2,1)} %copy-done.11) | copy-start | bytes 4325380
  173.6 59.2 %copy-start.7 = (f32[2048]{0:T(1024)S(1)}, f32[2048]{0:T(1024)}, u32[]{:S(2)}) copy-start(f32[2048]{0:T(1024)} %param.21) | copy-start | bytes 24580
  173.6 59.8 %all-to-all-start = ((bf16[8,128,2048]{2,1,0:T(8,128)(2,1)}), bf16[8,128,2048]{2,1,0:T(8,128)(2,1)}, u32[]{:S(2)}, u32[]{:S(2)}) async-start(bf16[8,128,2048]{2,1,0:T(8,128)(2,1)} %bitcast.20), calls=%async_computation.1 | async-start | bytes 8388608 | tf_op jit(solution)/shard_map/all_to_all | solution.py:23
  236.5 7.7 %copy-start.3 = (f32[128,704]{0,1:T(8,128)S(1)}, f32[128,704]{0,1:T(8,128)}, u32[]{:S(2)}) copy-start(f32[128,704]{0,1:T(8,128)} %param.20) | copy-start | bytes 1081348
  236.6 7.7 %copy-start.4 = (f32[128,704]{0,1:T(8,128)S(1)}, f32[128,704]{0,1:T(8,128)}, u32[]{:S(2)}) copy-start(f32[128,704]{0,1:T(8,128)} %param.19) | copy-start | bytes 1081348
  236.6 7.7 %copy-start.5 = (f32[128,704]{0,1:T(8,128)S(1)}, f32[128,704]{0,1:T(8,128)}, u32[]{:S(2)}) copy-start(f32[128,704]{0,1:T(8,128)} %param.18) | copy-start | bytes 1081348
Sparse Core Ops, SparseCore 0:
  10.7 81.1 all-gather.1
  107.5 37.1 reduce-scatter.4
  156.2 86.5 reduce-scatter.6
where the time goes:
time: 253 us; the launch traced here: 252 us
  waiting for transfers between devices  80.9 us (32%)
  matrix products  55.2 us (22%)
  blocking collectives  54.4 us (22%)
  other arithmetic  25.6 us (10%)
  local copies, waits for them, and re-layouts  16.6 us (7%)
  between operations  14 us (6%)
  starting transfers between devices  5.05 us (2%)
    all_gather x1, waiting for transfers between devices, side_by_side(): lax.all_gather(both, axis, axis=dim, tiled=True)  78.8 us
    psum x4, blocking collectives, by_axis(): array = lax.psum(array, axis)  54.4 us
    dot_general x3, matrix products, transposed(): lax.dot_general(matrix_a, matrix_b, (((1,), (1,)), ((), ())), preferred_e...  17.9 us
    unnamed x36, local copies, waits for them, and re-layouts  16.6 us
    dot_general x2, matrix products, outer_sum(): lax.dot_general(matrix_a, matrix_b, (((0,), (0,)), ((), ())), preferred_e...  12 us
    dot_general x1, matrix products, backward(): dhidden = jnp.dot(cotangent, w_down, preferred_element_type=jnp.float32)  6.67 us
    dot_general x1, matrix products, forward(): up_pre = jnp.dot(normed, w_up, preferred_element_type=jnp.float32)  6.43 us
    reduce_sum x2, other arithmetic, normalize(): jnp.mean(values * values, axis=1, keepdims=True) + norm_floor  6.3 us
  transfers between devices with their start and end apart: 4, of which 2 were waited for; matrix products, arithmetic and copies ran while one was open for 30% of the time, Pallas kernels for 0%

commit v1 on v0

v1 whole, which is shorter than its diff:
```python
import functools

import jax
import jax.numpy as jnp
from jax import lax
from jax.experimental import pallas as pl
from jax.experimental.pallas import tpu as pltpu
from jax.sharding import Mesh
from jax.sharding import PartitionSpec as P

FS = ("z", "x")
TP = ("y", "c")
ALL = ("z", "x", "y", "c")
MESH = pl.DeviceIdType.MESH
BF = jnp.bfloat16
F32 = jnp.float32
CHUNK = 256
N_CHUNK = 3
WIDE = 3 * CHUNK
SHARD = 128
NORM_FLOOR = 0.05


def pack(w):
    rows, cols = w.shape
    w = jnp.pad(w, ((0, 0), (0, N_CHUNK * CHUNK - cols)))
    return w.reshape(rows, N_CHUNK, CHUNK).transpose(1, 0, 2)


class Gather:
    def __init__(self, w, send, recv):
        self.w, self.send, self.recv = w, send, recv
        self.mz, self.mx = lax.axis_index("z"), lax.axis_index("x")

    def owner(self, h, jf, js):
        dx, dz = (jf, js) if h == 0 else (js, jf)
        return lax.rem(self.mz + dz + 4, 4) * 4 + lax.rem(self.mx + dx + 4, 4)

    def copy(self, c, h, msg, jf, js, sub, axis, d):
        start = self.owner(h, jf, js) * SHARD + h * (SHARD // 2)
        size = SHARD // 2
        if sub is not None:
            size = SHARD // 4
            start = start + sub * size
        view = self.w.at[c, pl.ds(pl.multiple_of(start, 32), size), :]
        name = ("x", "z")[h] if axis == "f" else ("z", "x")[h]
        me = self.mx if name == "x" else self.mz
        return pltpu.make_async_remote_copy(
            src_ref=view,
            dst_ref=view,
            send_sem=self.send.at[c, h, msg],
            recv_sem=self.recv.at[c, h, msg],
            device_id={name: lax.rem(me + d + 4, 4)},
            device_id_type=MESH,
        )

    def m1(self, c, h, d):
        return self.copy(c, h, 0 if d > 0 else 1, 0, 0, None, "f", d)

    def r1(self, c, h, d):
        return self.copy(c, h, 0 if d > 0 else 1, -d, 0, None, "f", d)

    def m2(self, c, h, d):
        return self.copy(c, h, 2 if d > 0 else 3, -d, 0, 0 if d > 0 else 1, "f", d)

    def r2(self, c, h, d):
        return self.copy(c, h, 2 if d > 0 else 3, -2 * d, 0, 0 if d > 0 else 1, "f", d)

    def m3(self, c, h, j, d):
        return self.copy(c, h, 4 + 2 * (j % 4) + (0 if d > 0 else 1), j, 0, None, "s", d)

    def r3(self, c, h, j, d):
        return self.copy(c, h, 4 + 2 * (j % 4) + (0 if d > 0 else 1), j, -d, None, "s", d)

    def m4(self, c, h, j, d):
        return self.copy(c, h, 12 + 2 * (j % 4) + (0 if d > 0 else 1), j, -d, 0 if d > 0 else 1, "s", d)

    def r4(self, c, h, j, d):
        return self.copy(c, h, 12 + 2 * (j % 4) + (0 if d > 0 else 1), j, -2 * d, 0 if d > 0 else 1, "s", d)

    def t0(self, c):
        for h in (0, 1):
            for d in (1, -1):
                self.m1(c, h, d).start()
        for h in (0, 1):
            for d in (1, -1):
                self.m3(c, h, 0, d).start()

    def t1(self, c):
        for d in (1, -1):
            for h in (0, 1):
                self.r1(c, h, d).wait_recv()
                self.m2(c, h, d).start()
                for e in (1, -1):
                    self.m3(c, h, -d, e).start()

    def pass_on(self, c, js):
        for j in js:
            for d in (1, -1):
                for h in (0, 1):
                    self.r3(c, h, j, d).wait_recv()
                    self.m4(c, h, j, d).start()

    def t2(self, c):
        self.pass_on(c, (0,))

    def t3(self, c):
        for h in (0, 1):
            for d in (1, -1):
                self.r2(c, h, d).wait_recv()
            for e in (1, -1):
                self.m3(c, h, 2, e).start()

    def t4(self, c):
        self.pass_on(c, (-1, 1))

    def t5(self, c):
        self.pass_on(c, (2,))

    def t6(self, c):
        for h in (0, 1):
            for j in (0, -1, 1, 2):
                for d in (1, -1):
                    self.r4(c, h, j, d).wait_recv()

    def drain(self, c):
        for h in (0, 1):
            for d in (1, -1):
                self.m1(c, h, d).wait_send()
                self.m2(c, h, d).wait_send()
                for j in (0, -1, 1, 2):
                    self.m3(c, h, j, d).wait_send()
                    self.m4(c, h, j, d).wait_send()


def greet(peers):
    barrier = pltpu.get_barrier_semaphore()
    for peer in peers:
        pl.semaphore_signal(barrier, inc=1, device_id=peer, device_id_type=MESH)
    pl.semaphore_wait(barrier, len(peers))


def ring_peers(names):
    peers = []
    for name in names:
        me = lax.axis_index(name)
        for d in (1, 3):
            peers.append({name: lax.rem(me + d, 4)})
    return peers


def nn(a, b):
    return jnp.dot(a, b, preferred_element_type=F32)


def k1_body(
    later_in, earlier_in, cot_in, gain, w_own,
    w_out, hl_out, dg_out, du_out, g_out,
    w, nl, ne, net, cot, cott, hl, dg, du, he, g,
    in_sem, own_sem, send, recv, out_sem,
):
    tokens, width = nl.shape
    ins = [
        pltpu.make_async_copy(later_in, nl, in_sem.at[0]),
        pltpu.make_async_copy(earlier_in, ne, in_sem.at[1]),
        pltpu.make_async_copy(cot_in, cot, in_sem.at[2]),
    ]
    me = lax.axis_index("z") * 4 + lax.axis_index("x")
    own = [
        pltpu.make_async_copy(
            w_own.at[c], w.at[c, pl.ds(pl.multiple_of(me * SHARD, SHARD), SHARD), :], own_sem.at[c]
        )
        for c in range(N_CHUNK)
    ]
    for copy in own:
        copy.start()
    for copy in ins:
        copy.start()
    greet(ring_peers(("x", "z")))
    for copy in own:
        copy.wait()
    ring = Gather(w, send, recv)
    ring.t0(0)

    gain_row = gain[...].astype(F32)

    def norm_block(ref, i, turned):
        rows = pl.ds(pl.multiple_of(i * 128, 128), 128)
        v = ref[rows, :].astype(F32)
        unit = v * lax.rsqrt(jnp.mean(v * v, axis=1, keepdims=True) + NORM_FLOOR)
        normed = (unit * gain_row).astype(BF)
        ref[rows, :] = normed
        if turned is not None:
            turned[:, rows] = normed.T

    blocks = tokens // 128

    ins[0].wait()

    @pl.loop(0, blocks)
    def _(i):
        norm_block(nl, i, None)

    ring.t1(0)
    ins[1].wait()

    @pl.loop(0, blocks // 2)
    def _(i):
        norm_block(ne, i, net)

    ring.t2(0)

    @pl.loop(blocks // 2, blocks)
    def _(i):
        norm_block(ne, i, net)

    ring.t3(0)
    ring.t0(1)
    ins[2].wait()

    def turn_block(i):
        rows = pl.ds(pl.multiple_of(i * 128, 128), 128)
        cott[:, rows] = cot[rows, :].T

    @pl.loop(0, blocks // 2)
    def _(i):
        turn_block(i)

    ring.t4(0)
    ring.t1(1)

    @pl.loop(blocks // 2, blocks)
    def _(i):
        turn_block(i)

    ring.t5(0)
    ring.t2(1)
    ring.t6(0)

    tb = 256

    def later_item(c, i):
        rows = pl.ds(i * tb, tb)
        pre = nn(nl[rows, :], w[c, :, : 2 * CHUNK])
        gate, up = pre[:, :CHUNK], pre[:, CHUNK:]
        hl[c, rows, :] = (gate * jax.nn.sigmoid(gate) * up).astype(BF)

    def earlier_item(c, i):
        rows = pl.ds(i * tb, tb)
        pre = nn(ne[rows, :], w[c, :, : 2 * CHUNK])
        dh = 0.5 * nn(cot[rows, :], w[c, :, 2 * CHUNK :])
        gate, up = pre[:, :CHUNK], pre[:, CHUNK:]
        s = jax.nn.sigmoid(gate)
        act = gate * s
        he[rows, :] = (act * up).astype(BF)
        dg[c, rows, :] = (dh * up * s * (1.0 + gate * (1.0 - s))).astype(BF)
        du[c, rows, :] = (dh * act).astype(BF)

    def grad_item(c, i):
        rows = pl.ds(i * 512, 512)
        g[c, rows, :CHUNK] = nn(net[rows, :], dg[c]).astype(BF)
        g[c, rows, CHUNK : 2 * CHUNK] = nn(net[rows, :], du[c]).astype(BF)
        g[c, rows, 2 * CHUNK :] = (0.5 * nn(cott[rows, :], he[...])).astype(BF)

    @pl.loop(0, N_CHUNK)
    def _(c):
        ahead = [ring.t3, None, ring.t4, None, ring.t5, None, ring.t6]
        behind = [None, ring.t0, None, ring.t1, None, ring.t2, None]
        items = [functools.partial(earlier_item, c, i) for i in range(tokens // tb)]
        items += [functools.partial(later_item, c, i) for i in range(tokens // tb)]
        items += [functools.partial(grad_item, c, i) for i in range(width // 512)]
        slots = [1, 2, 4, 5, 7, 8, 11]
        for n, item in enumerate(items):
            item()
            if n in slots:
                k = slots.index(n)
                if ahead[k] is not None:

                    @pl.when(c < N_CHUNK - 1)
                    def _():
                        ahead[k](c + 1)

                else:

                    @pl.when(c < N_CHUNK - 2)
                    def _():
                        behind[k](c + 2)

    outs = [
        pltpu.make_async_copy(a, b, out_sem.at[i])
        for i, (a, b) in enumerate([(w, w_out), (hl, hl_out), (dg, dg_out), (du, du_out), (g, g_out)])
    ]
    for copy in outs:
        copy.start()
    for c in range(N_CHUNK):
        ring.drain(c)
    for copy in outs:
        copy.wait()


def k1(later_in, earlier_in, cot, gain, w_own):
    tokens, width = later_in.shape
    any_ = pl.BlockSpec(memory_space=pl.ANY)
    vm = pl.BlockSpec(memory_space=pltpu.VMEM)
    act = (N_CHUNK, tokens, CHUNK)
    full = (N_CHUNK, width, WIDE)
    return pl.pallas_call(
        k1_body,
        out_shape=[jax.ShapeDtypeStruct(s, BF) for s in (full, act, act, act, full)],
        in_specs=[any_, any_, any_, vm, any_],
        out_specs=[any_] * 5,
        scratch_shapes=[
            pltpu.VMEM(full, BF),
            pltpu.VMEM((tokens, width), BF),
            pltpu.VMEM((tokens, width), BF),
            pltpu.VMEM((width, tokens), BF),
            pltpu.VMEM((tokens, width), BF),
            pltpu.VMEM((width, tokens), BF),
            pltpu.VMEM(act, BF),
            pltpu.VMEM(act, BF),
            pltpu.VMEM(act, BF),
            pltpu.VMEM((tokens, CHUNK), BF),
            pltpu.VMEM(full, BF),
            pltpu.SemaphoreType.DMA((3,)),
            pltpu.SemaphoreType.DMA((N_CHUNK,)),
            pltpu.SemaphoreType.DMA((N_CHUNK, 2, 20)),
            pltpu.SemaphoreType.DMA((N_CHUNK, 2, 20)),
            pltpu.SemaphoreType.DMA((5,)),
        ],
        compiler_params=pltpu.CompilerParams(
            collective_id=0, has_side_effects=True, vmem_limit_bytes=64 * 1024 * 1024 - 65536
        ),
        name="gather_compute",
    )(later_in, earlier_in, cot, gain.reshape(1, width), w_own)


def unit_of(tokens_in):
    v = tokens_in.astype(F32)
    scale = lax.rsqrt(jnp.mean(v * v, axis=1, keepdims=True) + NORM_FLOOR)
    return scale, v * scale


def sum_at_owner(array, axis):
    n = lax.axis_size(axis)
    parts = array.reshape(n, array.shape[0] // n, *array.shape[1:])
    arrived = lax.all_to_all(parts, axis, split_axis=0, concat_axis=0, tiled=True)
    return arrived.astype(F32).sum(axis=0)


def local(later_in, earlier_in, cot, gate_w, up_w, down_w, gain, gate_sum, up_sum, down_sum, gain_sum):
    cols = gate_w.shape[1]
    w_own = jnp.concatenate([pack(gate_w), pack(up_w), pack(down_w)], axis=2)
    w, hl, dg, du, g = k1(later_in, earlier_in, cot, gain, w_own)
    hidden = hl.transpose(1, 0, 2).reshape(hl.shape[1], -1)
    nt = lambda a, b: lax.dot_general(a, b, (((0, 2), (0, 2)), ((), ())), preferred_element_type=F32)
    own = later_in.shape[0] // 8
    at = lax.axis_index(TP) * own
    rows = lambda a: lax.dynamic_slice_in_dim(a, at, own, 0).astype(F32)
    later_sum = lax.psum_scatter(
        nt(hl, w[:, :, 2 * CHUNK :]).astype(BF), TP, scatter_dimension=0, tiled=True
    ).astype(F32)
    later_out = (rows(later_in) + 0.5 * later_sum).astype(BF)
    gs = lax.psum_scatter(g, FS, scatter_dimension=1, tiled=True).astype(F32)
    dn = nt(dg, w[:, :, :CHUNK]) + nt(du, w[:, :, CHUNK : 2 * CHUNK])
    scale, unit = unit_of(earlier_in)
    gain_part = jnp.sum(dn * unit, axis=0)
    weighted = dn * gain.astype(F32)
    branch = scale * (weighted - unit * jnp.mean(weighted * unit, axis=1, keepdims=True))
    earlier_grad = (rows(cot) + sum_at_owner(branch.astype(BF), TP)).astype(BF)
    gain_new = gain_sum + lax.psum(gain_part, ALL)
    gs = gs.transpose(1, 0, 2).reshape(gs.shape[1], N_CHUNK, 3, CHUNK)
    pick = lambda k: gs[:, :, k, :].reshape(gs.shape[0], -1)[:, :cols]
    return (
        later_out, hidden[:, :cols], earlier_grad,
        gate_sum + pick(0), up_sum + pick(1), down_sum + pick(2), gain_new,
    )


def solution(mesh):
    torus = Mesh(mesh.devices.reshape(4, 4, 4, 2), ALL)
    return jax.shard_map(
        local,
        mesh=torus,
        in_specs=(P(FS, None),) * 3 + (P(FS, TP),) * 3 + (P(),) + (P(FS, TP),) * 3 + (P(),),
        out_specs=(P(ALL, None), P(FS, TP), P(ALL, None), P(FS, TP), P(FS, TP), P(FS, TP), P()),
        check_vma=False,
    )
```

time: 253 us -> 264 us (1.043)
  Pallas kernels: 0 us -> 86.3 us
  waiting for transfers between devices: 80.9 us -> 0.72 us
  blocking collectives: 54.4 us -> 108 us
  matrix products: 55.2 us -> 23.9 us
  local copies, waits for them, and re-layouts: 16.6 us -> 7.11 us
  other arithmetic: 25.6 us -> 18.2 us
    pallas_call x0 -> x1, Pallas kernels: none -> 86.3 us  [k1(): pl.pallas_call(k1_body, out_shape=[jax.ShapeDtypeStruct(s, BF) for s in (...]
    all_gather x1 -> x0, waiting for transfers between devices: 78.8 us -> none  [side_by_side(): lax.all_gather(both, axis, axis=dim, tiled=True)]
    psum x4 -> x1, blocking collectives: 54.4 us -> 108 us  [local(): gain_new = gain_sum + lax.psum(gain_part, ALL)]
    dot_general x10 -> x3, matrix products: 55.2 us -> 23.9 us  [local(): lax.dot_general(a, b, (((0, 2), (0, 2)), ((), ())), preferred_element_typ...]
    unnamed x36 -> x18, local copies, waits for them, and re-layouts: 16.6 us -> 0.04 us
    concatenate x2 -> x1, other arithmetic: 6.24 us -> 0.85 us  [local(): w_own = jnp.concatenate([pack(gate_w), pack(up_w), pack(down_w)], axis=2)]
    reduce_sum x3 -> x2, other arithmetic: 9.37 us -> 6.26 us  [the longest x1 3.19 us: unit_of(): scale = lax.rsqrt(jnp.mean(v * v, axis=1, keepdims=True) + NORM_FLOOR)]
    pad x0 -> x3, local copies, waits for them, and re-layouts: none -> 2.81 us  [pack(): w = jnp.pad(w, ((0, 0), (0, N_CHUNK * CHUNK - cols)))]
  transfers between devices with their start and end apart: 4 -> 3, of which waited for: 2 -> 0; matrix products, arithmetic and copies ran while one was open for 30% -> 12% of each run, Pallas kernels for 0% -> 0%
where the time goes in v1:
time: 264 us; the launch traced here: 263 us
  blocking collectives  108 us (41%)
  Pallas kernels  86.3 us (33%)
  matrix products  23.9 us (9%)
  other arithmetic  18.2 us (7%)
  between operations  14.2 us (5%)
  local copies, waits for them, and re-layouts  7.11 us (3%)
  starting transfers between devices  4.78 us (2%)
    psum x1, blocking collectives, local(): gain_new = gain_sum + lax.psum(gain_part, ALL)  108 us
    pallas_call x1, Pallas kernels, k1(): pl.pallas_call(k1_body, out_shape=[jax.ShapeDtypeStruct(s, BF) for s in (...  86.3 us
    dot_general x3, matrix products, local(): lax.dot_general(a, b, (((0, 2), (0, 2)), ((), ())), preferred_element_typ...  23.9 us
    convert_element_type x2, other arithmetic, local(): earlier_grad = (rows(cot) + sum_at_owner(branch.astype(BF), TP)).astype(BF)  5.31 us
  transfers between devices with their start and end apart: 3, of which 0 were waited for; matrix products, arithmetic and copies ran while one was open for 12% of the time, Pallas kernels for 0%

profile of v1, /device:TPU:0, one launch (start us, length us, event | category | flops | bytes accessed | tf_op | source)
XLA Modules:
  0.0 263.1 jit_solution(4595355425486537434)
XLA Ops:
  7.2 0.0 reduce-scatter.3.cloned.1.call-start
  7.2 1.3 reshape.51.gain
  8.5 0.9 pad.10
  9.4 0.1 copy.21
  9.6 0.9 pad.11
  10.5 0.1 copy.22
  10.7 0.9 pad.12
  11.6 0.1 copy.23
  11.8 0.9 pad_maximum_fusion.w_own
  12.6 86.3 %gather_compute.1 = (bf16[3,2048,768]{2,1,0:T(8,128)(2,1)}, bf16[3,1024,256]{2,1,0:T(8,128)(2,1)}, bf16[3,1024,256]{2,1,0:T(8,128)(2,1)}, bf16[3,1024,256]{2,1,0:T(8,128)(2,1)}, bf16[3,2048,768]{2,1,0:T(8,128)(2,1)}) custom-call(bf16[1024,2048]{1,0:T(8,128)(2,1)} %later_in.1, bf16[1024,2048]{1,0:T(8,128)(2,1)} %earlier_in.1, bf16[1024,2048]{1,0:T(8,128)(2,1)} %cot_in.1, ...), custom_call_target="tpu_custom_call" | custom-call | tf_op jit(solution)/shard_map/gather_compute/pallas_call | solution.py:307
  98.9 7.9 %bitcast_convert_fusion = bf16[1024,2048]{1,0:T(8,128)(2,1)} fusion(bf16[3,1024,256]{2,1,0:T(8,128)(2,1)} %get-tuple-element.12, bf16[3,2048,768]{2,1,0:T(8,128)(2,1)} %get-tuple-element.13), kind=kOutput, calls=%fused_computation.12 | convolution fusion | flops 3223322624 | bytes 8912896 | tf_op jit(solution)/shard_map/dot_general | solution.py:355
  106.8 0.0 reduce-scatter.3.cloned.1.call-update
  106.9 0.0 reduce-scatter.5.cloned.1.call-start
  106.9 0.0 copy-start.5
  106.9 0.7 reduce-scatter.5.cloned.1.call-update
  107.6 0.0 copy-done.5
  107.6 0.0 copy-start.8
  107.7 3.2 %fusion.8 = f32[1024]{0:T(1024)S(1)} fusion(bf16[1024,2048]{1,0:T(8,128)(2,1)} %earlier_in.1), kind=kLoop, calls=%fused_computation.10 | loop fusion | flops 6290432 | bytes 4198400 | tf_op jit(solution)/shard_map/reduce_sum | solution.py:339
  110.9 0.0 copy-done.8
  110.9 0.0 copy-start
  110.9 0.0 copy-start.7
  110.9 7.8 %fusion.10 = f32[1024,2048,1]{1,0,2:T(8,128)} fusion(bf16[3,1024,256]{2,1,0:T(8,128)(2,1)S(1)} %copy-done.8, bf16[3,2048,768]{2,1,0:T(8,128)(2,1)} %get-tuple-element.13), kind=kOutput, calls=%fused_computation.15 | convolution fusion | flops 3221225472 | bytes 13107200 | tf_op jit(solution)/shard_map/dot_general | solution.py:355
  118.6 0.0 copy-done
  118.6 0.0 copy-done.7
  118.6 8.2 %fusion.7 = (f32[2048]{0:T(1024)S(1)}, f32[1024]{0:T(1024)S(1)}, f32[1024,2048]{1,0:T(8,128)S(1)}) fusion(bf16[1024,2048]{1,0:T(8,128)(2,1)S(1)} %copy-done, f32[1024]{0:T(1024)S(1)} %add_rsqrt_fusion, f32[2048]{0:T(1024)S(1)} %convert_element_type.41, bf16[3,1024,256]{2,1,0:T(8,128)(2,1)S(1)} %copy-done.7, bf16[3,2048,768]{2,1,0:T(8,128)(2,1)} %get-tuple-element.13, ...), kind=kOutput, calls=%fused_computation.9 | convolution fusion | flops 3237999616 | bytes 25714688 | tf_op jit(solution)/shard_map/dot_general | solution.py:355
  126.9 3.4 %fusion.6 = bf16[1024,2048]{1,0:T(8,128)(2,1)} fusion(bf16[1024,2048]{1,0:T(8,128)(2,1)S(1)} %copy-done, f32[1024,2048]{1,0:T(8,128)S(1)} %get-tuple-element.22, f32[1024]{0:T(1024)S(1)} %broadcast_multiply_fusion, f32[2048]{0:T(1024)S(1)} %convert_element_type.41, f32[1024]{0:T(1024)S(1)} %add_rsqrt_fusion), kind=kLoop, calls=%fused_computation.8 | loop fusion | flops 14680064 | bytes 16793600 | tf_op jit(solution)/shard_map/convert_element_type | solution.py:369
  130.2 0.0 copy-start.1
  130.2 4.7 %all-to-all-start = ((bf16[8,128,2048]{2,1,0:T(8,128)(2,1)}), bf16[8,128,2048]{2,1,0:T(8,128)(2,1)}, u32[]{:S(2)}, u32[]{:S(2)}) async-start(bf16[8,128,2048]{2,1,0:T(8,128)(2,1)} %bitcast.24), calls=%async_computation.1 | async-start | bytes 8388608 | tf_op jit(solution)/shard_map/all_to_all | solution.py:346
  134.9 0.0 copy-start.6
  135.0 0.0 copy-done.1
  135.0 0.9 copy.24
  135.9 1.2 slice.40
  137.1 107.9 %psum.7 = f32[2048]{0:T(1024)S(1)} all-reduce(f32[2048]{0:T(1024)S(1)} %get-tuple-element.17), channel_id=1, replica_groups=mesh['z'=4,'x'=4,'y'=4,'c'=2] {'z','x','y','c'}, use_global_device_ids=true, to_apply=%region_6.7 | all-reduce | flops 2048 | bytes 16384 | tf_op jit(solution)/shard_map/psum | solution.py:370
  245.0 0.0 copy-done.6
  245.0 0.6 add.61
  245.6 0.0 all-to-all-done
  245.6 3.1 %convert_reduce_fusion = f32[128,2048]{1,0:T(8,128)S(1)} fusion(bf16[8,128,2048]{2,1,0:T(8,128)(2,1)} %all-to-all-done), kind=kLoop, calls=%fused_computation.13 | loop fusion | flops 3932160 | bytes 5242880 | tf_op jit(solution)/shard_map/reduce_sum | solution.py:347
  248.6 2.0 add_convert_fusion
  250.6 0.0 copy-start.2
  250.6 0.0 copy-start.3
  250.6 0.0 copy-start.4
  250.6 0.0 reduce-scatter.3.cloned.1.call-done
  250.6 2.3 add_convert_fusion.1
  252.9 0.0 reduce-scatter.5.cloned.1.call-done
  252.9 1.1 convert_bitcast_fusion
  254.1 0.4 copy.25
  254.4 0.1 fusion.13
  254.5 0.0 copy-done.2
  254.5 0.8 slice_add_fusion.2
  255.3 0.0 copy-done.3
  255.3 0.0 copy-done.4
  255.3 0.9 slice_add_fusion
  (3 shorter events, 0.0 us)
Async XLA Ops:
  7.2 243.4 %reduce-scatter.3.cloned.1.call-start = ((), (), s32[]{:S(2)}) async-start(), calls=%async_computation.3 | async-start | bytes 4718592 | tf_op jit(solution)/shard_map/reduce_scatter | solution.py:359
  106.9 146.0 %reduce-scatter.5.cloned.1.call-start = ((), (), s32[]{:S(2)}) async-start(), calls=%async_computation.4 | async-start | bytes 10027008 | tf_op jit(solution)/shard_map/reduce_scatter | solution.py:363
  106.9 0.7 copy-start.5
  107.6 3.2 %copy-start.8 = (bf16[3,1024,256]{2,1,0:T(8,128)(2,1)S(1)}, bf16[3,1024,256]{2,1,0:T(8,128)(2,1)}, u32[]{:S(2)}) copy-start(bf16[3,1024,256]{2,1,0:T(8,128)(2,1)} %get-tuple-element.14) | copy-start | bytes 4718596
  110.9 7.8 %copy-start = (bf16[1024,2048]{1,0:T(8,128)(2,1)S(1)}, bf16[1024,2048]{1,0:T(8,128)(2,1)}, u32[]{:S(2)}) copy-start(bf16[1024,2048]{1,0:T(8,128)(2,1)} %earlier_in.1) | copy-start | bytes 12582916
  110.9 7.8 %copy-start.7 = (bf16[3,1024,256]{2,1,0:T(8,128)(2,1)S(1)}, bf16[3,1024,256]{2,1,0:T(8,128)(2,1)}, u32[]{:S(2)}) copy-start(bf16[3,1024,256]{2,1,0:T(8,128)(2,1)} %get-tuple-element.15) | copy-start | bytes 4718596
  130.2 4.7 %copy-start.1 = (bf16[3,1024,256]{2,1,0:T(8,128)(2,1)S(1)}, bf16[3,1024,256]{2,1,0:T(8,128)(2,1)}, u32[]{:S(2)}) copy-start(bf16[3,1024,256]{2,1,0:T(8,128)(2,1)} %get-tuple-element.12) | copy-start | bytes 4718596
  130.2 115.3 %all-to-all-start = ((bf16[8,128,2048]{2,1,0:T(8,128)(2,1)}), bf16[8,128,2048]{2,1,0:T(8,128)(2,1)}, u32[]{:S(2)}, u32[]{:S(2)}) async-start(bf16[8,128,2048]{2,1,0:T(8,128)(2,1)} %bitcast.24), calls=%async_computation.1 | async-start | bytes 8388608 | tf_op jit(solution)/shard_map/all_to_all | solution.py:346
  134.9 110.0 %copy-start.6 = (f32[2048]{0:T(1024)S(1)}, f32[2048]{0:T(1024)}, u32[]{:S(2)}) copy-start(f32[2048]{0:T(1024)} %param.21) | copy-start | bytes 24580
  250.6 3.9 %copy-start.2 = (f32[128,704]{0,1:T(8,128)S(1)}, f32[128,704]{0,1:T(8,128)}, u32[]{:S(2)}) copy-start(f32[128,704]{0,1:T(8,128)} %param.18) | copy-start | bytes 1081348
  250.6 4.7 %copy-start.3 = (f32[128,704]{0,1:T(8,128)S(1)}, f32[128,704]{0,1:T(8,128)}, u32[]{:S(2)}) copy-start(f32[128,704]{0,1:T(8,128)} %param.20) | copy-start | bytes 1081348
  250.6 4.7 %copy-start.4 = (f32[128,704]{0,1:T(8,128)S(1)}, f32[128,704]{0,1:T(8,128)}, u32[]{:S(2)}) copy-start(f32[128,704]{0,1:T(8,128)} %param.19) | copy-start | bytes 1081348
Sparse Core Ops, SparseCore 0:
  107.0 51.0 reduce-scatter.2
  161.6 90.5 reduce-scatter.4

commit v2 on v1

--- a/solution.py
+++ b/solution.py
@@ -334,17 +334,373 @@
     )(later_in, earlier_in, cot, gain.reshape(1, width), w_own)
 
 
-def unit_of(tokens_in):
-    v = tokens_in.astype(F32)
-    scale = lax.rsqrt(jnp.mean(v * v, axis=1, keepdims=True) + NORM_FLOOR)
-    return scale, v * scale
-
-
-def sum_at_owner(array, axis):
-    n = lax.axis_size(axis)
-    parts = array.reshape(n, array.shape[0] // n, *array.shape[1:])
-    arrived = lax.all_to_all(parts, axis, split_axis=0, concat_axis=0, tiled=True)
-    return arrived.astype(F32).sum(axis=0)
+class Scatter:
+    def __init__(self, g, r1, r2, r3, r4, send, recv, out):
+        self.g, self.r = g, (r1, r2, r3, r4)
+        self.send, self.recv, self.out = send, recv, out
+        self.at = {"z": lax.axis_index("z"), "x": lax.axis_index("x")}
+
+    def unit(self, c, h, jf, js=None, sub=None):
+        r0, n = h * 64, 64
+        if sub is not None:
+            r0, n = r0 + sub * 32, 32
+        fast, slow = (("x", "z"), ("z", "x"))[h]
+        f = lax.rem(self.at[fast] + jf + 4, 4)
+        s = slice(None) if js is None else lax.rem(self.at[slow] + js + 4, 4)
+        where = (s, f) if h == 0 else (f, s)
+        return self.g.at[(c, *where, slice(r0, r0 + n), slice(None))]
+
+    def copy(self, stage, c, h, d, src):
+        i = 0 if d > 0 else 1
+        name = (("x", "z"), ("z", "x"))[h][stage // 2]
+        m = stage * 2 + i
+        return pltpu.make_async_remote_copy(
+            src_ref=src,
+            dst_ref=self.r[stage].at[c, h, i],
+            send_sem=self.send.at[c, h, m],
+            recv_sem=self.recv.at[c, h, m],
+            device_id={name: lax.rem(self.at[name] + d + 4, 4)},
+            device_id_type=MESH,
+        )
+
+    def c1(self, c, h, d):
+        return self.copy(0, c, h, d, self.unit(c, h, 2, None, 0 if d > 0 else 1))
+
+    def c2(self, c, h, d):
+        return self.copy(1, c, h, d, self.unit(c, h, d))
+
+    def c3(self, c, h, d):
+        return self.copy(2, c, h, d, self.unit(c, h, 0, 2, 0 if d > 0 else 1))
+
+    def c4(self, c, h, d):
+        return self.copy(3, c, h, d, self.unit(c, h, 0, d))
+
+    def s1(self, c):
+        for h in (0, 1):
+            for d in (1, -1):
+                self.c1(c, h, d).start()
+
+    def a1(self, c):
+        for d in (1, -1):
+            for h in (0, 1):
+                i = 0 if d > 0 else 1
+                self.c1(c, h, d).wait_recv()
+                part = self.unit(c, h, d, None, i)
+                for k in range(4):
+                    part[k] = part[k] + self.r[0][c, h, i, k]
+                self.c2(c, h, d).start()
+
+    def a2(self, c):
+        for h in (0, 1):
+            for d in (1, -1):
+                self.c2(c, h, d).wait_recv()
+            whole = self.unit(c, h, 0)
+            for k in range(4):
+                whole[k] = (
+                    whole[k].astype(F32) + self.r[1][c, h, 0, k].astype(F32) + self.r[1][c, h, 1, k].astype(F32)
+                ).astype(BF)
+            for d in (1, -1):
+                self.c3(c, h, d).start()
+
+    def a3(self, c):
+        for d in (1, -1):
+            for h in (0, 1):
+                i = 0 if d > 0 else 1
+                self.c3(c, h, d).wait_recv()
+                part = self.unit(c, h, 0, d, i)
+                part[...] = part[...] + self.r[2][c, h, i]
+                self.c4(c, h, d).start()
+
+    def a4(self, c):
+        for h in (0, 1):
+            for d in (1, -1):
+                self.c4(c, h, d).wait_recv()
+            own = self.unit(c, h, 0, 0)
+            self.out[c, h * 64 : h * 64 + 64, :] = (
+                own[...].astype(F32) + self.r[3][c, h, 0].astype(F32) + self.r[3][c, h, 1].astype(F32)
+            )
+
+    def drain(self, c):
+        for h in (0, 1):
+            for d in (1, -1):
+                for copy in (self.c1, self.c2, self.c3, self.c4):
+                    copy(c, h, d).wait_send()
+
+
+class TokenScatter:
+    def __init__(self, t, p, rc, q1, q2, send, recv, out):
+        self.t, self.p, self.rc, self.q1, self.q2 = t, p, rc, q1, q2
+        self.send, self.recv, self.out = send, recv, out
+        self.y, self.c = lax.axis_index("y"), lax.axis_index("c")
+
+    def to(self, k):
+        return lax.rem(self.y + k + 4, 4)
+
+    def pair(self, k):
+        return pltpu.make_async_remote_copy(
+            src_ref=self.p.at[self.to(k), 1 - self.c],
+            dst_ref=self.rc.at[self.to(k)],
+            send_sem=self.send.at[self.t, k % 4],
+            recv_sem=self.recv.at[self.t, k % 4],
+            device_id={"c": 1 - self.c},
+            device_id_type=MESH,
+        )
+
+    def ring(self, src, dst, m, d):
+        return pltpu.make_async_remote_copy(
+            src_ref=src,
+            dst_ref=dst,
+            send_sem=self.send.at[self.t, m],
+            recv_sem=self.recv.at[self.t, m],
+            device_id={"y": self.to(d)},
+            device_id_type=MESH,
+        )
+
+    def y1(self, d):
+        i = 0 if d > 0 else 1
+        return self.ring(self.p.at[self.to(2), self.c, i * 64 : i * 64 + 64], self.q1.at[self.t, i], 4 + i, d)
+
+    def y2(self, d):
+        i = 0 if d > 0 else 1
+        return self.ring(self.p.at[self.to(d), self.c], self.q2.at[self.t, i], 6 + i, d)
+
+    def share(self, k):
+        self.pair(k).start()
+
+    def join(self, k):
+        self.pair(k).wait_recv()
+        mine = self.p.at[self.to(k), self.c]
+        mine[...] = mine[...] + self.rc[self.to(k)]
+
+    def far(self):
+        self.join(2)
+        for d in (1, -1):
+            self.y1(d).start()
+
+    def near(self, d):
+        i = 0 if d > 0 else 1
+        self.join(d)
+        self.y1(d).wait_recv()
+        part = self.p.at[self.to(d), self.c, i * 64 : i * 64 + 64]
+        part[...] = part[...] + self.q1[self.t, i]
+        self.y2(d).start()
+
+    def finish(self):
+        self.join(0)
+        for d in (1, -1):
+            self.y2(d).wait_recv()
+        self.out[...] = (
+            self.p[self.y, self.c].astype(F32) + self.q2[self.t, 0].astype(F32) + self.q2[self.t, 1].astype(F32)
+        )
+
+    def drain(self):
+        for k in (0, 1, 2, -1):
+            self.pair(k).wait_send()
+        for d in (1, -1):
+            self.y1(d).wait_send()
+            self.y2(d).wait_send()
+
+
+def butterfly():
+    steps = [("c", 1 - lax.axis_index("c"))]
+    for name in ("y", "x", "z"):
+        me = lax.axis_index(name)
+        steps.append((name, me + 1 - 2 * lax.rem(me, 2)))
+        steps.append((name, 3 - me))
+    return steps
+
+
+class GainSum:
+    def __init__(self, mine, theirs, send, recv):
+        self.mine, self.theirs, self.send, self.recv = mine, theirs, send, recv
+        self.steps = butterfly()
+
+    def copy(self, i):
+        name, partner = self.steps[i]
+        return pltpu.make_async_remote_copy(
+            src_ref=self.mine.at[i],
+            dst_ref=self.theirs.at[i],
+            send_sem=self.send.at[i],
+            recv_sem=self.recv.at[i],
+            device_id={name: partner},
+            device_id_type=MESH,
+        )
+
+    def start(self, i):
+        self.copy(i).start()
+
+    def end(self, i):
+        self.copy(i).wait_recv()
+        self.mine[i + 1] = self.mine[i] + self.theirs[i]
+
+    def drain(self):
+        for i in range(7):
+            self.copy(i).wait_send()
+
+
+def nt(a, b):
+    return lax.dot_general(a, b, (((1,), (1,)), ((), ())), preferred_element_type=F32)
+
+
+def k2_body(
+    g_in, w_in, hl_in, dg_in, du_in, earlier_in, gain,
+    gs_out, later_out, earlier_out, gain_out,
+    g, w, hl, dg, du, x, p, rc, q1, q2, r1, r2, r3, r4, dn, gacc, gmine, gtheirs,
+    in_sem, send, recv, tsend, trecv, gsend, grecv,
+):
+    loads = [pltpu.make_async_copy(g_in.at[c], g.at[c], in_sem.at[c]) for c in range(N_CHUNK)]
+    loads += [
+        pltpu.make_async_copy(a, b, in_sem.at[3 + i])
+        for i, (a, b) in enumerate([(w_in, w), (hl_in, hl), (dg_in, dg), (du_in, du), (earlier_in, x)])
+    ]
+    for copy in loads:
+        copy.start()
+    greet(ring_peers(("x", "z", "y")) + [{"c": 1 - lax.axis_index("c")}])
+    rs = Scatter(g, r1, r2, r3, r4, send, recv, gs_out)
+    later = TokenScatter(0, p.at[0], rc.at[0], q1, q2, tsend, trecv, later_out)
+    earlier = TokenScatter(1, p.at[1], rc.at[1], q1, q2, tsend, trecv, earlier_out)
+    total = GainSum(gmine, gtheirs, gsend, grecv)
+    gain_row = gain[...].astype(F32)
+    y = lax.axis_index("y")
+
+    def later_block(k):
+        b = lax.rem(y + k + 4, 4)
+        rows = pl.ds(pl.multiple_of(b * 256, 256), 256)
+        out = nt(hl[0, rows, :], w[0, :, 2 * CHUNK :])
+        for c in range(1, N_CHUNK):
+            out = out + nt(hl[c, rows, :], w[c, :, 2 * CHUNK :])
+        p[0, b, 0] = out[:128].astype(BF)
+        p[0, b, 1] = out[128:].astype(BF)
+        later.share(k)
+
+    def earlier_block(k):
+        b = lax.rem(y + k + 4, 4)
+        rows = pl.ds(pl.multiple_of(b * 256, 256), 256)
+        out = nt(dg[0, rows, :], w[0, :, :CHUNK])
+        out = out + nt(du[0, rows, :], w[0, :, CHUNK : 2 * CHUNK])
+        for c in range(1, N_CHUNK):
+            out = out + nt(dg[c, rows, :], w[c, :, :CHUNK])
+            out = out + nt(du[c, rows, :], w[c, :, CHUNK : 2 * CHUNK])
+        dn[...] = out
+
+        for half in (0, 1):
+
+            @pl.loop(0, 8)
+            def _(i):
+                at = half * 128 + i * 16
+                v = x[pl.ds(pl.multiple_of(b * 256 + at, 16), 16), :].astype(F32)
+                scale = lax.rsqrt(jnp.mean(v * v, axis=1, keepdims=True) + NORM_FLOOR)
+                unit = v * scale
+                d = dn[pl.ds(pl.multiple_of(at, 16), 16), :]
+                du_ = d * unit
+                gacc[...] += du_[:8] + du_[8:]
+                mean = jnp.mean(du_ * gain_row, axis=1, keepdims=True)
+                branch = scale * (d * gain_row - unit * mean)
+                p[1, b, half, pl.ds(pl.multiple_of(i * 16, 16), 16), :] = branch.astype(BF)
+
+        earlier.share(k)
+
+    gacc[...] = jnp.zeros_like(gacc)
+    for c in (0, 1):
+        loads[c].wait()
+        rs.s1(c)
+    loads[3].wait()
+    loads[4].wait()
+    later_block(2)
+    rs.a1(0)
+    loads[2].wait()
+    rs.s1(2)
+    later_block(1)
+    rs.a1(1)
+    later.far()
+    later_block(-1)
+    rs.a2(0)
+    later_block(0)
+    later.near(1)
+    later.near(-1)
+    rs.a1(2)
+    for copy in loads[5:]:
+        copy.wait()
+    earlier_block(2)
+    rs.a3(0)
+    rs.a2(1)
+    earlier_block(1)
+    earlier.far()
+    rs.a4(0)
+    rs.a3(1)
+    earlier_block(-1)
+    rs.a2(2)
+    earlier_block(0)
+    later.finish()
+    gmine[0] = jnp.sum(gacc[...], axis=0, keepdims=True)
+    total.start(0)
+    earlier.near(1)
+    earlier.near(-1)
+    total.end(0)
+    total.start(1)
+    rs.a4(1)
+    rs.a3(2)
+    for i in range(1, 6):
+        total.end(i)
+        total.start(i + 1)
+    total.end(6)
+    gain_out[...] = gmine[7]
+    earlier.finish()
+    rs.a4(2)
+    for c in range(N_CHUNK):
+        rs.drain(c)
+    later.drain()
+    earlier.drain()
+    total.drain()
+
+
+def k2(g, w, hl, dg, du, earlier_in, gain):
+    tokens, width = earlier_in.shape
+    any_ = pl.BlockSpec(memory_space=pl.ANY)
+    vm = pl.BlockSpec(memory_space=pltpu.VMEM)
+    act = (N_CHUNK, tokens, CHUNK)
+    return pl.pallas_call(
+        k2_body,
+        out_shape=[
+            jax.ShapeDtypeStruct((N_CHUNK, SHARD, WIDE), F32),
+            jax.ShapeDtypeStruct((tokens // 8, width), F32),
+            jax.ShapeDtypeStruct((tokens // 8, width), F32),
+            jax.ShapeDtypeStruct((1, width), F32),
+        ],
+        in_specs=[any_] * 6 + [vm],
+        out_specs=[vm] * 4,
+        scratch_shapes=[
+            pltpu.VMEM((N_CHUNK, 4, 4, SHARD, WIDE), BF),
+            pltpu.VMEM((N_CHUNK, width, WIDE), BF),
+            pltpu.VMEM(act, BF),
+            pltpu.VMEM(act, BF),
+            pltpu.VMEM(act, BF),
+            pltpu.VMEM((tokens, width), BF),
+            pltpu.VMEM((2, 4, 2, SHARD, width), BF),
+            pltpu.VMEM((2, 4, SHARD, width), BF),
+            pltpu.VMEM((2, 2, SHARD // 2, width), BF),
+            pltpu.VMEM((2, 2, SHARD, width), BF),
+            pltpu.VMEM((N_CHUNK, 2, 2, 4, SHARD // 4, WIDE), BF),
+            pltpu.VMEM((N_CHUNK, 2, 2, 4, SHARD // 2, WIDE), BF),
+            pltpu.VMEM((N_CHUNK, 2, 2, SHARD // 4, WIDE), BF),
+            pltpu.VMEM((N_CHUNK, 2, 2, SHARD // 2, WIDE), BF),
+            pltpu.VMEM((256, width), F32),
+            pltpu.VMEM((8, width), F32),
+            pltpu.VMEM((8, 1, width), F32),
+            pltpu.VMEM((7, 1, width), F32),
+            pltpu.SemaphoreType.DMA((8,)),
+            pltpu.SemaphoreType.DMA((N_CHUNK, 2, 8)),
+            pltpu.SemaphoreType.DMA((N_CHUNK, 2, 8)),
+            pltpu.SemaphoreType.DMA((2, 8)),
+            pltpu.SemaphoreType.DMA((2, 8)),
+            pltpu.SemaphoreType.DMA((7,)),
+            pltpu.SemaphoreType.DMA((7,)),
+        ],
+        compiler_params=pltpu.CompilerParams(
+            collective_id=1, has_side_effects=True, vmem_limit_bytes=64 * 1024 * 1024 - 65536
+        ),
+        name="scatter_compute",
+    )(g.reshape(N_CHUNK, 4, 4, SHARD, WIDE), w, hl, dg, du, earlier_in, gain.reshape(1, width))
 
 
 def local(later_in, earlier_in, cot, gate_w, up_w, down_w, gain, gate_sum, up_sum, down_sum, gain_sum):
@@ -352,22 +708,13 @@
     w_own = jnp.concatenate([pack(gate_w), pack(up_w), pack(down_w)], axis=2)
     w, hl, dg, du, g = k1(later_in, earlier_in, cot, gain, w_own)
     hidden = hl.transpose(1, 0, 2).reshape(hl.shape[1], -1)
-    nt = lambda a, b: lax.dot_general(a, b, (((0, 2), (0, 2)), ((), ())), preferred_element_type=F32)
     own = later_in.shape[0] // 8
     at = lax.axis_index(TP) * own
     rows = lambda a: lax.dynamic_slice_in_dim(a, at, own, 0).astype(F32)
-    later_sum = lax.psum_scatter(
-        nt(hl, w[:, :, 2 * CHUNK :]).astype(BF), TP, scatter_dimension=0, tiled=True
-    ).astype(F32)
+    gs, later_sum, earlier_sum, gain_total = k2(g, w, hl, dg, du, earlier_in, gain)
     later_out = (rows(later_in) + 0.5 * later_sum).astype(BF)
-    gs = lax.psum_scatter(g, FS, scatter_dimension=1, tiled=True).astype(F32)
-    dn = nt(dg, w[:, :, :CHUNK]) + nt(du, w[:, :, CHUNK : 2 * CHUNK])
-    scale, unit = unit_of(earlier_in)
-    gain_part = jnp.sum(dn * unit, axis=0)
-    weighted = dn * gain.astype(F32)
-    branch = scale * (weighted - unit * jnp.mean(weighted * unit, axis=1, keepdims=True))
-    earlier_grad = (rows(cot) + sum_at_owner(branch.astype(BF), TP)).astype(BF)
-    gain_new = gain_sum + lax.psum(gain_part, ALL)
+    earlier_grad = (rows(cot) + earlier_sum).astype(BF)
+    gain_new = gain_sum + gain_total[0]
     gs = gs.transpose(1, 0, 2).reshape(gs.shape[1], N_CHUNK, 3, CHUNK)
     pick = lambda k: gs[:, :, k, :].reshape(gs.shape[0], -1)[:, :cols]
     return (

time: 264 us -> 190 us (0.72)
  blocking collectives: 108 us -> 0 us
  Pallas kernels: 86.3 us -> 175 us
  matrix products: 23.9 us -> 0 us
  between operations: 14.2 us -> 0.76 us
  other arithmetic: 18.2 us -> 6.34 us
  starting transfers between devices: 4.78 us -> 0 us
    psum x1 -> x0, blocking collectives: 108 us -> none  [local(): gain_new = gain_sum + lax.psum(gain_part, ALL)]
    pallas_call x0 -> x1, Pallas kernels: none -> 88.7 us  [k2(): pl.pallas_call(k2_body, out_shape=[jax.ShapeDtypeStruct((N_CHUNK, SHARD,...]
    dot_general x3 -> x0, matrix products: 23.9 us -> none  [local(): lax.dot_general(a, b, (((0, 2), (0, 2)), ((), ())), preferred_element_typ...]
    reduce_sum x2 -> x0, other arithmetic: 6.26 us -> none  [the longest x1 3.19 us: unit_of(): scale = lax.rsqrt(jnp.mean(v * v, axis=1, keepdims=True) + NORM_FLOOR)]
    all_to_all x1 -> x0, starting transfers between devices: 4.7 us -> none  [sum_at_owner(): lax.all_to_all(parts, axis, split_axis=0, concat_axis=0, tiled=True)]
    convert_element_type x4 -> x1, other arithmetic: 7.59 us -> 3.19 us  [local(): earlier_grad = (rows(cot) + earlier_sum).astype(BF)]
  transfers between devices with their start and end apart: 3 -> 0, of which waited for: 0 -> 0; matrix products, arithmetic and copies ran while one was open for 12% -> 0% of each run, Pallas kernels for 0% -> 0%
where the time goes in v2:
time: 190 us; the launch traced here: 189 us
  Pallas kernels  175 us (92%)
  local copies, waits for them, and re-layouts  7.17 us (4%)
  other arithmetic  6.34 us (3%)
    pallas_call x1, Pallas kernels, k2(): pl.pallas_call(k2_body, out_shape=[jax.ShapeDtypeStruct((N_CHUNK, SHARD,...  88.7 us
    pallas_call x1, Pallas kernels, k1(): pl.pallas_call(k1_body, out_shape=[jax.ShapeDtypeStruct(s, BF) for s in (...  86.3 us

profile of v2, /device:TPU:0, one launch (start us, length us, event | category | flops | bytes accessed | tf_op | source)
XLA Modules:
  0.0 189.3 jit_solution(15684027559638026479)
XLA Ops:
  0.6 0.0 copy-start.5
  0.6 1.3 reshape.36.gain
  2.0 0.9 pad.10
  2.9 0.1 copy.21
  3.1 0.9 pad.11
  4.0 0.1 copy.22
  4.2 0.0 copy-done.5
  4.2 0.1 copy.23
  4.3 0.9 pad_maximum_fusion.w_own
  5.2 86.3 %gather_compute.1 = (bf16[3,2048,768]{2,1,0:T(8,128)(2,1)}, bf16[3,1024,256]{2,1,0:T(8,128)(2,1)}, bf16[3,1024,256]{2,1,0:T(8,128)(2,1)}, bf16[3,1024,256]{2,1,0:T(8,128)(2,1)}, bf16[3,2048,768]{2,1,0:T(8,128)(2,1)}) custom-call(bf16[1024,2048]{1,0:T(8,128)(2,1)} %later_in.1, bf16[1024,2048]{1,0:T(8,128)(2,1)} %earlier_in.3, bf16[1024,2048]{1,0:T(8,128)(2,1)} %cot_in.1, ...), custom_call_target="tpu_custom_call" | custom-call | tf_op jit(solution)/shard_map/gather_compute/pallas_call | solution.py:307
  91.5 88.7 %scatter_compute.1 = (f32[3,128,768]{2,1,0:T(8,128)}, f32[128,2048]{1,0:T(8,128)}, f32[128,2048]{1,0:T(8,128)}, f32[1,2048]{1,0:T(1,128)}) custom-call(bf16[3,4,4,128,768]{4,3,2,1,0:T(8,128)(2,1)} %bitcast.15, bf16[3,2048,768]{2,1,0:T(8,128)(2,1)} %get-tuple-element.17.w_in, bf16[3,1024,256]{2,1,0:T(8,128)(2,1)} %get-tuple-element.18.hl_in, ...), custom_call_target="tpu_custom_call" | custom-call | tf_op jit(solution)/shard_map/scatter_compute/pallas_call | solution.py:662
  180.2 0.0 copy-start.1
  180.2 3.2 %add_convert_fusion = (bf16[128,2048]{1,0:T(8,128)(2,1)}, bf16[128,2048]{1,0:T(8,128)(2,1)}) fusion(f32[128,2048]{1,0:T(8,128)} %get-tuple-element.22, bf16[1024,2048]{1,0:T(8,128)(2,1)} %cot_in.1, s32[]{:T(128)S(6)} %select_n.4, f32[128,2048]{1,0:T(8,128)} %get-tuple-element.21, bf16[1024,2048]{1,0:T(8,128)(2,1)} %later_in.1), kind=kLoop, calls=%fused_computation | loop fusion | flops 1835008 | bytes 4194308 | tf_op jit(solution)/shard_map/convert_element_type | solution.py:716
  183.4 0.0 copy-done.1
  183.4 0.4 copy.25
  183.8 0.0 copy-start.3
  183.8 0.0 copy-start.4
  183.8 0.1 fusion
  183.9 0.0 copy-start.2
  183.9 0.9 copy-done.3
  184.8 0.1 copy-done.4
  184.9 0.0 copy-start.6
  184.9 0.0 copy-start.7
  184.9 0.0 copy-start
  184.9 0.9 slice_add_fusion
  185.8 0.0 copy-done.2
  185.8 0.8 slice_add_fusion.2
  186.6 0.0 copy-done.6
  186.6 0.0 copy-done.7
  186.6 0.6 add.38
  187.2 0.0 copy-done
  187.2 0.9 copy.24
  188.1 1.2 slice.28
  (1 shorter events, 0.0 us)
Async XLA Ops:
  0.6 3.5 %copy-start.5 = (bf16[128,704]{0,1:T(8,128)(2,1)S(1)}, bf16[128,704]{0,1:T(8,128)(2,1)}, u32[]{:S(2)}) copy-start(bf16[128,704]{0,1:T(8,128)(2,1)} %param.16) | copy-start | bytes 540676
  180.2 3.2 %copy-start.1 = (f32[3,128,768]{2,1,0:T(8,128)S(1)}, f32[3,128,768]{2,1,0:T(8,128)}, u32[]{:S(2)}) copy-start(f32[3,128,768]{2,1,0:T(8,128)} %get-tuple-element.23) | copy-start | bytes 3538948
  183.8 1.0 copy-start.3
  183.8 1.1 copy-start.4
  183.9 1.9 %copy-start.2 = (f32[128,704]{0,1:T(8,128)S(1)}, f32[128,704]{0,1:T(8,128)}, u32[]{:S(2)}) copy-start(f32[128,704]{0,1:T(8,128)} %param.18) | copy-start | bytes 1081348
  184.9 1.7 copy-start.6
  184.9 1.7 copy-start.7
  184.9 2.3 %copy-start = (bf16[3,1024,256]{2,1,0:T(8,128)(2,1)S(1)}, bf16[3,1024,256]{2,1,0:T(8,128)(2,1)}, u32[]{:S(2)}) copy-start(bf16[3,1024,256]{2,1,0:T(8,128)(2,1)} %get-tuple-element.18.hl_in) | copy-start | bytes 4718596

commit v3 on v1

v3 whole, which is shorter than its diff:
```python
import functools

import jax
import jax.numpy as jnp
from jax import lax
from jax.experimental import pallas as pl
from jax.experimental.pallas import tpu as pltpu
from jax.sharding import Mesh
from jax.sharding import PartitionSpec as P

FS = ("z", "x")
TP = ("y", "c")
ALL = ("z", "x", "y", "c")
MESH = pl.DeviceIdType.MESH
BF = jnp.bfloat16
F32 = jnp.float32
CHUNK = 256
N_CHUNK = 3
WIDE = 3 * CHUNK
SHARD = 128
NORM_FLOOR = 0.05


class Gather:
    def __init__(self, w, send, recv):
        self.w, self.send, self.recv = w, send, recv
        self.mz, self.mx = lax.axis_index("z"), lax.axis_index("x")

    def owner(self, h, jf, js):
        dx, dz = (jf, js) if h == 0 else (js, jf)
        return lax.rem(self.mz + dz + 4, 4) * 4 + lax.rem(self.mx + dx + 4, 4)

    def copy(self, c, h, msg, jf, js, sub, axis, d):
        start = self.owner(h, jf, js) * SHARD + h * (SHARD // 2)
        size = SHARD // 2
        if sub is not None:
            size = SHARD // 4
            start = start + sub * size
        view = self.w.at[c, pl.ds(pl.multiple_of(start, 32), size), :]
        name = ("x", "z")[h] if axis == "f" else ("z", "x")[h]
        me = self.mx if name == "x" else self.mz
        return pltpu.make_async_remote_copy(
            src_ref=view,
            dst_ref=view,
            send_sem=self.send.at[c, h, msg],
            recv_sem=self.recv.at[c, h, msg],
            device_id={name: lax.rem(me + d + 4, 4)},
            device_id_type=MESH,
        )

    def m1(self, c, h, d):
        return self.copy(c, h, 0 if d > 0 else 1, 0, 0, None, "f", d)

    def r1(self, c, h, d):
        return self.copy(c, h, 0 if d > 0 else 1, -d, 0, None, "f", d)

    def m2(self, c, h, d):
        return self.copy(c, h, 2 if d > 0 else 3, -d, 0, 0 if d > 0 else 1, "f", d)

    def r2(self, c, h, d):
        return self.copy(c, h, 2 if d > 0 else 3, -2 * d, 0, 0 if d > 0 else 1, "f", d)

    def m3(self, c, h, j, d):
        return self.copy(c, h, 4 + 2 * (j % 4) + (0 if d > 0 else 1), j, 0, None, "s", d)

    def r3(self, c, h, j, d):
        return self.copy(c, h, 4 + 2 * (j % 4) + (0 if d > 0 else 1), j, -d, None, "s", d)

    def m4(self, c, h, j, d):
        return self.copy(c, h, 12 + 2 * (j % 4) + (0 if d > 0 else 1), j, -d, 0 if d > 0 else 1, "s", d)

    def r4(self, c, h, j, d):
        return self.copy(c, h, 12 + 2 * (j % 4) + (0 if d > 0 else 1), j, -2 * d, 0 if d > 0 else 1, "s", d)

    def t0(self, c):
        for h in (0, 1):
            for d in (1, -1):
                self.m1(c, h, d).start()
        for h in (0, 1):
            for d in (1, -1):
                self.m3(c, h, 0, d).start()

    def t1(self, c):
        for d in (1, -1):
            for h in (0, 1):
                self.r1(c, h, d).wait_recv()
                self.m2(c, h, d).start()
                for e in (1, -1):
                    self.m3(c, h, -d, e).start()

    def pass_on(self, c, js):
        for j in js:
            for d in (1, -1):
                for h in (0, 1):
                    self.r3(c, h, j, d).wait_recv()
                    self.m4(c, h, j, d).start()

    def t2(self, c):
        self.pass_on(c, (0,))

    def t3(self, c):
        for h in (0, 1):
            for d in (1, -1):
                self.r2(c, h, d).wait_recv()
            for e in (1, -1):
                self.m3(c, h, 2, e).start()

    def t4(self, c):
        self.pass_on(c, (-1, 1))

    def t5(self, c):
        self.pass_on(c, (2,))

    def t6(self, c):
        for h in (0, 1):
            for j in (0, -1, 1, 2):
                for d in (1, -1):
                    self.r4(c, h, j, d).wait_recv()

    def drain(self, c):
        for h in (0, 1):
            for d in (1, -1):
                self.m1(c, h, d).wait_send()
                self.m2(c, h, d).wait_send()
                for j in (0, -1, 1, 2):
                    self.m3(c, h, j, d).wait_send()
                    self.m4(c, h, j, d).wait_send()


def greet(peers):
    barrier = pltpu.get_barrier_semaphore()
    for peer in peers:
        pl.semaphore_signal(barrier, inc=1, device_id=peer, device_id_type=MESH)
    pl.semaphore_wait(barrier, len(peers))


def ring_peers(names):
    peers = []
    for name in names:
        me = lax.axis_index(name)
        for d in (1, 3):
            peers.append({name: lax.rem(me + d, 4)})
    return peers


def nn(a, b):
    return jnp.dot(a, b, preferred_element_type=F32)


class Scatter:
    def __init__(self, g, r1, r2, r3, r4, send, recv, out):
        self.g, self.r = g, (r1, r2, r3, r4)
        self.send, self.recv, self.out = send, recv, out
        self.at = {"z": lax.axis_index("z"), "x": lax.axis_index("x")}

    def unit(self, c, h, jf, js=None, sub=None):
        r0, n = h * 64, 64
        if sub is not None:
            r0, n = r0 + sub * 32, 32
        fast, slow = (("x", "z"), ("z", "x"))[h]
        f = lax.rem(self.at[fast] + jf + 4, 4)
        s = slice(None) if js is None else lax.rem(self.at[slow] + js + 4, 4)
        where = (s, f) if h == 0 else (f, s)
        return self.g.at[(c, *where, slice(r0, r0 + n), slice(None))]

    def copy(self, stage, c, h, d, src):
        i = 0 if d > 0 else 1
        name = (("x", "z"), ("z", "x"))[h][stage // 2]
        m = stage * 2 + i
        return pltpu.make_async_remote_copy(
            src_ref=src,
            dst_ref=self.r[stage].at[c, h, i],
            send_sem=self.send.at[c, h, m],
            recv_sem=self.recv.at[c, h, m],
            device_id={name: lax.rem(self.at[name] + d + 4, 4)},
            device_id_type=MESH,
        )

    def c1(self, c, h, d):
        return self.copy(0, c, h, d, self.unit(c, h, 2, None, 0 if d > 0 else 1))

    def c2(self, c, h, d):
        return self.copy(1, c, h, d, self.unit(c, h, d))

    def c3(self, c, h, d):
        return self.copy(2, c, h, d, self.unit(c, h, 0, 2, 0 if d > 0 else 1))

    def c4(self, c, h, d):
        return self.copy(3, c, h, d, self.unit(c, h, 0, d))

    def s1(self, c):
        for h in (0, 1):
            for d in (1, -1):
                self.c1(c, h, d).start()

    def a1(self, c):
        for d in (1, -1):
            for h in (0, 1):
                i = 0 if d > 0 else 1
                self.c1(c, h, d).wait_recv()
                part = self.unit(c, h, d, None, i)
                for k in range(4):
                    part[k] = part[k] + self.r[0][c, h, i, k]
                self.c2(c, h, d).start()

    def a2(self, c):
        for h in (0, 1):
            for d in (1, -1):
                self.c2(c, h, d).wait_recv()
            whole = self.unit(c, h, 0)
            for k in range(4):
                whole[k] = (
                    whole[k].astype(F32) + self.r[1][c, h, 0, k].astype(F32) + self.r[1][c, h, 1, k].astype(F32)
                ).astype(BF)
            for d in (1, -1):
                self.c3(c, h, d).start()

    def a3(self, c):
        for d in (1, -1):
            for h in (0, 1):
                i = 0 if d > 0 else 1
                self.c3(c, h, d).wait_recv()
                part = self.unit(c, h, 0, d, i)
                part[...] = part[...] + self.r[2][c, h, i]
                self.c4(c, h, d).start()

    def a4(self, c):
        for h in (0, 1):
            for d in (1, -1):
                self.c4(c, h, d).wait_recv()
            own = self.unit(c, h, 0, 0)
            done = own[...].astype(F32) + self.r[3][c, h, 0].astype(F32) + self.r[3][c, h, 1].astype(F32)
            at = slice(h * 64, h * 64 + 64)
            for k, out in enumerate(self.out):
                n = min(CHUNK, out.shape[1] - c * CHUNK)
                cols = slice(c * CHUNK, c * CHUNK + n)
                out[at, cols] = out[at, cols] + done[:, k * CHUNK : k * CHUNK + n]

    def drain(self, c):
        for h in (0, 1):
            for d in (1, -1):
                for copy in (self.c1, self.c2, self.c3, self.c4):
                    copy(c, h, d).wait_send()


class TokenScatter:
    def __init__(self, t, p, rc, q, credit, send, recv):
        self.t, self.p, self.rc, self.q, self.credit = t, p, rc, q, credit
        self.send, self.recv = send, recv
        self.y, self.c = lax.axis_index("y"), lax.axis_index("c")

    def to(self, k):
        return lax.rem(self.y + k + 4, 4)

    def rows(self, k, core, sub=None):
        start, n = (self.to(k) * 2 + core) * SHARD, SHARD
        if sub is not None:
            start, n = start + sub * (SHARD // 2), SHARD // 2
        return self.p.at[pl.ds(pl.multiple_of(start, SHARD // 2), n), :]

    def landed(self, k):
        start = self.t * 4 * SHARD + self.to(k) * SHARD
        return self.rc.at[pl.ds(pl.multiple_of(start, SHARD), SHARD), :]

    def q1(self, i):
        start = self.t * 3 * SHARD + i * (SHARD // 2)
        return self.q.at[start : start + SHARD // 2, :]

    def q2(self, i):
        start = self.t * 3 * SHARD + (1 + i) * SHARD
        return self.q.at[start : start + SHARD, :]

    def pair(self, k):
        return pltpu.make_async_remote_copy(
            src_ref=self.rows(k, 1 - self.c),
            dst_ref=self.landed(k),
            send_sem=self.send.at[self.t, k % 4],
            recv_sem=self.recv.at[self.t, k % 4],
            device_id={"c": 1 - self.c},
            device_id_type=MESH,
        )

    def ring(self, src, dst, m, d):
        return pltpu.make_async_remote_copy(
            src_ref=src,
            dst_ref=dst,
            send_sem=self.send.at[self.t, m],
            recv_sem=self.recv.at[self.t, m],
            device_id={"y": self.to(d)},
            device_id_type=MESH,
        )

    def y1(self, d):
        i = 0 if d > 0 else 1
        return self.ring(self.rows(2, self.c, i), self.q1(i), 4 + i, d)

    def y2(self, d):
        i = 0 if d > 0 else 1
        return self.ring(self.rows(d, self.c), self.q2(i), 6 + i, d)

    def share(self, k):
        if self.t == 0 and k == 2:
            pl.semaphore_wait(self.credit.at[0], 1)
        self.pair(k).start()

    def join(self, k):
        self.pair(k).wait_recv()
        mine = self.rows(k, self.c)
        mine[...] = mine[...] + self.landed(k)[...]

    def far(self):
        self.join(2)
        for d in (1, -1):
            if self.t == 0:
                pl.semaphore_wait(self.credit.at[1 if d > 0 else 2], 1)
            self.y1(d).start()

    def near(self, d):
        i = 0 if d > 0 else 1
        self.join(d)
        self.y1(d).wait_recv()
        part = self.rows(d, self.c, i)
        part[...] = part[...] + self.q1(i)[...]
        self.y2(d).start()

    def finish(self):
        self.join(0)
        for d in (1, -1):
            self.y2(d).wait_recv()
        return (
            self.rows(0, self.c)[...].astype(F32) + self.q2(0)[...].astype(F32) + self.q2(1)[...].astype(F32)
        )

    def drain(self):
        for k in (0, 1, 2, -1):
            self.pair(k).wait_send()
        for d in (1, -1):
            self.y1(d).wait_send()
            self.y2(d).wait_send()


def butterfly():
    steps = [("c", 1 - lax.axis_index("c"))]
    for name in ("y", "x", "z"):
        me = lax.axis_index(name)
        steps.append((name, me + 1 - 2 * lax.rem(me, 2)))
        steps.append((name, 3 - me))
    return steps


class GainSum:
    def __init__(self, mine, theirs, send, recv):
        self.mine, self.theirs, self.send, self.recv = mine, theirs, send, recv
        self.steps = butterfly()

    def copy(self, i):
        name, partner = self.steps[i]
        return pltpu.make_async_remote_copy(
            src_ref=self.mine.at[i],
            dst_ref=self.theirs.at[i],
            send_sem=self.send.at[i],
            recv_sem=self.recv.at[i],
            device_id={name: partner},
            device_id_type=MESH,
        )

    def start(self, i):
        self.copy(i).start()

    def end(self, i):
        self.copy(i).wait_recv()
        self.mine[i + 1] = self.mine[i] + self.theirs[i]

    def drain(self):
        for i in range(7):
            self.copy(i).wait_send()


def nt(a, b):
    return lax.dot_general(a, b, (((1,), (1,)), ((), ())), preferred_element_type=F32)


def sublayer(
    later_in, earlier_in, cot_in, gate_w, up_w, down_w, gain, gate_sum, up_sum, down_sum,
    later_out, hidden_out, earlier_out, gate_new, up_new, down_new, gain_out,
    w, g, nl, ne, cot, net, cott, hl, dg, du, he, r1, r2, r3, r4, dn, lrow, crow, gacc, gmine, gtheirs,
    in_sem, wsend, wrecv, send, recv, tsend, trecv, gsend, grecv, credit, out_sem,
):
    tokens, width = nl.shape
    half = width // 2
    z, x, y, c_me = (lax.axis_index(n) for n in ALL)
    me = z * 4 + x
    own_rows = pl.ds(pl.multiple_of((y * 2 + c_me) * SHARD, SHARD), SHARD)
    pairs = [
        (later_in, nl), (earlier_in, ne), (cot_in, cot),
        (gate_sum, gate_new), (up_sum, up_new), (down_sum, down_new),
        (later_in.at[own_rows, :], lrow), (cot_in.at[own_rows, :], crow),
    ]
    ins = [pltpu.make_async_copy(a, b, in_sem.at[i]) for i, (a, b) in enumerate(pairs)]
    ins[0].start()
    ins[1].start()
    mine = pl.ds(pl.multiple_of(me * SHARD, SHARD), SHARD)
    for k, ref in enumerate((gate_w, up_w, down_w)):
        cols = ref.shape[1]
        for c in range(N_CHUNK):
            n = min(CHUNK, cols - c * CHUNK)
            part = ref[:, c * CHUNK : c * CHUNK + n]
            if n < CHUNK:
                part = jnp.concatenate([part, jnp.zeros((SHARD, CHUNK - n), BF)], axis=1)
            w[c, mine, k * CHUNK : (k + 1) * CHUNK] = part
    greet(ring_peers(("x", "z", "y")) + [{"c": 1 - c_me}])
    ring = Gather(w, wsend, wrecv)
    ring.t0(0)
    for copy in ins[2:]:
        copy.start()
    rs = Scatter(g, r1, r2, r3, r4, send, recv, (gate_new, up_new, down_new))
    later = TokenScatter(0, nl, net, cot, credit, tsend, trecv)
    earlier = TokenScatter(1, ne, net, cot, credit, tsend, trecv)
    total = GainSum(gmine, gtheirs, gsend, grecv)

    gain_row = gain[...].astype(F32)

    def turn(ref, i):
        rows = pl.ds(pl.multiple_of(i * 128, 128), 128)
        return [ref[rows, j * half : (j + 1) * half].T for j in (0, 1)]

    def put(turned, ref, i):
        start = pl.multiple_of(i * 128, 128)
        flipped = turn(ref, i)
        turned[:, pl.ds(start, 128)] = flipped[0]
        turned[:, pl.ds(pl.multiple_of(start + tokens, 128), 128)] = flipped[1]

    def norm_block(ref, i):
        rows = pl.ds(pl.multiple_of(i * 64, 64), 64)
        v = ref[rows, :].astype(F32)
        unit = v * lax.rsqrt(jnp.mean(v * v, axis=1, keepdims=True) + NORM_FLOOR)
        ref[rows, :] = (unit * gain_row).astype(BF)

    blocks = tokens // 128

    def norms(ref, first, last):
        @pl.loop(first, last)
        def _(i):
            norm_block(ref, i)

    def turns(turned, ref, first, last):
        @pl.loop(first, last)
        def _(i):
            put(turned, ref, i)

    ins[0].wait()
    norms(nl, 0, blocks)
    ring.t1(0)
    norms(nl, blocks, 2 * blocks)
    ring.t2(0)
    ins[1].wait()
    norms(ne, 0, blocks)
    ring.t3(0)
    ring.t0(1)
    norms(ne, blocks, 2 * blocks)
    turns(net, ne, 0, blocks // 2)
    ring.t4(0)
    ring.t1(1)
    turns(net, ne, blocks // 2, blocks)
    ins[2].wait()
    turns(cott, cot, 0, blocks // 2)
    ring.t5(0)
    ring.t2(1)
    turns(cott, cot, blocks // 2, blocks)
    ring.t6(0)
    for copy in ins[3:]:
        copy.wait()

    tb = 256

    def later_item(c, i):
        rows = pl.ds(i * tb, tb)
        pre = nn(nl[rows, :], w[c, :, : 2 * CHUNK])
        gate, up = pre[:, :CHUNK], pre[:, CHUNK:]
        hl[c, rows, :] = (gate * jax.nn.sigmoid(gate) * up).astype(BF)

    def earlier_item(c, i):
        rows = pl.ds(i * tb, tb)
        pre = nn(ne[rows, :], w[c, :, : 2 * CHUNK])
        dh = 0.5 * nn(cot[rows, :], w[c, :, 2 * CHUNK :])
        gate, up = pre[:, :CHUNK], pre[:, CHUNK:]
        s = jax.nn.sigmoid(gate)
        act = gate * s
        he[rows, :] = (act * up).astype(BF)
        dg[c, rows, :] = (dh * up * s * (1.0 + gate * (1.0 - s))).astype(BF)
        du[c, rows, :] = (dh * act).astype(BF)

    def grad_item(c, i):
        rows = pl.ds((i % 2) * 512, 512)
        cols = pl.ds((i // 2) * tokens, tokens)
        shape = (4, SHARD, CHUNK)
        g[c, i, :, :, :CHUNK] = nn(net[rows, cols], dg[c]).astype(BF).reshape(shape)
        g[c, i, :, :, CHUNK : 2 * CHUNK] = nn(net[rows, cols], du[c]).astype(BF).reshape(shape)
        g[c, i, :, :, 2 * CHUNK :] = (0.5 * nn(cott[rows, cols], he[...])).astype(BF).reshape(shape)

    reload = pltpu.make_async_copy(earlier_in, cott, in_sem.at[8])

    def free():
        reload.start()
        pl.semaphore_signal(credit.at[0], inc=1, device_id={"c": 1 - c_me}, device_id_type=MESH)
        pl.semaphore_signal(credit.at[1], inc=1, device_id={"y": lax.rem(y + 3, 4)}, device_id_type=MESH)
        pl.semaphore_signal(credit.at[2], inc=1, device_id={"y": lax.rem(y + 1, 4)}, device_id_type=MESH)

    outs = [
        pltpu.make_async_copy(hl.at[c], hidden_out.at[:, c * CHUNK : (c + 1) * CHUNK], out_sem.at[c])
        for c in range(N_CHUNK)
    ]

    ticks = {
        0: {0: [ring.t3, 1], 1: [ring.t0, 2], 3: [ring.t4, 1], 4: [ring.t1, 2], 6: [ring.t5, 1], 7: [ring.t2, 2], 9: [ring.t6, 1]},
        1: {0: [ring.t3, 2], 3: [ring.t4, 2], 6: [ring.t5, 2], 8: [rs.s1, 0], 11: [ring.t6, 2]},
        2: {0: [rs.s1, 1], 4: [rs.a1, 0], 7: [rs.s1, 2], 10: [rs.a1, 1]},
    }

    @pl.loop(0, N_CHUNK)
    def _(c):
        items = [functools.partial(earlier_item, c, i) for i in range(tokens // tb)]
        items += [functools.partial(grad_item, c, i) for i in range(width // 512)]
        items += [functools.partial(later_item, c, i) for i in range(tokens // tb)]
        for n, item in enumerate(items):
            item()
            for when in range(N_CHUNK):
                todo = ticks[when].get(n)
                if todo is not None or (when == 2 and n == 7):

                    @pl.when(c == when)
                    def _():
                        if when == 2 and n == 7:
                            free()
                        if todo is not None:
                            todo[0](todo[1])

    for copy in outs:
        copy.start()

    def token_rows(b):
        return pl.ds(pl.multiple_of(b * 256, 256), 256)

    def later_block(k):
        b = lax.rem(y + k + 4, 4)
        rows = token_rows(b)

        @pl.loop(0, 4)
        def _(n):
            f = pl.ds(pl.multiple_of(n * 512, 512), 512)
            out = nt(hl[0, rows, :], w[0, f, 2 * CHUNK :])
            for c in range(1, N_CHUNK):
                out = out + nt(hl[c, rows, :], w[c, f, 2 * CHUNK :])
            nl[rows, f] = out.astype(BF)

        later.share(k)

    def earlier_block(k):
        b = lax.rem(y + k + 4, 4)
        rows = token_rows(b)

        @pl.loop(0, 4)
        def _(n):
            f = pl.ds(pl.multiple_of(n * 512, 512), 512)
            out = nt(dg[0, rows, :], w[0, f, :CHUNK])
            out = out + nt(du[0, rows, :], w[0, f, CHUNK : 2 * CHUNK])
            for c in range(1, N_CHUNK):
                out = out + nt(dg[c, rows, :], w[c, f, :CHUNK])
                out = out + nt(du[c, rows, :], w[c, f, CHUNK : 2 * CHUNK])
            dn[:, f] = out

        @pl.loop(0, 16)
        def _(i):
            at = pl.ds(pl.multiple_of(b * 256 + i * 16, 16), 16)
            v = cott[at, :].astype(F32)
            scale = lax.rsqrt(jnp.mean(v * v, axis=1, keepdims=True) + NORM_FLOOR)
            unit = v * scale
            d = dn[pl.ds(pl.multiple_of(i * 16, 16), 16), :]
            terms = d * unit
            gacc[...] += terms[:8] + terms[8:]
            mean = jnp.mean(terms * gain_row, axis=1, keepdims=True)
            ne[at, :] = (scale * (d * gain_row - unit * mean)).astype(BF)

        earlier.share(k)

    gacc[...] = jnp.zeros_like(gacc)
    later_block(2)
    later_block(1)
    later.far()
    reload.wait()
    earlier_block(2)
    later_block(-1)
    earlier.far()
    later_block(0)
    rs.a2(0)
    earlier_block(1)
    later.near(1)
    later.near(-1)
    rs.a1(2)
    earlier_block(-1)
    earlier.near(1)
    earlier.near(-1)
    earlier_block(0)
    gmine[0] = jnp.sum(gacc[...], axis=0, keepdims=True)
    total.start(0)
    rs.a2(1)
    rs.a3(0)
    total.end(0)
    total.start(1)
    later_out[...] = (lrow[...].astype(F32) + 0.5 * later.finish()).astype(BF)
    total.end(1)
    total.start(2)
    rs.a2(2)
    rs.a3(1)
    total.end(2)
    total.start(3)
    rs.a4(0)
    rs.a3(2)
    total.end(3)
    total.start(4)
    rs.a4(1)
    total.end(4)
    total.start(5)
    earlier_out[...] = (crow[...].astype(F32) + earlier.finish()).astype(BF)
    total.end(5)
    total.start(6)
    rs.a4(2)
    total.end(6)
    gain_out[...] = gmine[7]
    for c in range(N_CHUNK):
        ring.drain(c)
        rs.drain(c)
    later.drain()
    earlier.drain()
    total.drain()
    for copy in outs:
        copy.wait()


def run(later_in, earlier_in, cot, gate_w, up_w, down_w, gain, gate_sum, up_sum, down_sum):
    tokens, width = later_in.shape
    rows, cols = gate_w.shape
    any_ = pl.BlockSpec(memory_space=pl.ANY)
    vm = pl.BlockSpec(memory_space=pltpu.VMEM)
    act = (N_CHUNK, tokens, CHUNK)
    tok = (tokens, width)
    dma = pltpu.SemaphoreType.DMA
    return pl.pallas_call(
        sublayer,
        out_shape=[
            jax.ShapeDtypeStruct((tokens // 8, width), BF),
            jax.ShapeDtypeStruct((tokens, N_CHUNK * CHUNK), BF),
            jax.ShapeDtypeStruct((tokens // 8, width), BF),
            jax.ShapeDtypeStruct((rows, cols), F32),
            jax.ShapeDtypeStruct((rows, cols), F32),
            jax.ShapeDtypeStruct((rows, cols), F32),
            jax.ShapeDtypeStruct((1, width), F32),
        ],
        in_specs=[any_] * 3 + [vm] * 4 + [any_] * 3,
        out_specs=[vm, any_] + [vm] * 5,
        scratch_shapes=[
            pltpu.VMEM((N_CHUNK, width, WIDE), BF),
            pltpu.VMEM((N_CHUNK, 4, 4, SHARD, WIDE), BF),
            pltpu.VMEM(tok, BF),
            pltpu.VMEM(tok, BF),
            pltpu.VMEM(tok, BF),
            pltpu.VMEM(tok, BF),
            pltpu.VMEM(tok, BF),
            pltpu.VMEM(act, BF),
            pltpu.VMEM(act, BF),
            pltpu.VMEM(act, BF),
            pltpu.VMEM((tokens, CHUNK), BF),
            pltpu.VMEM((N_CHUNK, 2, 2, 4, SHARD // 4, WIDE), BF),
            pltpu.VMEM((N_CHUNK, 2, 2, 4, SHARD // 2, WIDE), BF),
            pltpu.VMEM((N_CHUNK, 2, 2, SHARD // 4, WIDE), BF),
            pltpu.VMEM((N_CHUNK, 2, 2, SHARD // 2, WIDE), BF),
            pltpu.VMEM((256, width), F32),
            pltpu.VMEM((SHARD, width), BF),
            pltpu.VMEM((SHARD, width), BF),
            pltpu.VMEM((8, width), F32),
            pltpu.VMEM((8, 1, width), F32),
            pltpu.VMEM((7, 1, width), F32),
            dma((9,)),
            dma((N_CHUNK, 2, 20)),
            dma((N_CHUNK, 2, 20)),
            dma((N_CHUNK, 2, 8)),
            dma((N_CHUNK, 2, 8)),
            dma((2, 8)),
            dma((2, 8)),
            dma((7,)),
            dma((7,)),
            pltpu.SemaphoreType.REGULAR((3,)),
            dma((N_CHUNK,)),
        ],
        compiler_params=pltpu.CompilerParams(
            collective_id=0, has_side_effects=True, vmem_limit_bytes=64 * 1024 * 1024 - 65536
        ),
        name="sublayer",
    )(later_in, earlier_in, cot, gate_w, up_w, down_w, gain.reshape(1, width), gate_sum, up_sum, down_sum)


def local(later_in, earlier_in, cot, gate_w, up_w, down_w, gain, gate_sum, up_sum, down_sum, gain_sum):
    later_out, hidden, earlier_grad, gate_new, up_new, down_new, gain_total = run(
        later_in, earlier_in, cot, gate_w, up_w, down_w, gain, gate_sum, up_sum, down_sum
    )
    return (
        later_out, hidden[:, : gate_w.shape[1]], earlier_grad,
        gate_new, up_new, down_new, gain_sum + gain_total[0],
    )


def solution(mesh):
    torus = Mesh(mesh.devices.reshape(4, 4, 4, 2), ALL)
    return jax.shard_map(
        local,
        mesh=torus,
        in_specs=(P(FS, None),) * 3 + (P(FS, TP),) * 3 + (P(),) + (P(FS, TP),) * 3 + (P(),),
        out_specs=(P(ALL, None), P(FS, TP), P(ALL, None), P(FS, TP), P(FS, TP), P(FS, TP), P()),
        check_vma=False,
    )
```

time: 264 us -> 166 us (0.63)
  blocking collectives: 108 us -> 0 us
  Pallas kernels: 86.3 us -> 142 us
  matrix products: 23.9 us -> 0 us
  other arithmetic: 18.2 us -> 1.31 us
  local copies, waits for them, and re-layouts: 7.11 us -> 21.1 us
  between operations: 14.2 us -> 0.67 us
  starting transfers between devices: 4.78 us -> 0 us
    psum x1 -> x0, blocking collectives: 108 us -> none  [local(): gain_new = gain_sum + lax.psum(gain_part, ALL)]
    pallas_call x1, Pallas kernels: 86.3 us -> 142 us  [run(): pl.pallas_call(sublayer, out_shape=[jax.ShapeDtypeStruct((tokens // 8, wi...]
    dot_general x3 -> x0, matrix products: 23.9 us -> none  [local(): lax.dot_general(a, b, (((0, 2), (0, 2)), ((), ())), preferred_element_typ...]
    unnamed x18, local copies, waits for them, and re-layouts: 0.04 us -> 19.8 us
    convert_element_type x4 -> x0, other arithmetic: 7.59 us -> none  [the longest x2 5.31 us: local(): earlier_grad = (rows(cot) + sum_at_owner(branch.astype(BF), TP)).astype(BF)]
    reduce_sum x2 -> x0, other arithmetic: 6.26 us -> none  [the longest x1 3.19 us: unit_of(): scale = lax.rsqrt(jnp.mean(v * v, axis=1, keepdims=True) + NORM_FLOOR)]
    all_to_all x1 -> x0, starting transfers between devices: 4.7 us -> none  [sum_at_owner(): lax.all_to_all(parts, axis, split_axis=0, concat_axis=0, tiled=True)]
    pad x3 -> x0, local copies, waits for them, and re-layouts: 2.81 us -> none  [pack(): w = jnp.pad(w, ((0, 0), (0, N_CHUNK * CHUNK - cols)))]
  transfers between devices with their start and end apart: 3 -> 0, of which waited for: 0 -> 0; matrix products, arithmetic and copies ran while one was open for 12% -> 0% of each run, Pallas kernels for 0% -> 0%
where the time goes in v3:
time: 166 us; the launch traced here: 165 us
  Pallas kernels  142 us (86%)
  local copies, waits for them, and re-layouts  21.1 us (13%)
    pallas_call x1, Pallas kernels, run(): pl.pallas_call(sublayer, out_shape=[jax.ShapeDtypeStruct((tokens // 8, wi...  142 us
    unnamed x18, local copies, waits for them, and re-layouts  19.8 us

profile of v3, /device:TPU:0, one launch (start us, length us, event | category | flops | bytes accessed | tf_op | source)
XLA Modules:
  0.0 165.1 jit_solution(15254301120995006354)
XLA Ops:
  0.6 1.3 reshape.17.gain
  1.9 1.7 %copy.18.gate_w = bf16[128,704]{1,0:T(8,128)(2,1)} copy(bf16[128,704]{0,1:T(8,128)(2,1)} %param.14) | data formatting | bytes 360448 | tf_op args[3]
  3.7 1.7 %copy.19.up_w = bf16[128,704]{1,0:T(8,128)(2,1)} copy(bf16[128,704]{0,1:T(8,128)(2,1)} %param.15) | data formatting | bytes 360448 | tf_op args[4]
  5.4 1.7 %copy.20.down_w = bf16[128,704]{1,0:T(8,128)(2,1)} copy(bf16[128,704]{0,1:T(8,128)(2,1)} %param.16) | data formatting | bytes 360448 | tf_op args[5]
  7.1 1.9 %copy.21.gate_sum = f32[128,704]{1,0:T(8,128)} copy(f32[128,704]{0,1:T(8,128)} %param.18) | data formatting | bytes 720896 | tf_op args[7]
  9.0 1.9 %copy.22.up_sum = f32[128,704]{1,0:T(8,128)} copy(f32[128,704]{0,1:T(8,128)} %param.19) | data formatting | bytes 720896 | tf_op args[8]
  10.9 1.9 %copy.23.down_sum = f32[128,704]{1,0:T(8,128)} copy(f32[128,704]{0,1:T(8,128)} %param.20) | data formatting | bytes 720896 | tf_op args[9]
  12.8 142.0 %sublayer.1 = (bf16[128,2048]{1,0:T(8,128)(2,1)}, bf16[1024,768]{1,0:T(8,128)(2,1)}, bf16[128,2048]{1,0:T(8,128)(2,1)}, f32[128,704]{1,0:T(8,128)}, f32[128,704]...) custom-call(bf16[1024,2048]{1,0:T(8,128)(2,1)} %later_in.1, bf16[1024,2048]{1,0:T(8,128)(2,1)} %earlier_in.1, ...), custom_call_target="tpu_custom_call" | custom-call | tf_op jit(solution)/shard_map/sublayer/pallas_call | solution.py:648
  154.8 0.0 copy-start.2
  154.8 0.0 copy-start.1
  154.8 0.0 copy-start
  154.8 2.6 %copy.24 = bf16[1024,704]{0,1:T(8,128)(2,1)} copy(bf16[1024,704]{1,0:T(8,128)(2,1)} %bitcast.2) | data formatting | bytes 2883584
  157.5 1.3 add.3
  158.8 1.9 %copy.25 = f32[128,704]{0,1:T(8,128)} copy(f32[128,704]{1,0:T(8,128)} %get-tuple-element.24) | data formatting | bytes 720896
  160.7 1.9 %copy.26 = f32[128,704]{0,1:T(8,128)} copy(f32[128,704]{1,0:T(8,128)} %get-tuple-element.25) | data formatting | bytes 720896
  162.6 0.0 copy-done.2
  162.6 0.9 copy.27
  163.5 0.0 copy-done.1
  163.5 0.8 copy.30
  164.3 0.0 copy-done
  164.3 0.8 copy.31
Async XLA Ops:
  154.8 7.8 %copy-start.2 = (f32[128,704]{1,0:T(8,128)S(1)}, f32[128,704]{1,0:T(8,128)}, u32[]{:S(2)}) copy-start(f32[128,704]{1,0:T(8,128)} %get-tuple-element.26) | copy-start | bytes 1081348
  154.8 8.7 %copy-start.1 = (bf16[128,2048]{1,0:T(8,128)(2,1)S(1)}, bf16[128,2048]{1,0:T(8,128)(2,1)}, u32[]{:S(2)}) copy-start(bf16[128,2048]{1,0:T(8,128)(2,1)} %get-tuple-element.35) | copy-start | bytes 1572868
  154.8 9.5 %copy-start = (bf16[128,2048]{1,0:T(8,128)(2,1)S(1)}, bf16[128,2048]{1,0:T(8,128)(2,1)}, u32[]{:S(2)}) copy-start(bf16[128,2048]{1,0:T(8,128)(2,1)} %get-tuple-element.37) | copy-start | bytes 1572868

commit v4 on v3

--- a/solution.py
+++ b/solution.py
@@ -14,11 +14,18 @@
 MESH = pl.DeviceIdType.MESH
 BF = jnp.bfloat16
 F32 = jnp.float32
-CHUNK = 256
-N_CHUNK = 3
+N_CHUNK = 2
+CHUNK = 352
 WIDE = 3 * CHUNK
+HALF = WIDE // 2
+CUT = 272
 SHARD = 128
 NORM_FLOOR = 0.05
+
+
+def span(h, sub=None):
+    at = h * HALF
+    return slice(at + (CUT if sub == 1 else 0), at + (CUT if sub == 0 else HALF))
 
 
 class Gather:
@@ -31,12 +38,9 @@
         return lax.rem(self.mz + dz + 4, 4) * 4 + lax.rem(self.mx + dx + 4, 4)
 
     def copy(self, c, h, msg, jf, js, sub, axis, d):
-        start = self.owner(h, jf, js) * SHARD + h * (SHARD // 2)
-        size = SHARD // 2
-        if sub is not None:
-            size = SHARD // 4
-            start = start + sub * size
-        view = self.w.at[c, pl.ds(pl.multiple_of(start, 32), size), :]
+        view = self.w.at[
+            c, span(h, sub), pl.ds(pl.multiple_of(self.owner(h, jf, js) * SHARD, SHARD), SHARD)
+        ]
         name = ("x", "z")[h] if axis == "f" else ("z", "x")[h]
         me = self.mx if name == "x" else self.mz
         return pltpu.make_async_remote_copy(
@@ -154,14 +158,18 @@
         self.at = {"z": lax.axis_index("z"), "x": lax.axis_index("x")}
 
     def unit(self, c, h, jf, js=None, sub=None):
-        r0, n = h * 64, 64
-        if sub is not None:
-            r0, n = r0 + sub * 32, 32
         fast, slow = (("x", "z"), ("z", "x"))[h]
         f = lax.rem(self.at[fast] + jf + 4, 4)
         s = slice(None) if js is None else lax.rem(self.at[slow] + js + 4, 4)
         where = (s, f) if h == 0 else (f, s)
-        return self.g.at[(c, *where, slice(r0, r0 + n), slice(None))]
+        return self.g.at[(c, *where, span(h, sub), slice(None))]
+
+    def landing(self, stage, c, h, i):
+        ref = self.r[stage]
+        if stage % 2:
+            return ref.at[c, h, i]
+        n = CUT if i == 0 else HALF - CUT
+        return ref.at[c, h, i, :, :n] if stage == 0 else ref.at[c, h, i, :n]
 
     def copy(self, stage, c, h, d, src):
         i = 0 if d > 0 else 1
@@ -169,7 +177,7 @@
         m = stage * 2 + i
         return pltpu.make_async_remote_copy(
             src_ref=src,
-            dst_ref=self.r[stage].at[c, h, i],
+            dst_ref=self.landing(stage, c, h, i),
             send_sem=self.send.at[c, h, m],
             recv_sem=self.recv.at[c, h, m],
             device_id={name: lax.rem(self.at[name] + d + 4, 4)},
@@ -200,7 +208,7 @@
                 self.c1(c, h, d).wait_recv()
                 part = self.unit(c, h, d, None, i)
                 for k in range(4):
-                    part[k] = part[k] + self.r[0][c, h, i, k]
+                    part[k] = part[k] + self.landing(0, c, h, i)[k]
                 self.c2(c, h, d).start()
 
     def a2(self, c):
@@ -221,7 +229,7 @@
                 i = 0 if d > 0 else 1
                 self.c3(c, h, d).wait_recv()
                 part = self.unit(c, h, 0, d, i)
-                part[...] = part[...] + self.r[2][c, h, i]
+                part[...] = part[...] + self.landing(2, c, h, i)[...]
                 self.c4(c, h, d).start()
 
     def a4(self, c):
@@ -230,11 +238,11 @@
                 self.c4(c, h, d).wait_recv()
             own = self.unit(c, h, 0, 0)
             done = own[...].astype(F32) + self.r[3][c, h, 0].astype(F32) + self.r[3][c, h, 1].astype(F32)
-            at = slice(h * 64, h * 64 + 64)
             for k, out in enumerate(self.out):
-                n = min(CHUNK, out.shape[1] - c * CHUNK)
-                cols = slice(c * CHUNK, c * CHUNK + n)
-                out[at, cols] = out[at, cols] + done[:, k * CHUNK : k * CHUNK + n]
+                first, last = max(h * HALF, k * CHUNK), min((h + 1) * HALF, (k + 1) * CHUNK)
+                if first < last:
+                    at = slice(c * CHUNK + first - k * CHUNK, c * CHUNK + last - k * CHUNK)
+                    out[at, :] = out[at, :] + done[first - h * HALF : last - h * HALF]
 
     def drain(self, c):
         for h in (0, 1):
@@ -376,42 +384,43 @@
             self.copy(i).wait_send()
 
 
-def nt(a, b):
-    return lax.dot_general(a, b, (((1,), (1,)), ((), ())), preferred_element_type=F32)
-
-
 def sublayer(
     later_in, earlier_in, cot_in, gate_w, up_w, down_w, gain, gate_sum, up_sum, down_sum,
     later_out, hidden_out, earlier_out, gate_new, up_new, down_new, gain_out,
-    w, g, nl, ne, cot, net, cott, hl, dg, du, he, r1, r2, r3, r4, dn, lrow, crow, gacc, gmine, gtheirs,
-    in_sem, wsend, wrecv, send, recv, tsend, trecv, gsend, grecv, credit, out_sem,
+    w, g, nl, ne, cot, nlt, net, cott, hl, dx, he, hb, xb, r1, r2, r3, r4, dn, lrow, crow, gacc, gmine, gtheirs,
+    in_sem, own_sem, wsend, wrecv, send, recv, tsend, trecv, gsend, grecv, credit, out_sem,
 ):
     tokens, width = nl.shape
     half = width // 2
     z, x, y, c_me = (lax.axis_index(n) for n in ALL)
     me = z * 4 + x
     own_rows = pl.ds(pl.multiple_of((y * 2 + c_me) * SHARD, SHARD), SHARD)
+    mine = pl.ds(pl.multiple_of(me * SHARD, SHARD), SHARD)
+    own = [
+        pltpu.make_async_copy(
+            ref.at[c * CHUNK : (c + 1) * CHUNK, :],
+            w.at[c, k * CHUNK : (k + 1) * CHUNK, mine],
+            own_sem.at[c, k],
+        )
+        for c in range(N_CHUNK)
+        for k, ref in enumerate((gate_w, up_w, down_w))
+    ]
     pairs = [
         (later_in, nl), (earlier_in, ne), (cot_in, cot),
         (gate_sum, gate_new), (up_sum, up_new), (down_sum, down_new),
         (later_in.at[own_rows, :], lrow), (cot_in.at[own_rows, :], crow),
     ]
     ins = [pltpu.make_async_copy(a, b, in_sem.at[i]) for i, (a, b) in enumerate(pairs)]
-    ins[0].start()
-    ins[1].start()
-    mine = pl.ds(pl.multiple_of(me * SHARD, SHARD), SHARD)
-    for k, ref in enumerate((gate_w, up_w, down_w)):
-        cols = ref.shape[1]
-        for c in range(N_CHUNK):
-            n = min(CHUNK, cols - c * CHUNK)
-            part = ref[:, c * CHUNK : c * CHUNK + n]
-            if n < CHUNK:
-                part = jnp.concatenate([part, jnp.zeros((SHARD, CHUNK - n), BF)], axis=1)
-            w[c, mine, k * CHUNK : (k + 1) * CHUNK] = part
+    for copy in own:
+        copy.start()
+    for copy in ins[:3]:
+        copy.start()
     greet(ring_peers(("x", "z", "y")) + [{"c": 1 - c_me}])
+    for copy in own:
+        copy.wait()
     ring = Gather(w, wsend, wrecv)
     ring.t0(0)
-    for copy in ins[2:]:
+    for copy in ins[3:]:
         copy.start()
     rs = Scatter(g, r1, r2, r3, r4, send, recv, (gate_new, up_new, down_new))
     later = TokenScatter(0, nl, net, cot, credit, tsend, trecv)
@@ -420,83 +429,80 @@
 
     gain_row = gain[...].astype(F32)
 
-    def turn(ref, i):
+    def turn_block(turned, ref, i):
         rows = pl.ds(pl.multiple_of(i * 128, 128), 128)
-        return [ref[rows, j * half : (j + 1) * half].T for j in (0, 1)]
-
-    def put(turned, ref, i):
-        start = pl.multiple_of(i * 128, 128)
-        flipped = turn(ref, i)
-        turned[:, pl.ds(start, 128)] = flipped[0]
-        turned[:, pl.ds(pl.multiple_of(start + tokens, 128), 128)] = flipped[1]
-
-    def norm_block(ref, i):
-        rows = pl.ds(pl.multiple_of(i * 64, 64), 64)
-        v = ref[rows, :].astype(F32)
-        unit = v * lax.rsqrt(jnp.mean(v * v, axis=1, keepdims=True) + NORM_FLOOR)
-        ref[rows, :] = (unit * gain_row).astype(BF)
-
-    blocks = tokens // 128
+        for j in (0, 1):
+            at = pl.ds(pl.multiple_of(i * 128 + j * tokens, 128), 128)
+            turned[:, at] = ref[rows, j * half : (j + 1) * half].T
+
+    def turned_cols(turned, i):
+        return jnp.concatenate(
+            [turned[:, j * tokens + i * 256 : j * tokens + (i + 1) * 256] for j in (0, 1)], axis=0
+        )
 
     def norms(ref, first, last):
         @pl.loop(first, last)
         def _(i):
-            norm_block(ref, i)
+            rows = pl.ds(pl.multiple_of(i * 64, 64), 64)
+            v = ref[rows, :].astype(F32)
+            unit = v * lax.rsqrt(jnp.mean(v * v, axis=1, keepdims=True) + NORM_FLOOR)
+            ref[rows, :] = (unit * gain_row).astype(BF)
 
     def turns(turned, ref, first, last):
         @pl.loop(first, last)
         def _(i):
-            put(turned, ref, i)
+            turn_block(turned, ref, i)
+
+    blocks = tokens // 128
 
     ins[0].wait()
     norms(nl, 0, blocks)
     ring.t1(0)
     norms(nl, blocks, 2 * blocks)
+    turns(nlt, nl, 0, blocks)
     ring.t2(0)
     ins[1].wait()
-    norms(ne, 0, blocks)
+    norms(ne, 0, 2 * blocks)
     ring.t3(0)
     ring.t0(1)
-    norms(ne, blocks, 2 * blocks)
-    turns(net, ne, 0, blocks // 2)
+    turns(net, ne, 0, blocks)
     ring.t4(0)
     ring.t1(1)
-    turns(net, ne, blocks // 2, blocks)
     ins[2].wait()
-    turns(cott, cot, 0, blocks // 2)
+    turns(cott, cot, 0, blocks)
     ring.t5(0)
     ring.t2(1)
-    turns(cott, cot, blocks // 2, blocks)
-    ring.t6(0)
     for copy in ins[3:]:
         copy.wait()
-
-    tb = 256
+    ring.t6(0)
+
+    def tok_cols(i):
+        return slice(i * 256, (i + 1) * 256)
 
     def later_item(c, i):
-        rows = pl.ds(i * tb, tb)
-        pre = nn(nl[rows, :], w[c, :, : 2 * CHUNK])
-        gate, up = pre[:, :CHUNK], pre[:, CHUNK:]
-        hl[c, rows, :] = (gate * jax.nn.sigmoid(gate) * up).astype(BF)
+        pre = nn(w[c, : 2 * CHUNK, :], turned_cols(nlt, i))
+        gate, up = pre[:CHUNK], pre[CHUNK:]
+        hl[c * CHUNK : (c + 1) * CHUNK, tok_cols(i)] = (gate * jax.nn.sigmoid(gate) * up).astype(BF)
 
     def earlier_item(c, i):
-        rows = pl.ds(i * tb, tb)
-        pre = nn(ne[rows, :], w[c, :, : 2 * CHUNK])
-        dh = 0.5 * nn(cot[rows, :], w[c, :, 2 * CHUNK :])
-        gate, up = pre[:, :CHUNK], pre[:, CHUNK:]
+        pre = nn(w[c, : 2 * CHUNK, :], turned_cols(net, i))
+        dh = 0.5 * nn(w[c, 2 * CHUNK :, :], turned_cols(cott, i))
+        gate, up = pre[:CHUNK], pre[CHUNK:]
         s = jax.nn.sigmoid(gate)
         act = gate * s
-        he[rows, :] = (act * up).astype(BF)
-        dg[c, rows, :] = (dh * up * s * (1.0 + gate * (1.0 - s))).astype(BF)
-        du[c, rows, :] = (dh * act).astype(BF)
+        he[:, tok_cols(i)] = (act * up).astype(BF)
+        dx[c, :CHUNK, tok_cols(i)] = (dh * up * s * (1.0 + gate * (1.0 - s))).astype(BF)
+        dx[c, CHUNK:, tok_cols(i)] = (dh * act).astype(BF)
 
     def grad_item(c, i):
-        rows = pl.ds((i % 2) * 512, 512)
-        cols = pl.ds((i // 2) * tokens, tokens)
-        shape = (4, SHARD, CHUNK)
-        g[c, i, :, :, :CHUNK] = nn(net[rows, cols], dg[c]).astype(BF).reshape(shape)
-        g[c, i, :, :, CHUNK : 2 * CHUNK] = nn(net[rows, cols], du[c]).astype(BF).reshape(shape)
-        g[c, i, :, :, 2 * CHUNK :] = (0.5 * nn(cott[rows, cols], he[...])).astype(BF).reshape(shape)
+        for j in (0, 1):
+            cols = slice(i * 512 + j * 256, i * 512 + (j + 1) * 256)
+            both = nn(dx[c], ne[:, cols]).astype(BF)
+            down = (0.5 * nn(he[...], cot[:, cols])).astype(BF)
+            for n in (0, 1):
+                lanes = slice(n * SHARD, (n + 1) * SHARD)
+                g[c, i, 2 * j + n, : 2 * CHUNK, :] = both[:, lanes]
+                g[c, i, 2 * j + n, 2 * CHUNK :, :] = down[:, lanes]
 
     reload = pltpu.make_async_copy(earlier_in, cott, in_sem.at[8])
 
@@ -506,68 +512,27 @@
         pl.semaphore_signal(credit.at[1], inc=1, device_id={"y": lax.rem(y + 3, 4)}, device_id_type=MESH)
         pl.semaphore_signal(credit.at[2], inc=1, device_id={"y": lax.rem(y + 1, 4)}, device_id_type=MESH)
 
-    outs = [
-        pltpu.make_async_copy(hl.at[c], hidden_out.at[:, c * CHUNK : (c + 1) * CHUNK], out_sem.at[c])
-        for c in range(N_CHUNK)
-    ]
-
-    ticks = {
-        0: {0: [ring.t3, 1], 1: [ring.t0, 2], 3: [ring.t4, 1], 4: [ring.t1, 2], 6: [ring.t5, 1], 7: [ring.t2, 2], 9: [ring.t6, 1]},
-        1: {0: [ring.t3, 2], 3: [ring.t4, 2], 6: [ring.t5, 2], 8: [rs.s1, 0], 11: [ring.t6, 2]},
-        2: {0: [rs.s1, 1], 4: [rs.a1, 0], 7: [rs.s1, 2], 10: [rs.a1, 1]},
-    }
-
-    @pl.loop(0, N_CHUNK)
-    def _(c):
-        items = [functools.partial(earlier_item, c, i) for i in range(tokens // tb)]
-        items += [functools.partial(grad_item, c, i) for i in range(width // 512)]
-        items += [functools.partial(later_item, c, i) for i in range(tokens // tb)]
-        for n, item in enumerate(items):
-            item()
-            for when in range(N_CHUNK):
-                todo = ticks[when].get(n)
-                if todo is not None or (when == 2 and n == 7):
-
-                    @pl.when(c == when)
-                    def _():
-                        if when == 2 and n == 7:
-                            free()
-                        if todo is not None:
-                            todo[0](todo[1])
-
-    for copy in outs:
-        copy.start()
-
-    def token_rows(b):
+    hidden = pltpu.make_async_copy(hl, hidden_out, out_sem)
+
+    def token_cols(b):
         return pl.ds(pl.multiple_of(b * 256, 256), 256)
 
     def later_block(k):
         b = lax.rem(y + k + 4, 4)
-        rows = token_rows(b)
-
-        @pl.loop(0, 4)
-        def _(n):
-            f = pl.ds(pl.multiple_of(n * 512, 512), 512)
-            out = nt(hl[0, rows, :], w[0, f, 2 * CHUNK :])
-            for c in range(1, N_CHUNK):
-                out = out + nt(hl[c, rows, :], w[c, f, 2 * CHUNK :])
-            nl[rows, f] = out.astype(BF)
-
-        later.share(k)
+        hb[...] = hl[:, token_cols(b)].T
+        for n in range(width // 512):
+            f = slice(n * 512, (n + 1) * 512)
+            nl[token_cols(b), f] = nn(
+                hb[...], jnp.concatenate([w[c, 2 * CHUNK :, f] for c in range(N_CHUNK)], axis=0)
+            ).astype(BF)
 
     def earlier_block(k):
         b = lax.rem(y + k + 4, 4)
-        rows = token_rows(b)
-
-        @pl.loop(0, 4)
-        def _(n):
-            f = pl.ds(pl.multiple_of(n * 512, 512), 512)
-            out = nt(dg[0, rows, :], w[0, f, :CHUNK])
-            out = out + nt(du[0, rows, :], w[0, f, CHUNK : 2 * CHUNK])
-            for c in range(1, N_CHUNK):
-                out = out + nt(dg[c, rows, :], w[c, f, :CHUNK])
-                out = out + nt(du[c, rows, :], w[c, f, CHUNK : 2 * CHUNK])
-            dn[:, f] = out
+        for c in range(N_CHUNK):
+            xb[c] = dx[c, :, token_cols(b)].T
+        for n in range(width // 512):
+            f = slice(n * 512, (n + 1) * 512)
+            dn[:, f] = nn(xb[0], w[0, : 2 * CHUNK, f]) + nn(xb[1], w[1, : 2 * CHUNK, f])
 
         @pl.loop(0, 16)
         def _(i):
@@ -584,47 +549,71 @@
         earlier.share(k)
 
     gacc[...] = jnp.zeros_like(gacc)
+    for i in range(4):
+        earlier_item(0, i)
+        if i == 1:
+            ring.t3(1)
+    ring.t4(1)
+    for i in range(4):
+        grad_item(0, i)
+        if i == 1:
+            ring.t5(1)
+    for i in range(4):
+        later_item(0, i)
+        if i == 1:
+            rs.s1(0)
+    ring.t6(1)
+    for i in range(4):
+        later_item(1, i)
+    hidden.start()
+    rs.a1(0)
     later_block(2)
     later_block(1)
+    for i in range(4):
+        earlier_item(1, i)
+    rs.a2(0)
+    for i in range(4):
+        grad_item(1, i)
+    free()
+    rs.s1(1)
+    later.share(2)
+    later.share(1)
     later.far()
     reload.wait()
     earlier_block(2)
     later_block(-1)
+    later.share(-1)
     earlier.far()
     later_block(0)
-    rs.a2(0)
+    later.share(0)
+    rs.a3(0)
     earlier_block(1)
     later.near(1)
     later.near(-1)
-    rs.a1(2)
+    rs.a1(1)
     earlier_block(-1)
     earlier.near(1)
     earlier.near(-1)
+    rs.a4(0)
     earlier_block(0)
     gmine[0] = jnp.sum(gacc[...], axis=0, keepdims=True)
     total.start(0)
-    rs.a2(1)
-    rs.a3(0)
+    later_out[...] = (lrow[...].astype(F32) + 0.5 * later.finish()).astype(BF)
     total.end(0)
     total.start(1)
-    later_out[...] = (lrow[...].astype(F32) + 0.5 * later.finish()).astype(BF)
+    rs.a2(1)
     total.end(1)
     total.start(2)
-    rs.a2(2)
     rs.a3(1)
     total.end(2)
     total.start(3)
-    rs.a4(0)
-    rs.a3(2)
+    earlier_out[...] = (crow[...].astype(F32) + earlier.finish()).astype(BF)
     total.end(3)
     total.start(4)
     rs.a4(1)
-    total.end(4)
-    total.start(5)
-    earlier_out[...] = (crow[...].astype(F32) + earlier.finish()).astype(BF)
-    total.end(5)
-    total.start(6)
-    rs.a4(2)
+    for i in (4, 5):
+        total.end(i)
+        total.start(i + 1)
     total.end(6)
     gain_out[...] = gmine[7]
     for c in range(N_CHUNK):
@@ -633,47 +622,42 @@
     later.drain()
     earlier.drain()
     total.drain()
-    for copy in outs:
-        copy.wait()
+    hidden.wait()
 
 
 def run(later_in, earlier_in, cot, gate_w, up_w, down_w, gain, gate_sum, up_sum, down_sum):
     tokens, width = later_in.shape
-    rows, cols = gate_w.shape
+    cols, rows = gate_w.shape
     any_ = pl.BlockSpec(memory_space=pl.ANY)
     vm = pl.BlockSpec(memory_space=pltpu.VMEM)
-    act = (N_CHUNK, tokens, CHUNK)
     tok = (tokens, width)
     dma = pltpu.SemaphoreType.DMA
     return pl.pallas_call(
         sublayer,
         out_shape=[
             jax.ShapeDtypeStruct((tokens // 8, width), BF),
-            jax.ShapeDtypeStruct((tokens, N_CHUNK * CHUNK), BF),
+            jax.ShapeDtypeStruct((cols, tokens), BF),
             jax.ShapeDtypeStruct((tokens // 8, width), BF),
-            jax.ShapeDtypeStruct((rows, cols), F32),
-            jax.ShapeDtypeStruct((rows, cols), F32),
-            jax.ShapeDtypeStruct((rows, cols), F32),
+            jax.ShapeDtypeStruct((cols, rows), F32),
+            jax.ShapeDtypeStruct((cols, rows), F32),
+            jax.ShapeDtypeStruct((cols, rows), F32),
             jax.ShapeDtypeStruct((1, width), F32),
         ],
-        in_specs=[any_] * 3 + [vm] * 4 + [any_] * 3,
+        in_specs=[any_] * 6 + [vm] + [any_] * 3,
         out_specs=[vm, any_] + [vm] * 5,
         scratch_shapes=[
-            pltpu.VMEM((N_CHUNK, width, WIDE), BF),
-            pltpu.VMEM((N_CHUNK, 4, 4, SHARD, WIDE), BF),
-            pltpu.VMEM(tok, BF),
-            pltpu.VMEM(tok, BF),
-            pltpu.VMEM(tok, BF),
-            pltpu.VMEM(tok, BF),
-            pltpu.VMEM(tok, BF),
-            pltpu.VMEM(act, BF),
-            pltpu.VMEM(act, BF),
-            pltpu.VMEM(act, BF),
-            pltpu.VMEM((tokens, CHUNK), BF),
-            pltpu.VMEM((N_CHUNK, 2, 2, 4, SHARD // 4, WIDE), BF),
-            pltpu.VMEM((N_CHUNK, 2, 2, 4, SHARD // 2, WIDE), BF),
-            pltpu.VMEM((N_CHUNK, 2, 2, SHARD // 4, WIDE), BF),
-            pltpu.VMEM((N_CHUNK, 2, 2, SHARD // 2, WIDE), BF),
+            pltpu.VMEM((N_CHUNK, WIDE, width), BF),
+            pltpu.VMEM((N_CHUNK, 4, 4, WIDE, SHARD), BF),
+            *[pltpu.VMEM(tok, BF)] * 6,
+            pltpu.VMEM((N_CHUNK * CHUNK, tokens), BF),
+            pltpu.VMEM((N_CHUNK, 2 * CHUNK, tokens), BF),
+            pltpu.VMEM((CHUNK, tokens), BF),
+            pltpu.VMEM((256, 2 * CHUNK), BF),
+            pltpu.VMEM((N_CHUNK, 256, 2 * CHUNK), BF),
+            pltpu.VMEM((N_CHUNK, 2, 2, 4, CUT, SHARD), BF),
+            pltpu.VMEM((N_CHUNK, 2, 2, 4, HALF, SHARD), BF),
+            pltpu.VMEM((N_CHUNK, 2, 2, CUT, SHARD), BF),
+            pltpu.VMEM((N_CHUNK, 2, 2, HALF, SHARD), BF),
             pltpu.VMEM((256, width), F32),
             pltpu.VMEM((SHARD, width), BF),
             pltpu.VMEM((SHARD, width), BF),
@@ -681,6 +665,7 @@
             pltpu.VMEM((8, 1, width), F32),
             pltpu.VMEM((7, 1, width), F32),
             dma((9,)),
+            dma((N_CHUNK, 3)),
             dma((N_CHUNK, 2, 20)),
             dma((N_CHUNK, 2, 20)),
             dma((N_CHUNK, 2, 8)),
@@ -690,7 +675,7 @@
             dma((7,)),
             dma((7,)),
             pltpu.SemaphoreType.REGULAR((3,)),
-            dma((N_CHUNK,)),
+            dma,
         ],
         compiler_params=pltpu.CompilerParams(
             collective_id=0, has_side_effects=True, vmem_limit_bytes=64 * 1024 * 1024 - 65536
@@ -701,11 +686,11 @@
 
 def local(later_in, earlier_in, cot, gate_w, up_w, down_w, gain, gate_sum, up_sum, down_sum, gain_sum):
     later_out, hidden, earlier_grad, gate_new, up_new, down_new, gain_total = run(
-        later_in, earlier_in, cot, gate_w, up_w, down_w, gain, gate_sum, up_sum, down_sum
+        later_in, earlier_in, cot, gate_w.T, up_w.T, down_w.T, gain, gate_sum.T, up_sum.T, down_sum.T
     )
     return (
-        later_out, hidden[:, : gate_w.shape[1]], earlier_grad,
-        gate_new, up_new, down_new, gain_sum + gain_total[0],
+        later_out, hidden.T, earlier_grad,
+        gate_new.T, up_new.T, down_new.T, gain_sum + gain_total[0],
     )
 
 

time: 166 us -> 152 us (0.916)
  local copies, waits for them, and re-layouts: 21.1 us -> 8.75 us
  Pallas kernels: 142 us -> 140 us
    unnamed x18 -> x14, local copies, waits for them, and re-layouts: 19.8 us -> 7.46 us
where the time goes in v4:
time: 152 us; the launch traced here: 151 us
  Pallas kernels  140 us (92%)
  local copies, waits for them, and re-layouts  8.75 us (6%)
    pallas_call x1, Pallas kernels, run(): pl.pallas_call(sublayer, out_shape=[jax.ShapeDtypeStruct((tokens // 8, wi...  140 us
    unnamed x14, local copies, waits for them, and re-layouts  7.46 us

profile of v4, /device:TPU:0, one launch (start us, length us, event | category | flops | bytes accessed | tf_op | source)
XLA Modules:
  0.0 151.2 jit_solution(3197063076774925856)
XLA Ops:
  0.6 1.3 reshape.17.gain
  1.9 140.4 %sublayer.1 = (bf16[128,2048]{1,0:T(8,128)(2,1)}, bf16[704,1024]{1,0:T(8,128)(2,1)}, bf16[128,2048]{1,0:T(8,128)(2,1)}, f32[704,128]{1,0:T(8,128)}, f32[704,128]...) custom-call(bf16[1024,2048]{1,0:T(8,128)(2,1)} %later_in.1, bf16[1024,2048]{1,0:T(8,128)(2,1)} %earlier_in.1, ...), custom_call_target="tpu_custom_call" | custom-call | tf_op jit(solution)/shard_map/sublayer/pallas_call | solution.py:635
  142.3 0.0 copy-start
  142.3 0.0 copy-start.3
  142.3 0.0 copy-start.2
  142.3 0.0 copy-start.1
  142.4 1.4 add.3
  143.8 1.9 %copy.24 = bf16[128,2048]{1,0:T(8,128)(2,1)} copy(bf16[128,2048]{1,0:T(8,128)(2,1)} %get-tuple-element.28) | data formatting | bytes 1048576
  145.7 2.6 %copy.25 = bf16[1024,704]{0,1:T(8,128)(2,1)} copy(bf16[1024,704]{0,1:T(8,128)(2,1)} %bitcast.11) | data formatting | bytes 2883584
  148.2 0.0 copy-done
  148.2 0.8 copy.26
  149.0 0.0 copy-done.3
  149.0 0.7 copy.27
  149.8 0.0 copy-done.2
  149.8 0.7 copy.28
  150.5 0.0 copy-done.1
  150.5 0.7 copy.29
Async XLA Ops:
  142.3 5.9 %copy-start = (bf16[128,2048]{1,0:T(8,128)(2,1)S(1)}, bf16[128,2048]{1,0:T(8,128)(2,1)}, u32[]{:S(2)}) copy-start(bf16[128,2048]{1,0:T(8,128)(2,1)} %get-tuple-element.30) | copy-start | bytes 1572868
  142.3 6.7 %copy-start.3 = (f32[704,128]{1,0:T(8,128)S(1)}, f32[704,128]{1,0:T(8,128)}, u32[]{:S(2)}) copy-start(f32[704,128]{1,0:T(8,128)} %get-tuple-element.17) | copy-start | bytes 1081348
  142.3 7.4 %copy-start.2 = (f32[704,128]{1,0:T(8,128)S(1)}, f32[704,128]{1,0:T(8,128)}, u32[]{:S(2)}) copy-start(f32[704,128]{1,0:T(8,128)} %get-tuple-element.18) | copy-start | bytes 1081348
  142.3 8.2 %copy-start.1 = (f32[704,128]{1,0:T(8,128)S(1)}, f32[704,128]{1,0:T(8,128)}, u32[]{:S(2)}) copy-start(f32[704,128]{1,0:T(8,128)} %get-tuple-element.19) | copy-start | bytes 1081348

commit v5 on v4

--- a/solution.py
+++ b/solution.py
@@ -14,18 +14,21 @@
 MESH = pl.DeviceIdType.MESH
 BF = jnp.bfloat16
 F32 = jnp.float32
-N_CHUNK = 2
-CHUNK = 352
-WIDE = 3 * CHUNK
-HALF = WIDE // 2
-CUT = 272
+SIZES = (192, 256, 256)
+STARTS = (0, 192, 448)
+N_CHUNK = 3
 SHARD = 128
 NORM_FLOOR = 0.05
 
 
-def span(h, sub=None):
-    at = h * HALF
-    return slice(at + (CUT if sub == 1 else 0), at + (CUT if sub == 0 else HALF))
+def half_of(c):
+    return SIZES[c] * 3 // 2
+
+
+def span(c, h, sub=None):
+    n = half_of(c)
+    at = h * n
+    return slice(at + (n // 2 if sub == 1 else 0), at + (n // 2 if sub == 0 else n))
 
 
 class Gather:
@@ -38,8 +41,8 @@
         return lax.rem(self.mz + dz + 4, 4) * 4 + lax.rem(self.mx + dx + 4, 4)
 
     def copy(self, c, h, msg, jf, js, sub, axis, d):
-        view = self.w.at[
-            c, span(h, sub), pl.ds(pl.multiple_of(self.owner(h, jf, js) * SHARD, SHARD), SHARD)
+        view = self.w[c].at[
+            span(c, h, sub), pl.ds(pl.multiple_of(self.owner(h, jf, js) * SHARD, SHARD), SHARD)
         ]
         name = ("x", "z")[h] if axis == "f" else ("z", "x")[h]
         me = self.mx if name == "x" else self.mz
@@ -152,8 +155,8 @@
 
 
 class Scatter:
-    def __init__(self, g, r1, r2, r3, r4, send, recv, out):
-        self.g, self.r = g, (r1, r2, r3, r4)
+    def __init__(self, g, r, send, recv, out):
+        self.g, self.r = g, r
         self.send, self.recv, self.out = send, recv, out
         self.at = {"z": lax.axis_index("z"), "x": lax.axis_index("x")}
 
@@ -162,14 +165,10 @@
         f = lax.rem(self.at[fast] + jf + 4, 4)
         s = slice(None) if js is None else lax.rem(self.at[slow] + js + 4, 4)
         where = (s, f) if h == 0 else (f, s)
-        return self.g.at[(c, *where, span(h, sub), slice(None))]
+        return self.g[c].at[(*where, span(c, h, sub), slice(None))]
 
     def landing(self, stage, c, h, i):
-        ref = self.r[stage]
-        if stage % 2:
-            return ref.at[c, h, i]
-        n = CUT if i == 0 else HALF - CUT
-        return ref.at[c, h, i, :, :n] if stage == 0 else ref.at[c, h, i, :n]
+        return self.r[c][stage].at[h, i]
 
     def copy(self, stage, c, h, d, src):
         i = 0 if d > 0 else 1
@@ -218,7 +217,9 @@
             whole = self.unit(c, h, 0)
             for k in range(4):
                 whole[k] = (
-                    whole[k].astype(F32) + self.r[1][c, h, 0, k].astype(F32) + self.r[1][c, h, 1, k].astype(F32)
+                    whole[k].astype(F32)
+                    + self.landing(1, c, h, 0)[k].astype(F32)
+                    + self.landing(1, c, h, 1)[k].astype(F32)
                 ).astype(BF)
             for d in (1, -1):
                 self.c3(c, h, d).start()
@@ -237,12 +238,17 @@
             for d in (1, -1):
                 self.c4(c, h, d).wait_recv()
             own = self.unit(c, h, 0, 0)
-            done = own[...].astype(F32) + self.r[3][c, h, 0].astype(F32) + self.r[3][c, h, 1].astype(F32)
+            done = (
+                own[...].astype(F32)
+                + self.landing(3, c, h, 0)[...].astype(F32)
+                + self.landing(3, c, h, 1)[...].astype(F32)
+            )
+            n, size = half_of(c), SIZES[c]
             for k, out in enumerate(self.out):
-                first, last = max(h * HALF, k * CHUNK), min((h + 1) * HALF, (k + 1) * CHUNK)
+                first, last = max(h * n, k * size), min((h + 1) * n, (k + 1) * size)
                 if first < last:
-                    at = slice(c * CHUNK + first - k * CHUNK, c * CHUNK + last - k * CHUNK)
-                    out[at, :] = out[at, :] + done[first - h * HALF : last - h * HALF]
+                    at = slice(STARTS[c] + first - k * size, STARTS[c] + last - k * size)
+                    out[at, :] = out[at, :] + done[first - h * n : last - h * n]
 
     def drain(self, c):
         for h in (0, 1):
@@ -252,8 +258,8 @@
 
 
 class TokenScatter:
-    def __init__(self, t, p, rc, q, credit, send, recv):
-        self.t, self.p, self.rc, self.q, self.credit = t, p, rc, q, credit
+    def __init__(self, t, p, buf, credit, send, recv):
+        self.t, self.p, self.buf, self.credit = t, p, buf, credit
         self.send, self.recv = send, recv
         self.y, self.c = lax.axis_index("y"), lax.axis_index("c")
 
@@ -267,16 +273,19 @@
         return self.p.at[pl.ds(pl.multiple_of(start, SHARD // 2), n), :]
 
     def landed(self, k):
-        start = self.t * 4 * SHARD + self.to(k) * SHARD
-        return self.rc.at[pl.ds(pl.multiple_of(start, SHARD), SHARD), :]
+        return self.buf.at[pl.ds(pl.multiple_of(self.to(k) * SHARD, SHARD), SHARD), :]
 
     def q1(self, i):
-        start = self.t * 3 * SHARD + i * (SHARD // 2)
-        return self.q.at[start : start + SHARD // 2, :]
+        start = 4 * SHARD + i * (SHARD // 2)
+        return self.buf.at[start : start + SHARD // 2, :]
 
     def q2(self, i):
-        start = self.t * 3 * SHARD + (1 + i) * SHARD
-        return self.q.at[start : start + SHARD, :]
+        start = (5 + i) * SHARD
+        return self.buf.at[start : start + SHARD, :]
+
+    def ready(self):
+        for i, peer in enumerate(({"c": 1 - self.c}, {"y": self.to(-1)}, {"y": self.to(1)})):
+            pl.semaphore_signal(self.credit.at[self.t, i], inc=1, device_id=peer, device_id_type=MESH)
 
     def pair(self, k):
         return pltpu.make_async_remote_copy(
@@ -307,8 +316,8 @@
         return self.ring(self.rows(d, self.c), self.q2(i), 6 + i, d)
 
     def share(self, k):
-        if self.t == 0 and k == 2:
-            pl.semaphore_wait(self.credit.at[0], 1)
+        if k == 2:
+            pl.semaphore_wait(self.credit.at[self.t, 0], 1)
         self.pair(k).start()
 
     def join(self, k):
@@ -319,8 +328,7 @@
     def far(self):
         self.join(2)
         for d in (1, -1):
-            if self.t == 0:
-                pl.semaphore_wait(self.credit.at[1 if d > 0 else 2], 1)
+            pl.semaphore_wait(self.credit.at[self.t, 1 if d > 0 else 2], 1)
             self.y1(d).start()
 
     def near(self, d):
@@ -387,7 +395,7 @@
 def sublayer(
     later_in, earlier_in, cot_in, gate_w, up_w, down_w, gain, gate_sum, up_sum, down_sum,
     later_out, hidden_out, earlier_out, gate_new, up_new, down_new, gain_out,
-    w, g, nl, ne, cot, nlt, net, cott, hl, dx, he, hb, xb, r1, r2, r3, r4, dn, lrow, crow, gacc, gmine, gtheirs,
+    w, g, r, nl, ne, cot, nlt, net, cott, hl, dx, he, hb, xb, dn, lrow, crow, gacc, gmine, gtheirs,
     in_sem, own_sem, wsend, wrecv, send, recv, tsend, trecv, gsend, grecv, credit, out_sem,
 ):
     tokens, width = nl.shape
@@ -398,8 +406,8 @@
     mine = pl.ds(pl.multiple_of(me * SHARD, SHARD), SHARD)
     own = [
         pltpu.make_async_copy(
-            ref.at[c * CHUNK : (c + 1) * CHUNK, :],
-            w.at[c, k * CHUNK : (k + 1) * CHUNK, mine],
+            ref.at[STARTS[c] : STARTS[c] + SIZES[c], :],
+            w[c].at[k * SIZES[c] : (k + 1) * SIZES[c], mine],
             own_sem.at[c, k],
         )
         for c in range(N_CHUNK)
@@ -422,9 +430,9 @@
     ring.t0(0)
     for copy in ins[3:]:
         copy.start()
-    rs = Scatter(g, r1, r2, r3, r4, send, recv, (gate_new, up_new, down_new))
-    later = TokenScatter(0, nl, net, cot, credit, tsend, trecv)
-    earlier = TokenScatter(1, ne, net, cot, credit, tsend, trecv)
+    rs = Scatter(g, r, send, recv, (gate_new, up_new, down_new))
+    later = TokenScatter(0, nl, nlt, credit, tsend, trecv)
+    earlier = TokenScatter(1, ne, net, credit, tsend, trecv)
     total = GainSum(gmine, gtheirs, gsend, grecv)
 
     gain_row = gain[...].astype(F32)
@@ -435,9 +443,12 @@
             at = pl.ds(pl.multiple_of(i * 128 + j * tokens, 128), 128)
             turned[:, at] = ref[rows, j * half : (j + 1) * half].T
 
+    def tok(i):
+        return pl.ds(pl.multiple_of(i * 256, 256), 256)
+
     def turned_cols(turned, i):
         return jnp.concatenate(
-            [turned[:, j * tokens + i * 256 : j * tokens + (i + 1) * 256] for j in (0, 1)], axis=0
+            [turned[:, pl.ds(pl.multiple_of(i * 256 + j * tokens, 256), 256)] for j in (0, 1)], axis=0
         )
 
     def norms(ref, first, last):
@@ -455,84 +466,71 @@
 
     blocks = tokens // 128
 
-    ins[0].wait()
-    norms(nl, 0, blocks)
-    ring.t1(0)
-    norms(nl, blocks, 2 * blocks)
-    turns(nlt, nl, 0, blocks)
-    ring.t2(0)
-    ins[1].wait()
-    norms(ne, 0, 2 * blocks)
-    ring.t3(0)
-    ring.t0(1)
-    turns(net, ne, 0, blocks)
-    ring.t4(0)
-    ring.t1(1)
-    ins[2].wait()
-    turns(cott, cot, 0, blocks)
-    ring.t5(0)
-    ring.t2(1)
-    for copy in ins[3:]:
-        copy.wait()
-    ring.t6(0)
-
-    def tok_cols(i):
-        return slice(i * 256, (i + 1) * 256)
+    def looped(item, c, first, count):
+        @pl.loop(first, first + count)
+        def _(i):
+            item(c, i)
 
     def later_item(c, i):
-        pre = nn(w[c, : 2 * CHUNK, :], turned_cols(nlt, i))
-        gate, up = pre[:CHUNK], pre[CHUNK:]
-        hl[c * CHUNK : (c + 1) * CHUNK, tok_cols(i)] = (gate * jax.nn.sigmoid(gate) * up).astype(BF)
+        n = SIZES[c]
+        pre = nn(w[c][: 2 * n, :], turned_cols(nlt, i))
+        gate, up = pre[:n], pre[n:]
+        hl[STARTS[c] : STARTS[c] + n, tok(i)] = (gate * jax.nn.sigmoid(gate) * up).astype(BF)
 
     def earlier_item(c, i):
-        pre = nn(w[c, : 2 * CHUNK, :], turned_cols(net, i))
-        dh = 0.5 * nn(w[c, 2 * CHUNK :, :], turned_cols(cott, i))
-        gate, up = pre[:CHUNK], pre[CHUNK:]
+        n = SIZES[c]
+        pre = nn(w[c][: 2 * n, :], turned_cols(net, i))
+        dh = 0.5 * nn(w[c][2 * n :, :], turned_cols(cott, i))
+        gate, up = pre[:n], pre[n:]
         s = jax.nn.sigmoid(gate)
         act = gate * s
-        he[:, tok_cols(i)] = (act * up).astype(BF)
-        dx[c, :CHUNK, tok_cols(i)] = (dh * up * s * (1.0 + gate * (1.0 - s))).astype(BF)
-        dx[c, CHUNK:, tok_cols(i)] = (dh * act).astype(BF)
+        he[:n, tok(i)] = (act * up).astype(BF)
+        dx[c][:n, tok(i)] = (dh * up * s * (1.0 + gate * (1.0 - s))).astype(BF)
+        dx[c][n:, tok(i)] = (dh * act).astype(BF)
 
     def grad_item(c, i):
+        n = SIZES[c]
         for j in (0, 1):
-            cols = slice(i * 512 + j * 256, i * 512 + (j + 1) * 256)
-            both = nn(dx[c], ne[:, cols]).astype(BF)
-            down = (0.5 * nn(he[...], cot[:, cols])).astype(BF)
-            for n in (0, 1):
-                lanes = slice(n * SHARD, (n + 1) * SHARD)
-                g[c, i, 2 * j + n, : 2 * CHUNK, :] = both[:, lanes]
-                g[c, i, 2 * j + n, 2 * CHUNK :, :] = down[:, lanes]
+            cols = pl.ds(pl.multiple_of(i * 512 + j * 256, 256), 256)
+            both = nn(dx[c][...], ne[:, cols]).astype(BF)
+            down = (0.5 * nn(he[:n, :], cot[:, cols])).astype(BF)
+            for m in (0, 1):
+                lanes = slice(m * SHARD, (m + 1) * SHARD)
+                g[c][i, 2 * j + m, : 2 * n, :] = both[:, lanes]
+                g[c][i, 2 * j + m, 2 * n :, :] = down[:, lanes]
+
+    L = functools.partial(looped, later_item)
+    E = functools.partial(looped, earlier_item)
+    G = functools.partial(looped, grad_item)
 
     reload = pltpu.make_async_copy(earlier_in, cott, in_sem.at[8])
-
-    def free():
-        reload.start()
-        pl.semaphore_signal(credit.at[0], inc=1, device_id={"c": 1 - c_me}, device_id_type=MESH)
-        pl.semaphore_signal(credit.at[1], inc=1, device_id={"y": lax.rem(y + 3, 4)}, device_id_type=MESH)
-        pl.semaphore_signal(credit.at[2], inc=1, device_id={"y": lax.rem(y + 1, 4)}, device_id_type=MESH)
-
     hidden = pltpu.make_async_copy(hl, hidden_out, out_sem)
 
-    def token_cols(b):
-        return pl.ds(pl.multiple_of(b * 256, 256), 256)
+    def features(n):
+        return pl.ds(pl.multiple_of(n * 512, 512), 512)
 
     def later_block(k):
         b = lax.rem(y + k + 4, 4)
-        hb[...] = hl[:, token_cols(b)].T
-        for n in range(width // 512):
-            f = slice(n * 512, (n + 1) * 512)
-            nl[token_cols(b), f] = nn(
-                hb[...], jnp.concatenate([w[c, 2 * CHUNK :, f] for c in range(N_CHUNK)], axis=0)
-            ).astype(BF)
+        hb[...] = hl[:, tok(b)].T
+
+        @pl.loop(0, width // 512)
+        def _(n):
+            f = features(n)
+            rows = [w[c][2 * SIZES[c] :, f] for c in range(N_CHUNK)]
+            nl[tok(b), f] = nn(hb[...], jnp.concatenate(rows, axis=0)).astype(BF)
+
+        later.share(k)
 
     def earlier_block(k):
         b = lax.rem(y + k + 4, 4)
         for c in range(N_CHUNK):
-            xb[c] = dx[c, :, token_cols(b)].T
-        for n in range(width // 512):
-            f = slice(n * 512, (n + 1) * 512)
-            dn[:, f] = nn(xb[0], w[0, : 2 * CHUNK, f]) + nn(xb[1], w[1, : 2 * CHUNK, f])
+            xb[:, 2 * STARTS[c] : 2 * (STARTS[c] + SIZES[c])] = dx[c][:, tok(b)].T
+
+        @pl.loop(0, width // 512)
+        def _(n):
+            f = features(n)
+            rows = [w[c][: 2 * SIZES[c], f] for c in range(N_CHUNK)]
+            dn[:, f] = nn(xb[...], jnp.concatenate(rows, axis=0))
 
         @pl.loop(0, 16)
         def _(i):
@@ -548,72 +546,106 @@
 
         earlier.share(k)
 
+    ins[0].wait()
+    norms(nl, 0, blocks)
+    ring.t1(0)
+    norms(nl, blocks, 2 * blocks)
+    turns(nlt, nl, 0, blocks // 2)
+    ring.t2(0)
+    turns(nlt, nl, blocks // 2, blocks)
+    ring.t3(0)
+    ring.t0(1)
+    ins[1].wait()
+    norms(ne, 0, 2 * blocks)
+    ring.t4(0)
+    turns(net, ne, 0, blocks)
+    ring.t5(0)
+    ring.t1(1)
+    ins[2].wait()
+    turns(cott, cot, 0, blocks)
     gacc[...] = jnp.zeros_like(gacc)
-    for i in range(4):
-        earlier_item(0, i)
-        if i == 1:
-            ring.t3(1)
+    for copy in ins[3:]:
+        copy.wait()
+    ring.t6(0)
+
+    E(0, 0, 2)
+    ring.t2(1)
+    E(0, 2, 2)
+    ring.t3(1)
+    ring.t0(2)
+    G(0, 0, 2)
     ring.t4(1)
-    for i in range(4):
-        grad_item(0, i)
-        if i == 1:
-            ring.t5(1)
-    for i in range(4):
-        later_item(0, i)
-        if i == 1:
-            rs.s1(0)
+    G(0, 2, 2)
+    ring.t5(1)
+    ring.t1(2)
+    L(0, 0, 4)
     ring.t6(1)
-    for i in range(4):
-        later_item(1, i)
+
+    E(1, 0, 2)
+    ring.t2(2)
+    E(1, 2, 2)
+    ring.t3(2)
+    rs.s1(0)
+    G(1, 0, 2)
+    ring.t4(2)
+    G(1, 2, 2)
+    ring.t5(2)
+    rs.s1(1)
+    L(1, 0, 4)
+    rs.a1(0)
+    ring.t6(2)
+
+    L(2, 0, 4)
+    later.ready()
     hidden.start()
-    rs.a1(0)
     later_block(2)
     later_block(1)
-    for i in range(4):
-        earlier_item(1, i)
+    rs.a1(1)
+    later.far()
+    E(2, 0, 2)
     rs.a2(0)
-    for i in range(4):
-        grad_item(1, i)
-    free()
-    rs.s1(1)
-    later.share(2)
-    later.share(1)
-    later.far()
+    E(2, 2, 2)
+    earlier.ready()
+    reload.start()
+    G(2, 0, 4)
+    rs.s1(2)
+    later_block(-1)
+    rs.a3(0)
+    later_block(0)
+    later.near(1)
+    later.near(-1)
     reload.wait()
     earlier_block(2)
-    later_block(-1)
-    later.share(-1)
+    rs.a1(2)
+    rs.a2(1)
+    earlier_block(1)
     earlier.far()
-    later_block(0)
-    later.share(0)
-    rs.a3(0)
-    earlier_block(1)
-    later.near(1)
-    later.near(-1)
-    rs.a1(1)
+    rs.a4(0)
     earlier_block(-1)
-    earlier.near(1)
-    earlier.near(-1)
-    rs.a4(0)
+    rs.a3(1)
     earlier_block(0)
     gmine[0] = jnp.sum(gacc[...], axis=0, keepdims=True)
     total.start(0)
-    later_out[...] = (lrow[...].astype(F32) + 0.5 * later.finish()).astype(BF)
     total.end(0)
     total.start(1)
-    rs.a2(1)
+    later_out[...] = (lrow[...].astype(F32) + 0.5 * later.finish()).astype(BF)
     total.end(1)
     total.start(2)
-    rs.a3(1)
+    earlier.near(1)
+    earlier.near(-1)
     total.end(2)
     total.start(3)
-    earlier_out[...] = (crow[...].astype(F32) + earlier.finish()).astype(BF)
+    rs.a2(2)
     total.end(3)
     total.start(4)
+    rs.a3(2)
     rs.a4(1)
-    for i in (4, 5):
-        total.end(i)
-        total.start(i + 1)
+    total.end(4)
+    total.start(5)
+    rs.a4(2)
+    total.end(5)
+    total.start(6)
+    earlier_out[...] = (crow[...].astype(F32) + earlier.finish()).astype(BF)
     total.end(6)
     gain_out[...] = gmine[7]
     for c in range(N_CHUNK):
@@ -646,18 +678,23 @@
         in_specs=[any_] * 6 + [vm] + [any_] * 3,
         out_specs=[vm, any_] + [vm] * 5,
         scratch_shapes=[
-            pltpu.VMEM((N_CHUNK, WIDE, width), BF),
-            pltpu.VMEM((N_CHUNK, 4, 4, WIDE, SHARD), BF),
+            [pltpu.VMEM((3 * n, width), BF) for n in SIZES],
+            [pltpu.VMEM((4, 4, 3 * n, SHARD), BF) for n in SIZES],
+            [
+                [
+                    pltpu.VMEM((2, 2, 4, half_of(c) // 2, SHARD), BF),
+                    pltpu.VMEM((2, 2, 4, half_of(c), SHARD), BF),
+                    pltpu.VMEM((2, 2, half_of(c) // 2, SHARD), BF),
+                    pltpu.VMEM((2, 2, half_of(c), SHARD), BF),
+                ]
+                for c in range(N_CHUNK)
+            ],
             *[pltpu.VMEM(tok, BF)] * 6,
-            pltpu.VMEM((N_CHUNK * CHUNK, tokens), BF),
-            pltpu.VMEM((N_CHUNK, 2 * CHUNK, tokens), BF),
-            pltpu.VMEM((CHUNK, tokens), BF),
-            pltpu.VMEM((256, 2 * CHUNK), BF),
-            pltpu.VMEM((N_CHUNK, 256, 2 * CHUNK), BF),
-            pltpu.VMEM((N_CHUNK, 2, 2, 4, CUT, SHARD), BF),
-            pltpu.VMEM((N_CHUNK, 2, 2, 4, HALF, SHARD), BF),
-            pltpu.VMEM((N_CHUNK, 2, 2, CUT, SHARD), BF),
-            pltpu.VMEM((N_CHUNK, 2, 2, HALF, SHARD), BF),
+            pltpu.VMEM((cols, tokens), BF),
+            [pltpu.VMEM((2 * n, tokens), BF) for n in SIZES],
+            pltpu.VMEM((max(SIZES), tokens), BF),
+            pltpu.VMEM((256, cols), BF),
+            pltpu.VMEM((256, 2 * cols), BF),
             pltpu.VMEM((256, width), F32),
             pltpu.VMEM((SHARD, width), BF),
             pltpu.VMEM((SHARD, width), BF),
@@ -674,7 +711,7 @@
             dma((2, 8)),
             dma((7,)),
             dma((7,)),
-            pltpu.SemaphoreType.REGULAR((3,)),
+            pltpu.SemaphoreType.REGULAR((2, 3)),
             dma,
         ],
         compiler_params=pltpu.CompilerParams(

time: 152 us -> 140 us (0.921)
  Pallas kernels: 140 us -> 129 us
    pallas_call x1, Pallas kernels: 140 us -> 129 us  [run(): pl.pallas_call(sublayer, out_shape=[jax.ShapeDtypeStruct((tokens // 8, wi...]
where the time goes in v5:
time: 140 us
  Pallas kernels  129 us (92%)
  local copies, waits for them, and re-layouts  8.75 us (6%)
  other arithmetic  1.43 us (1%)
    pallas_call x1, Pallas kernels, run(): pl.pallas_call(sublayer, out_shape=[jax.ShapeDtypeStruct((tokens // 8, wi...  129 us
    unnamed x14, local copies, waits for them, and re-layouts  7.46 us

profile of v5, /device:TPU:0, one launch (start us, length us, event | category | flops | bytes accessed | tf_op | source)
XLA Modules:
  0.0 139.9 jit_solution(7170938368225140504)
XLA Ops:
  0.6 1.3 reshape.17.gain
  1.9 129.1 %sublayer.1 = (bf16[128,2048]{1,0:T(8,128)(2,1)}, bf16[704,1024]{1,0:T(8,128)(2,1)}, bf16[128,2048]{1,0:T(8,128)(2,1)}, f32[704,128]{1,0:T(8,128)}, f32[704,128]...) custom-call(bf16[1024,2048]{1,0:T(8,128)(2,1)} %later_in.1, bf16[1024,2048]{1,0:T(8,128)(2,1)} %earlier_in.1, ...), custom_call_target="tpu_custom_call" | custom-call | tf_op jit(solution)/shard_map/sublayer/pallas_call | solution.py:667
  131.0 0.0 copy-start
  131.0 0.0 copy-start.3
  131.0 0.0 copy-start.2
  131.0 0.0 copy-start.1
  131.0 1.4 %add.3 = f32[2048]{0:T(1024)} add(f32[2048]{0:T(1024)} %param.21, f32[2048]{0:T(1024)} %bitcast.21) | non-fusion elementwise | flops 2048 | bytes 24576 | tf_op jit(solution)/shard_map/add | solution.py:730
  132.5 1.9 %copy.24 = bf16[128,2048]{1,0:T(8,128)(2,1)} copy(bf16[128,2048]{1,0:T(8,128)(2,1)} %get-tuple-element.28) | data formatting | bytes 1048576
  134.3 2.6 %copy.25 = bf16[1024,704]{0,1:T(8,128)(2,1)} copy(bf16[1024,704]{0,1:T(8,128)(2,1)} %bitcast.11) | data formatting | bytes 2883584
  136.9 0.0 copy-done
  136.9 0.8 copy.26
  137.7 0.0 copy-done.3
  137.7 0.7 copy.27
  138.4 0.0 copy-done.2
  138.4 0.7 copy.28
  139.2 0.0 copy-done.1
  139.2 0.7 copy.29
Async XLA Ops:
  131.0 5.9 %copy-start = (bf16[128,2048]{1,0:T(8,128)(2,1)S(1)}, bf16[128,2048]{1,0:T(8,128)(2,1)}, u32[]{:S(2)}) copy-start(bf16[128,2048]{1,0:T(8,128)(2,1)} %get-tuple-element.30) | copy-start | bytes 1572868
  131.0 6.7 %copy-start.3 = (f32[704,128]{1,0:T(8,128)S(1)}, f32[704,128]{1,0:T(8,128)}, u32[]{:S(2)}) copy-start(f32[704,128]{1,0:T(8,128)} %get-tuple-element.17) | copy-start | bytes 1081348
  131.0 7.4 %copy-start.2 = (f32[704,128]{1,0:T(8,128)S(1)}, f32[704,128]{1,0:T(8,128)}, u32[]{:S(2)}) copy-start(f32[704,128]{1,0:T(8,128)} %get-tuple-element.18) | copy-start | bytes 1081348
  131.0 8.2 %copy-start.1 = (f32[704,128]{1,0:T(8,128)S(1)}, f32[704,128]{1,0:T(8,128)}, u32[]{:S(2)}) copy-start(f32[704,128]{1,0:T(8,128)} %get-tuple-element.19) | copy-start | bytes 1081348

commit v6 on v5

--- a/solution.py
+++ b/solution.py
@@ -87,36 +87,21 @@
             for d in (1, -1):
                 self.m3(c, h, 0, d).start()
 
-    def t1(self, c):
+    def t1(self, c, h, d):
+        self.r1(c, h, d).wait_recv()
+        self.m2(c, h, d).start()
+        for e in (1, -1):
+            self.m3(c, h, -d, e).start()
+
+    def t3(self, c, h):
         for d in (1, -1):
-            for h in (0, 1):
-                self.r1(c, h, d).wait_recv()
-                self.m2(c, h, d).start()
-                for e in (1, -1):
-                    self.m3(c, h, -d, e).start()
-
-    def pass_on(self, c, js):
-        for j in js:
-            for d in (1, -1):
-                for h in (0, 1):
-                    self.r3(c, h, j, d).wait_recv()
-                    self.m4(c, h, j, d).start()
-
-    def t2(self, c):
-        self.pass_on(c, (0,))
-
-    def t3(self, c):
-        for h in (0, 1):
-            for d in (1, -1):
-                self.r2(c, h, d).wait_recv()
-            for e in (1, -1):
-                self.m3(c, h, 2, e).start()
-
-    def t4(self, c):
-        self.pass_on(c, (-1, 1))
-
-    def t5(self, c):
-        self.pass_on(c, (2,))
+            self.r2(c, h, d).wait_recv()
+        for e in (1, -1):
+            self.m3(c, h, 2, e).start()
+
+    def hand(self, c, h, j, d):
+        self.r3(c, h, j, d).wait_recv()
+        self.m4(c, h, j, d).start()
 
     def t6(self, c):
         for h in (0, 1):
@@ -200,55 +185,49 @@
             for d in (1, -1):
                 self.c1(c, h, d).start()
 
-    def a1(self, c):
+    def a1(self, c, h, d):
+        i = 0 if d > 0 else 1
+        self.c1(c, h, d).wait_recv()
+        part = self.unit(c, h, d, None, i)
+        for k in range(4):
+            part[k] = part[k] + self.landing(0, c, h, i)[k]
+        self.c2(c, h, d).start()
+
+    def a2(self, c, h):
         for d in (1, -1):
-            for h in (0, 1):
-                i = 0 if d > 0 else 1
-                self.c1(c, h, d).wait_recv()
-                part = self.unit(c, h, d, None, i)
-                for k in range(4):
-                    part[k] = part[k] + self.landing(0, c, h, i)[k]
-                self.c2(c, h, d).start()
-
-    def a2(self, c):
-        for h in (0, 1):
-            for d in (1, -1):
-                self.c2(c, h, d).wait_recv()
-            whole = self.unit(c, h, 0)
-            for k in range(4):
-                whole[k] = (
-                    whole[k].astype(F32)
-                    + self.landing(1, c, h, 0)[k].astype(F32)
-                    + self.landing(1, c, h, 1)[k].astype(F32)
-                ).astype(BF)
-            for d in (1, -1):
-                self.c3(c, h, d).start()
-
-    def a3(self, c):
+            self.c2(c, h, d).wait_recv()
+        whole = self.unit(c, h, 0)
+        for k in range(4):
+            whole[k] = (
+                whole[k].astype(F32)
+                + self.landing(1, c, h, 0)[k].astype(F32)
+                + self.landing(1, c, h, 1)[k].astype(F32)
+            ).astype(BF)
         for d in (1, -1):
-            for h in (0, 1):
-                i = 0 if d > 0 else 1
-                self.c3(c, h, d).wait_recv()
-                part = self.unit(c, h, 0, d, i)
-                part[...] = part[...] + self.landing(2, c, h, i)[...]
-                self.c4(c, h, d).start()
-
-    def a4(self, c):
-        for h in (0, 1):
-            for d in (1, -1):
-                self.c4(c, h, d).wait_recv()
-            own = self.unit(c, h, 0, 0)
-            done = (
-                own[...].astype(F32)
-                + self.landing(3, c, h, 0)[...].astype(F32)
-                + self.landing(3, c, h, 1)[...].astype(F32)
-            )
-            n, size = half_of(c), SIZES[c]
-            for k, out in enumerate(self.out):
-                first, last = max(h * n, k * size), min((h + 1) * n, (k + 1) * size)
-                if first < last:
-                    at = slice(STARTS[c] + first - k * size, STARTS[c] + last - k * size)
-                    out[at, :] = out[at, :] + done[first - h * n : last - h * n]
+            self.c3(c, h, d).start()
+
+    def a3(self, c, h, d):
+        i = 0 if d > 0 else 1
+        self.c3(c, h, d).wait_recv()
+        part = self.unit(c, h, 0, d, i)
+        part[...] = part[...] + self.landing(2, c, h, i)[...]
+        self.c4(c, h, d).start()
+
+    def a4(self, c, h):
+        for d in (1, -1):
+            self.c4(c, h, d).wait_recv()
+        own = self.unit(c, h, 0, 0)
+        done = (
+            own[...].astype(F32)
+            + self.landing(3, c, h, 0)[...].astype(F32)
+            + self.landing(3, c, h, 1)[...].astype(F32)
+        )
+        n, size = half_of(c), SIZES[c]
+        for k, out in enumerate(self.out):
+            first, last = max(h * n, k * size), min((h + 1) * n, (k + 1) * size)
+            if first < last:
+                at = slice(STARTS[c] + first - k * size, STARTS[c] + last - k * size)
+                out[at, :] = out[at, :] + done[first - h * n : last - h * n]
 
     def drain(self, c):
         for h in (0, 1):
@@ -355,47 +334,50 @@
             self.y2(d).wait_send()
 
 
-def butterfly():
-    steps = [("c", 1 - lax.axis_index("c"))]
-    for name in ("y", "x", "z"):
+class GainSum:
+    AXES = (("c", 2), ("x", 4), ("z", 4), ("y", 4))
+
+    def __init__(self, rows, send, recv):
+        self.rows, self.send, self.recv = rows, send, recv
+
+    def copy(self, i, d, arriving):
+        name, n = self.AXES[i]
         me = lax.axis_index(name)
-        steps.append((name, me + 1 - 2 * lax.rem(me, 2)))
-        steps.append((name, 3 - me))
-    return steps
-
-
-class GainSum:
-    def __init__(self, mine, theirs, send, recv):
-        self.mine, self.theirs, self.send, self.recv = mine, theirs, send, recv
-        self.steps = butterfly()
-
-    def copy(self, i):
-        name, partner = self.steps[i]
+        src = lax.rem(me + n - d, n) if arriving else me
         return pltpu.make_async_remote_copy(
-            src_ref=self.mine.at[i],
-            dst_ref=self.theirs.at[i],
-            send_sem=self.send.at[i],
-            recv_sem=self.recv.at[i],
-            device_id={name: partner},
+            src_ref=self.rows.at[i, src],
+            dst_ref=self.rows.at[i, src],
+            send_sem=self.send.at[i, d],
+            recv_sem=self.recv.at[i, d],
+            device_id={name: lax.rem(me + d, n)},
             device_id_type=MESH,
         )
 
-    def start(self, i):
-        self.copy(i).start()
+    def start(self, i, row):
+        name, n = self.AXES[i]
+        self.rows[i, lax.axis_index(name)] = row
+        for d in range(1, n):
+            self.copy(i, d, False).start()
 
     def end(self, i):
-        self.copy(i).wait_recv()
-        self.mine[i + 1] = self.mine[i] + self.theirs[i]
+        n = self.AXES[i][1]
+        for d in range(1, n):
+            self.copy(i, d, True).wait_recv()
+        row = self.rows[i, 0]
+        for k in range(1, n):
+            row = row + self.rows[i, k]
+        return row
 
     def drain(self):
-        for i in range(7):
-            self.copy(i).wait_send()
+        for i, (_, n) in enumerate(self.AXES):
+            for d in range(1, n):
+                self.copy(i, d, False).wait_send()
 
 
 def sublayer(
     later_in, earlier_in, cot_in, gate_w, up_w, down_w, gain, gate_sum, up_sum, down_sum,
     later_out, hidden_out, earlier_out, gate_new, up_new, down_new, gain_out,
-    w, g, r, nl, ne, cot, nlt, net, cott, hl, dx, he, hb, xb, dn, lrow, crow, gacc, gmine, gtheirs,
+    w, g, r, nl, ne, cot, nlt, net, cott, hl, dx, he, hb, xb, dn, lrow, crow, gacc, grows,
     in_sem, own_sem, wsend, wrecv, send, recv, tsend, trecv, gsend, grecv, credit, out_sem,
 ):
     tokens, width = nl.shape
@@ -423,7 +405,8 @@
         copy.start()
     for copy in ins[:3]:
         copy.start()
-    greet(ring_peers(("x", "z", "y")) + [{"c": 1 - c_me}])
+    across = [{n: lax.rem(lax.axis_index(n) + 2, 4)} for n in ("x", "z", "y")]
+    greet(ring_peers(("x", "z", "y")) + [{"c": 1 - c_me}] + across)
     for copy in own:
         copy.wait()
     ring = Gather(w, wsend, wrecv)
@@ -433,7 +416,7 @@
     rs = Scatter(g, r, send, recv, (gate_new, up_new, down_new))
     later = TokenScatter(0, nl, nlt, credit, tsend, trecv)
     earlier = TokenScatter(1, ne, net, credit, tsend, trecv)
-    total = GainSum(gmine, gtheirs, gsend, grecv)
+    total = GainSum(grows, gsend, grecv)
 
     gain_row = gain[...].astype(F32)
 
@@ -546,108 +529,204 @@
 
         earlier.share(k)
 
+    def gain_step(i):
+        row = total.end(i - 1) if i else jnp.sum(gacc[...], axis=0, keepdims=True)
+        if i < 4:
+            total.start(i, row)
+        else:
+            gain_out[...] = row
+
+    def later_end():
+        later_out[...] = (lrow[...].astype(F32) + 0.5 * later.finish()).astype(BF)
+
+    def earlier_end():
+        earlier_out[...] = (crow[...].astype(F32) + earlier.finish()).astype(BF)
+
+    gacc[...] = jnp.zeros_like(gacc)
     ins[0].wait()
     norms(nl, 0, blocks)
-    ring.t1(0)
     norms(nl, blocks, 2 * blocks)
+    ins[1].wait()
+    norms(ne, 0, blocks)
+    ring.t1(0,0,1)
+    ring.t1(0,0,-1)
+    ring.t1(0,1,1)
+    ring.t1(0,1,-1)
     turns(nlt, nl, 0, blocks // 2)
-    ring.t2(0)
+    ring.hand(0,0,0,1)
+    ring.hand(0,0,0,-1)
+    ring.hand(0,1,0,1)
+    ring.hand(0,1,0,-1)
     turns(nlt, nl, blocks // 2, blocks)
-    ring.t3(0)
+    ring.t3(0,0)
+    ring.hand(0,0,-1,1)
+    ring.hand(0,0,-1,-1)
+    norms(ne, blocks, 2 * blocks)
+    ring.hand(0,0,1,1)
+    ring.hand(0,0,1,-1)
+    ring.hand(0,1,-1,1)
+    ring.hand(0,1,-1,-1)
+    ring.t3(0,1)
+    ring.hand(0,1,1,1)
+    ring.hand(0,1,1,-1)
     ring.t0(1)
-    ins[1].wait()
-    norms(ne, 0, 2 * blocks)
-    ring.t4(0)
-    turns(net, ne, 0, blocks)
-    ring.t5(0)
-    ring.t1(1)
+    turns(net, ne, 0, blocks // 2)
+    turns(net, ne, blocks // 2, blocks)
+    ring.hand(0,0,2,1)
+    ring.hand(0,0,2,-1)
     ins[2].wait()
-    turns(cott, cot, 0, blocks)
-    gacc[...] = jnp.zeros_like(gacc)
+    turns(cott, cot, 0, blocks // 2)
+    ring.t1(1,1,1)
+    ring.t1(1,1,-1)
+    ring.hand(0,1,2,1)
+    ring.hand(0,1,2,-1)
+    turns(cott, cot, blocks // 2, blocks)
+    ring.t1(1,0,1)
+    ring.t1(1,0,-1)
+    ring.hand(1,0,0,1)
+    ring.hand(1,0,0,-1)
+    ring.hand(1,1,0,1)
+    ring.hand(1,1,0,-1)
+    ring.t3(1,1)
+    ring.hand(1,1,-1,1)
+    ring.hand(1,1,-1,-1)
+    ring.hand(1,0,-1,-1)
+    ring.hand(1,0,-1,1)
+    ring.hand(1,1,1,1)
+    ring.hand(1,1,1,-1)
+    ring.t6(0)
+    L(0, 3, 1)
+    ring.hand(1,0,1,1)
+    ring.hand(1,0,1,-1)
+    E(0, 0, 1)
+    ring.t3(1,0)
+    ring.t0(2)
+    L(0, 0, 1)
+    L(0, 2, 1)
+    E(0, 1, 1)
+    L(0, 1, 1)
+    E(0, 2, 1)
+    ring.hand(1,1,2,1)
+    ring.hand(1,1,2,-1)
+    E(0, 3, 1)
+    G(0, 1, 1)
+    G(0, 0, 1)
+    ring.hand(1,0,2,1)
+    ring.hand(1,0,2,-1)
+    G(0, 2, 2)
+    ring.t1(2,1,1)
+    ring.t1(2,1,-1)
+    ring.t1(2,0,1)
+    ring.t1(2,0,-1)
+    ring.hand(2,0,0,1)
+    ring.hand(2,0,0,-1)
+    ring.hand(2,1,0,1)
+    ring.hand(2,1,0,-1)
     for copy in ins[3:]:
         copy.wait()
-    ring.t6(0)
-
-    E(0, 0, 2)
-    ring.t2(1)
-    E(0, 2, 2)
-    ring.t3(1)
-    ring.t0(2)
-    G(0, 0, 2)
-    ring.t4(1)
-    G(0, 2, 2)
-    ring.t5(1)
-    ring.t1(2)
-    L(0, 0, 4)
     ring.t6(1)
-
-    E(1, 0, 2)
-    ring.t2(2)
-    E(1, 2, 2)
-    ring.t3(2)
+    E(1, 0, 1)
+    ring.t3(2,1)
+    L(1, 0, 1)
+    E(1, 2, 1)
+    ring.hand(2,1,-1,1)
+    ring.hand(2,1,-1,-1)
+    L(1, 3, 1)
+    ring.hand(2,0,-1,1)
+    ring.hand(2,0,-1,-1)
+    L(1, 1, 1)
+    E(1, 3, 1)
+    ring.hand(2,0,1,1)
+    ring.hand(2,0,1,-1)
+    ring.hand(2,1,1,1)
+    ring.hand(2,1,1,-1)
+    L(1, 2, 1)
+    ring.t3(2,0)
     rs.s1(0)
-    G(1, 0, 2)
-    ring.t4(2)
-    G(1, 2, 2)
-    ring.t5(2)
+    E(1, 1, 1)
+    G(1, 1, 2)
+    ring.hand(2,1,2,1)
+    ring.hand(2,1,2,-1)
+    G(1, 0, 1)
+    G(1, 3, 1)
+    ring.hand(2,0,2,1)
+    ring.hand(2,0,2,-1)
     rs.s1(1)
-    L(1, 0, 4)
-    rs.a1(0)
+    rs.a1(0,1,1)
+    rs.a1(0,0,1)
+    rs.a1(0,0,-1)
+    rs.a1(0,1,-1)
     ring.t6(2)
-
-    L(2, 0, 4)
+    E(2, 3, 1)
+    L(2, 1, 1)
+    E(2, 1, 1)
+    L(2, 0, 1)
+    L(2, 3, 1)
+    rs.a1(1,1,1)
+    rs.a1(1,0,1)
+    rs.a1(1,0,-1)
+    rs.a1(1,1,-1)
+    L(2, 2, 1)
     later.ready()
     hidden.start()
-    later_block(2)
-    later_block(1)
-    rs.a1(1)
-    later.far()
-    E(2, 0, 2)
-    rs.a2(0)
-    E(2, 2, 2)
+    E(2, 0, 1)
+    E(2, 2, 1)
     earlier.ready()
     reload.start()
-    G(2, 0, 4)
+    G(2, 3, 1)
+    G(2, 2, 1)
+    later_block(2)
+    rs.a2(0,0)
+    rs.a2(0,1)
+    later.far()
+    G(2, 0, 2)
     rs.s1(2)
-    later_block(-1)
-    rs.a3(0)
-    later_block(0)
-    later.near(1)
-    later.near(-1)
     reload.wait()
     earlier_block(2)
-    rs.a1(2)
-    rs.a2(1)
+    later_block(-1)
+    rs.a2(1,0)
+    rs.a3(0,0,1)
+    earlier.far()
+    rs.a3(0,0,-1)
+    rs.a3(0,1,1)
+    rs.a3(0,1,-1)
+    rs.a2(1,1)
+    later.near(-1)
+    later_block(1)
+    rs.a1(2,1,1)
+    rs.a1(2,0,1)
+    rs.a1(2,0,-1)
+    rs.a3(1,0,1)
+    rs.a3(1,0,-1)
+    rs.a1(2,1,-1)
+    rs.a4(0,1)
+    later.near(1)
+    earlier_block(-1)
+    rs.a3(1,1,1)
+    rs.a3(1,1,-1)
+    rs.a4(0,0)
     earlier_block(1)
-    earlier.far()
-    rs.a4(0)
-    earlier_block(-1)
-    rs.a3(1)
+    earlier.near(-1)
     earlier_block(0)
-    gmine[0] = jnp.sum(gacc[...], axis=0, keepdims=True)
-    total.start(0)
-    total.end(0)
-    total.start(1)
-    later_out[...] = (lrow[...].astype(F32) + 0.5 * later.finish()).astype(BF)
-    total.end(1)
-    total.start(2)
     earlier.near(1)
-    earlier.near(-1)
-    total.end(2)
-    total.start(3)
-    rs.a2(2)
-    total.end(3)
-    total.start(4)
-    rs.a3(2)
-    rs.a4(1)
-    total.end(4)
-    total.start(5)
-    rs.a4(2)
-    total.end(5)
-    total.start(6)
-    earlier_out[...] = (crow[...].astype(F32) + earlier.finish()).astype(BF)
-    total.end(6)
-    gain_out[...] = gmine[7]
+    gain_step(0)
+    rs.a2(2,0)
+    rs.a2(2,1)
+    gain_step(1)
+    rs.a4(1,0)
+    rs.a4(1,1)
+    later_block(0)
+    rs.a3(2,0,-1)
+    rs.a3(2,0,1)
+    rs.a3(2,1,-1)
+    rs.a3(2,1,1)
+    later_end()
+    gain_step(2)
+    rs.a4(2,0)
+    rs.a4(2,1)
+    gain_step(3)
+    earlier_end()
+    gain_step(4)
     for c in range(N_CHUNK):
         ring.drain(c)
         rs.drain(c)
@@ -699,8 +778,7 @@
             pltpu.VMEM((SHARD, width), BF),
             pltpu.VMEM((SHARD, width), BF),
             pltpu.VMEM((8, width), F32),
-            pltpu.VMEM((8, 1, width), F32),
-            pltpu.VMEM((7, 1, width), F32),
+            pltpu.VMEM((4, 4, 1, width), F32),
             dma((9,)),
             dma((N_CHUNK, 3)),
             dma((N_CHUNK, 2, 20)),
@@ -709,8 +787,8 @@
             dma((N_CHUNK, 2, 8)),
             dma((2, 8)),
             dma((2, 8)),
-            dma((7,)),
-            dma((7,)),
+            dma((4, 4)),
+            dma((4, 4)),
             pltpu.SemaphoreType.REGULAR((2, 3)),
             dma,
         ],

time: 140 us -> 141 us (level)
  no operation moved by 1% of the time
where the time goes in v6:
time: 141 us; the launch traced here: 140 us
  Pallas kernels  129 us (91%)
  local copies, waits for them, and re-layouts  8.75 us (6%)
  other arithmetic  1.43 us (1%)
    pallas_call x1, Pallas kernels, run(): pl.pallas_call(sublayer, out_shape=[jax.ShapeDtypeStruct((tokens // 8, wi...  129 us
    unnamed x14, local copies, waits for them, and re-layouts  7.46 us

profile of v6, /device:TPU:0, one launch (start us, length us, event | category | flops | bytes accessed | tf_op | source)
XLA Modules:
  0.0 139.7 jit_solution(4360041927008026790)
XLA Ops:
  0.6 1.3 reshape.17.gain
  1.9 128.9 %sublayer.1 = (bf16[128,2048]{1,0:T(8,128)(2,1)}, bf16[704,1024]{1,0:T(8,128)(2,1)}, bf16[128,2048]{1,0:T(8,128)(2,1)}, f32[704,128]{1,0:T(8,128)}, f32[704,128]...) custom-call(bf16[1024,2048]{1,0:T(8,128)(2,1)} %later_in.1, bf16[1024,2048]{1,0:T(8,128)(2,1)} %earlier_in.1, ...), custom_call_target="tpu_custom_call" | custom-call | tf_op jit(solution)/shard_map/sublayer/pallas_call | solution.py:746
  130.8 0.0 copy-start
  130.8 0.0 copy-start.3
  130.8 0.0 copy-start.2
  130.8 0.0 copy-start.1
  130.8 1.4 %add.3 = f32[2048]{0:T(1024)} add(f32[2048]{0:T(1024)} %param.21, f32[2048]{0:T(1024)} %bitcast.21) | non-fusion elementwise | flops 2048 | bytes 24576 | tf_op jit(solution)/shard_map/add | solution.py:808
  132.3 1.9 %copy.24 = bf16[128,2048]{1,0:T(8,128)(2,1)} copy(bf16[128,2048]{1,0:T(8,128)(2,1)} %get-tuple-element.28) | data formatting | bytes 1048576
  134.1 2.6 %copy.25 = bf16[1024,704]{0,1:T(8,128)(2,1)} copy(bf16[1024,704]{0,1:T(8,128)(2,1)} %bitcast.11) | data formatting | bytes 2883584
  136.7 0.0 copy-done
  136.7 0.8 copy.26
  137.5 0.0 copy-done.3
  137.5 0.7 copy.27
  138.2 0.0 copy-done.2
  138.3 0.7 copy.28
  139.0 0.0 copy-done.1
  139.0 0.7 copy.29
Async XLA Ops:
  130.8 5.9 %copy-start = (bf16[128,2048]{1,0:T(8,128)(2,1)S(1)}, bf16[128,2048]{1,0:T(8,128)(2,1)}, u32[]{:S(2)}) copy-start(bf16[128,2048]{1,0:T(8,128)(2,1)} %get-tuple-element.30) | copy-start | bytes 1572868
  130.8 6.7 %copy-start.3 = (f32[704,128]{1,0:T(8,128)S(1)}, f32[704,128]{1,0:T(8,128)}, u32[]{:S(2)}) copy-start(f32[704,128]{1,0:T(8,128)} %get-tuple-element.17) | copy-start | bytes 1081348
  130.8 7.4 %copy-start.2 = (f32[704,128]{1,0:T(8,128)S(1)}, f32[704,128]{1,0:T(8,128)}, u32[]{:S(2)}) copy-start(f32[704,128]{1,0:T(8,128)} %get-tuple-element.18) | copy-start | bytes 1081348
  130.8 8.2 %copy-start.1 = (f32[704,128]{1,0:T(8,128)S(1)}, f32[704,128]{1,0:T(8,128)}, u32[]{:S(2)}) copy-start(f32[704,128]{1,0:T(8,128)} %get-tuple-element.19) | copy-start | bytes 1081348

commit v7 on v6

--- a/solution.py
+++ b/solution.py
@@ -418,7 +418,7 @@
     earlier = TokenScatter(1, ne, net, credit, tsend, trecv)
     total = GainSum(grows, gsend, grecv)
 
-    gain_row = gain[...].astype(F32)
+    gain_row = gain[...].astype(F32).reshape(1, width)
 
     def turn_block(turned, ref, i):
         rows = pl.ds(pl.multiple_of(i * 128, 128), 128)
@@ -543,188 +543,188 @@
         earlier_out[...] = (crow[...].astype(F32) + earlier.finish()).astype(BF)
 
     gacc[...] = jnp.zeros_like(gacc)
-    ins[0].wait()
-    norms(nl, 0, blocks)
-    norms(nl, blocks, 2 * blocks)
-    ins[1].wait()
-    norms(ne, 0, blocks)
+    ins[2].wait()
+    turns(cott, cot, 0, blocks // 2)
+    turns(cott, cot, blocks // 2, blocks)
     ring.t1(0,0,1)
     ring.t1(0,0,-1)
     ring.t1(0,1,1)
     ring.t1(0,1,-1)
-    turns(nlt, nl, 0, blocks // 2)
+    ins[0].wait()
+    norms(nl, 0, blocks)
     ring.hand(0,0,0,1)
     ring.hand(0,0,0,-1)
     ring.hand(0,1,0,1)
     ring.hand(0,1,0,-1)
-    turns(nlt, nl, blocks // 2, blocks)
+    norms(nl, blocks, 2 * blocks)
     ring.t3(0,0)
+    ins[1].wait()
+    norms(ne, 0, blocks)
     ring.hand(0,0,-1,1)
     ring.hand(0,0,-1,-1)
+    ring.hand(0,1,-1,1)
+    ring.hand(0,1,-1,-1)
     norms(ne, blocks, 2 * blocks)
+    ring.t3(0,1)
+    ring.t0(1)
     ring.hand(0,0,1,1)
     ring.hand(0,0,1,-1)
-    ring.hand(0,1,-1,1)
-    ring.hand(0,1,-1,-1)
-    ring.t3(0,1)
     ring.hand(0,1,1,1)
     ring.hand(0,1,1,-1)
-    ring.t0(1)
     turns(net, ne, 0, blocks // 2)
-    turns(net, ne, blocks // 2, blocks)
     ring.hand(0,0,2,1)
     ring.hand(0,0,2,-1)
-    ins[2].wait()
-    turns(cott, cot, 0, blocks // 2)
+    turns(net, ne, blocks // 2, blocks)
+    ring.hand(0,1,2,1)
+    ring.hand(0,1,2,-1)
+    turns(nlt, nl, 0, blocks // 2)
+    ring.t1(1,0,1)
+    ring.t1(1,0,-1)
     ring.t1(1,1,1)
     ring.t1(1,1,-1)
-    ring.hand(0,1,2,1)
-    ring.hand(0,1,2,-1)
-    turns(cott, cot, blocks // 2, blocks)
-    ring.t1(1,0,1)
-    ring.t1(1,0,-1)
+    turns(nlt, nl, blocks // 2, blocks)
     ring.hand(1,0,0,1)
     ring.hand(1,0,0,-1)
     ring.hand(1,1,0,1)
     ring.hand(1,1,0,-1)
-    ring.t3(1,1)
+    ring.t6(0)
+    E(0, 3, 1)
+    E(0, 1, 1)
+    ring.t3(1,0)
+    ring.hand(1,0,-1,1)
+    ring.hand(1,0,-1,-1)
+    E(0, 0, 1)
+    E(0, 2, 1)
+    ring.hand(1,0,1,1)
+    ring.hand(1,0,1,-1)
     ring.hand(1,1,-1,1)
     ring.hand(1,1,-1,-1)
-    ring.hand(1,0,-1,-1)
-    ring.hand(1,0,-1,1)
+    G(0, 2, 1)
+    ring.t3(1,1)
+    ring.t0(2)
+    G(0, 0, 1)
     ring.hand(1,1,1,1)
     ring.hand(1,1,1,-1)
-    ring.t6(0)
+    L(0, 2, 1)
+    G(0, 3, 1)
+    L(0, 1, 1)
     L(0, 3, 1)
-    ring.hand(1,0,1,1)
-    ring.hand(1,0,1,-1)
-    E(0, 0, 1)
-    ring.t3(1,0)
-    ring.t0(2)
+    ring.hand(1,0,2,1)
+    ring.hand(1,0,2,-1)
     L(0, 0, 1)
-    L(0, 2, 1)
-    E(0, 1, 1)
-    L(0, 1, 1)
-    E(0, 2, 1)
+    G(0, 1, 1)
     ring.hand(1,1,2,1)
     ring.hand(1,1,2,-1)
-    E(0, 3, 1)
-    G(0, 1, 1)
-    G(0, 0, 1)
-    ring.hand(1,0,2,1)
-    ring.hand(1,0,2,-1)
-    G(0, 2, 2)
+    ring.t1(2,0,-1)
+    ring.t1(2,0,1)
+    ring.t1(2,1,-1)
     ring.t1(2,1,1)
-    ring.t1(2,1,-1)
-    ring.t1(2,0,1)
-    ring.t1(2,0,-1)
+    ring.hand(2,1,0,-1)
+    ring.hand(2,1,0,1)
+    ring.hand(2,0,0,-1)
     ring.hand(2,0,0,1)
-    ring.hand(2,0,0,-1)
-    ring.hand(2,1,0,1)
-    ring.hand(2,1,0,-1)
     for copy in ins[3:]:
         copy.wait()
     ring.t6(1)
+    L(1, 0, 1)
+    E(1, 3, 1)
+    ring.t3(2,0)
+    ring.hand(2,0,1,1)
+    ring.hand(2,0,1,-1)
+    L(1, 2, 2)
+    ring.hand(2,0,-1,1)
+    ring.hand(2,0,-1,-1)
+    ring.hand(2,1,1,1)
+    ring.hand(2,1,1,-1)
     E(1, 0, 1)
     ring.t3(2,1)
-    L(1, 0, 1)
+    rs.s1(0)
     E(1, 2, 1)
     ring.hand(2,1,-1,1)
     ring.hand(2,1,-1,-1)
-    L(1, 3, 1)
-    ring.hand(2,0,-1,1)
-    ring.hand(2,0,-1,-1)
-    L(1, 1, 1)
-    E(1, 3, 1)
-    ring.hand(2,0,1,1)
-    ring.hand(2,0,1,-1)
-    ring.hand(2,1,1,1)
-    ring.hand(2,1,1,-1)
-    L(1, 2, 1)
-    ring.t3(2,0)
-    rs.s1(0)
     E(1, 1, 1)
-    G(1, 1, 2)
+    G(1, 2, 1)
+    ring.hand(2,0,2,1)
+    ring.hand(2,0,2,-1)
+    G(1, 0, 1)
+    G(1, 3, 1)
     ring.hand(2,1,2,1)
     ring.hand(2,1,2,-1)
-    G(1, 0, 1)
-    G(1, 3, 1)
-    ring.hand(2,0,2,1)
-    ring.hand(2,0,2,-1)
+    G(1, 1, 1)
     rs.s1(1)
+    L(1, 1, 1)
+    rs.a1(0,0,-1)
+    rs.a1(0,0,1)
     rs.a1(0,1,1)
-    rs.a1(0,0,1)
-    rs.a1(0,0,-1)
     rs.a1(0,1,-1)
     ring.t6(2)
+    L(2, 3, 1)
     E(2, 3, 1)
-    L(2, 1, 1)
-    E(2, 1, 1)
-    L(2, 0, 1)
-    L(2, 3, 1)
+    L(2, 2, 1)
+    L(2, 0, 2)
+    later.ready()
+    hidden.start()
     rs.a1(1,1,1)
     rs.a1(1,0,1)
     rs.a1(1,0,-1)
     rs.a1(1,1,-1)
-    L(2, 2, 1)
-    later.ready()
-    hidden.start()
+    later_block(2)
+    later_block(1)
+    later_block(-1)
+    later.far()
     E(2, 0, 1)
-    E(2, 2, 1)
+    rs.a2(0,1)
+    rs.a2(0,0)
+    E(2, 1, 2)
     earlier.ready()
     reload.start()
+    G(2, 0, 1)
+    G(2, 2, 1)
+    G(2, 1, 1)
+    later.near(1)
+    later.near(-1)
+    rs.a2(1,1)
+    rs.a2(1,0)
+    rs.a3(0,0,1)
+    rs.a3(0,0,-1)
+    rs.a3(0,1,1)
+    rs.a3(0,1,-1)
     G(2, 3, 1)
-    G(2, 2, 1)
-    later_block(2)
-    rs.a2(0,0)
-    rs.a2(0,1)
-    later.far()
-    G(2, 0, 2)
     rs.s1(2)
     reload.wait()
     earlier_block(2)
-    later_block(-1)
-    rs.a2(1,0)
-    rs.a3(0,0,1)
-    earlier.far()
-    rs.a3(0,0,-1)
-    rs.a3(0,1,1)
-    rs.a3(0,1,-1)
-    rs.a2(1,1)
-    later.near(-1)
-    later_block(1)
-    rs.a1(2,1,1)
-    rs.a1(2,0,1)
-    rs.a1(2,0,-1)
     rs.a3(1,0,1)
     rs.a3(1,0,-1)
-    rs.a1(2,1,-1)
-    rs.a4(0,1)
-    later.near(1)
-    earlier_block(-1)
     rs.a3(1,1,1)
     rs.a3(1,1,-1)
     rs.a4(0,0)
+    rs.a4(0,1)
+    earlier_block(-1)
+    earlier.far()
+    rs.a1(2,0,1)
+    rs.a1(2,0,-1)
+    rs.a1(2,1,1)
+    rs.a1(2,1,-1)
+    rs.a4(1,0)
+    rs.a4(1,1)
     earlier_block(1)
-    earlier.near(-1)
     earlier_block(0)
     earlier.near(1)
+    earlier.near(-1)
     gain_step(0)
+    later_block(0)
+    gain_step(1)
     rs.a2(2,0)
     rs.a2(2,1)
-    gain_step(1)
-    rs.a4(1,0)
-    rs.a4(1,1)
-    later_block(0)
+    later_end()
+    gain_step(2)
     rs.a3(2,0,-1)
     rs.a3(2,0,1)
     rs.a3(2,1,-1)
     rs.a3(2,1,1)
-    later_end()
-    gain_step(2)
+    gain_step(3)
     rs.a4(2,0)
     rs.a4(2,1)
-    gain_step(3)
     earlier_end()
     gain_step(4)
     for c in range(N_CHUNK):
@@ -796,13 +796,44 @@
             collective_id=0, has_side_effects=True, vmem_limit_bytes=64 * 1024 * 1024 - 65536
         ),
         name="sublayer",
-    )(later_in, earlier_in, cot, gate_w, up_w, down_w, gain.reshape(1, width), gate_sum, up_sum, down_sum)
+    )(later_in, earlier_in, cot, gate_w, up_w, down_w, gain, gate_sum, up_sum, down_sum)
+
+
+def deliver_body(*refs):
+    n = (len(refs) - 2) // 3
+    srcs, outs, bufs = refs[:n], refs[n : 2 * n], refs[2 * n : 3 * n]
+    in_sem, out_sem = refs[-2:]
+    ins = [pltpu.make_async_copy(a, b, in_sem.at[i]) for i, (a, b) in enumerate(zip(srcs, bufs))]
+    for copy in ins:
+        copy.start()
+    puts = [pltpu.make_async_copy(a, b, out_sem.at[i]) for i, (a, b) in enumerate(zip(bufs, outs))]
+    for copy, put in zip(ins, puts):
+        copy.wait()
+        put.start()
+    for put in puts:
+        put.wait()
+
+
+def deliver(arrays):
+    any_ = pl.BlockSpec(memory_space=pl.ANY)
+    n = len(arrays)
+    return pl.pallas_call(
+        deliver_body,
+        out_shape=[jax.ShapeDtypeStruct(a.shape, a.dtype) for a in arrays],
+        in_specs=[any_] * n,
+        out_specs=[any_] * n,
+        scratch_shapes=[pltpu.VMEM(a.shape, a.dtype) for a in arrays]
+        + [pltpu.SemaphoreType.DMA((n,)), pltpu.SemaphoreType.DMA((n,))],
+        compiler_params=pltpu.CompilerParams(vmem_limit_bytes=64 * 1024 * 1024 - 65536),
+        name="deliver",
+    )(*arrays)
 
 
 def local(later_in, earlier_in, cot, gate_w, up_w, down_w, gain, gate_sum, up_sum, down_sum, gain_sum):
-    later_out, hidden, earlier_grad, gate_new, up_new, down_new, gain_total = run(
+    *parts, gain_total = run(
         later_in, earlier_in, cot, gate_w.T, up_w.T, down_w.T, gain, gate_sum.T, up_sum.T, down_sum.T
     )
+    later_out, hidden, earlier_grad, gate_new, up_new, down_new = deliver(parts)
     return (
         later_out, hidden.T, earlier_grad,
         gate_new.T, up_new.T, down_new.T, gain_sum + gain_total[0],

time: 141 us -> 128 us (0.908)
  local copies, waits for them, and re-layouts: 8.75 us -> 0 us
  Pallas kernels: 129 us -> 125 us
    unnamed x14 -> x0, local copies, waits for them, and re-layouts: 7.46 us -> none
    pallas_call x1, Pallas kernels: 129 us -> 122 us  [run(): pl.pallas_call(sublayer, out_shape=[jax.ShapeDtypeStruct((tokens // 8, wi...]
    pallas_call x0 -> x1, Pallas kernels: none -> 3.26 us  [deliver(): pl.pallas_call(deliver_body, out_shape=[jax.ShapeDtypeStruct(a.shape, a.d...]
where the time goes in v7:
time: 128 us; the launch traced here: 127 us
  Pallas kernels  125 us (98%)
  other arithmetic  1.32 us (1%)
    pallas_call x1, Pallas kernels, run(): pl.pallas_call(sublayer, out_shape=[jax.ShapeDtypeStruct((tokens // 8, wi...  122 us
    pallas_call x1, Pallas kernels, deliver(): pl.pallas_call(deliver_body, out_shape=[jax.ShapeDtypeStruct(a.shape, a.d...  3.26 us

profile of v7, /device:TPU:0, one launch (start us, length us, event | category | flops | bytes accessed | tf_op | source)
XLA Modules:
  0.0 127.3 jit_solution(14133286680028205144)
XLA Ops:
  0.6 122.1 %sublayer.1 = (bf16[128,2048]{1,0:T(8,128)(2,1)}, bf16[704,1024]{1,0:T(8,128)(2,1)}, bf16[128,2048]{1,0:T(8,128)(2,1)}, f32[704,128]{1,0:T(8,128)}, f32[704,128]...) custom-call(bf16[1024,2048]{1,0:T(8,128)(2,1)} %later_in.1, bf16[1024,2048]{1,0:T(8,128)(2,1)} %earlier_in.1, ...), custom_call_target="tpu_custom_call" | custom-call | tf_op jit(solution)/shard_map/sublayer/pallas_call | solution.py:746
  122.8 3.3 %deliver.1 = (bf16[128,2048]{1,0:T(8,128)(2,1)}, bf16[704,1024]{1,0:T(8,128)(2,1)}, bf16[128,2048]{1,0:T(8,128)(2,1)}, f32[704,128]{1,0:T(8,128)}, f32[704,128]{1,0:T(8,128)}, /*index=5*/f32[704,128]{1,0:T(8,128)}) custom-call(bf16[128,2048]{1,0:T(8,128)(2,1)} %get-tuple-element.20.refs_0_, bf16[704,1024]{1,0:T(8,128)(2,1)} %get-tuple-element.21.refs_1_, ...), custom_call_target="tpu_custom_call" | custom-call | tf_op jit(solution)/shard_map/deliver/pallas_call | solution.py:820
  126.0 1.3 %add.3 = f32[2048]{0:T(1024)} add(f32[2048]{0:T(1024)} %param.21, f32[2048]{0:T(1024)} %bitcast.17) | non-fusion elementwise | flops 2048 | bytes 24576 | tf_op jit(solution)/shard_map/add | solution.py:839

commit v8 on v7

--- a/solution.py
+++ b/solution.py
@@ -14,8 +14,8 @@
 MESH = pl.DeviceIdType.MESH
 BF = jnp.bfloat16
 F32 = jnp.float32
-SIZES = (192, 256, 256)
-STARTS = (0, 192, 448)
+SIZES = (256, 320, 128)
+STARTS = (0, 256, 576)
 N_CHUNK = 3
 SHARD = 128
 NORM_FLOOR = 0.05
@@ -543,186 +543,187 @@
         earlier_out[...] = (crow[...].astype(F32) + earlier.finish()).astype(BF)
 
     gacc[...] = jnp.zeros_like(gacc)
-    ins[2].wait()
-    turns(cott, cot, 0, blocks // 2)
-    turns(cott, cot, blocks // 2, blocks)
+    ins[0].wait()
+    norms(nl, 0, blocks)
+    ins[1].wait()
+    norms(ne, 0, blocks)
+    norms(ne, blocks, 2 * blocks)
     ring.t1(0,0,1)
     ring.t1(0,0,-1)
     ring.t1(0,1,1)
     ring.t1(0,1,-1)
-    ins[0].wait()
-    norms(nl, 0, blocks)
+    turns(net, ne, 0, blocks // 2)
     ring.hand(0,0,0,1)
     ring.hand(0,0,0,-1)
     ring.hand(0,1,0,1)
     ring.hand(0,1,0,-1)
+    turns(net, ne, blocks // 2, blocks)
+    ring.t3(0,0)
     norms(nl, blocks, 2 * blocks)
-    ring.t3(0,0)
-    ins[1].wait()
-    norms(ne, 0, blocks)
     ring.hand(0,0,-1,1)
     ring.hand(0,0,-1,-1)
     ring.hand(0,1,-1,1)
     ring.hand(0,1,-1,-1)
-    norms(ne, blocks, 2 * blocks)
+    turns(nlt, nl, 0, blocks // 2)
     ring.t3(0,1)
     ring.t0(1)
     ring.hand(0,0,1,1)
     ring.hand(0,0,1,-1)
     ring.hand(0,1,1,1)
     ring.hand(0,1,1,-1)
-    turns(net, ne, 0, blocks // 2)
+    turns(nlt, nl, blocks // 2, blocks)
+    ins[2].wait()
+    turns(cott, cot, 0, blocks // 2)
     ring.hand(0,0,2,1)
     ring.hand(0,0,2,-1)
-    turns(net, ne, blocks // 2, blocks)
+    turns(cott, cot, blocks // 2, blocks)
     ring.hand(0,1,2,1)
     ring.hand(0,1,2,-1)
-    turns(nlt, nl, 0, blocks // 2)
+    ring.t1(1,1,-1)
+    ring.t1(1,1,1)
+    ring.t1(1,0,-1)
     ring.t1(1,0,1)
-    ring.t1(1,0,-1)
-    ring.t1(1,1,1)
-    ring.t1(1,1,-1)
-    turns(nlt, nl, blocks // 2, blocks)
+    ring.hand(1,0,0,-1)
     ring.hand(1,0,0,1)
-    ring.hand(1,0,0,-1)
+    ring.hand(1,1,0,-1)
     ring.hand(1,1,0,1)
-    ring.hand(1,1,0,-1)
     ring.t6(0)
     E(0, 3, 1)
+    ring.t3(1,1)
     E(0, 1, 1)
-    ring.t3(1,0)
+    L(0, 0, 1)
+    ring.hand(1,1,1,1)
+    ring.hand(1,1,1,-1)
+    E(0, 0, 1)
+    ring.hand(1,0,1,1)
+    ring.hand(1,0,1,-1)
+    E(0, 2, 1)
+    ring.hand(1,1,-1,1)
+    ring.hand(1,1,-1,-1)
+    L(0, 2, 1)
     ring.hand(1,0,-1,1)
     ring.hand(1,0,-1,-1)
-    E(0, 0, 1)
-    E(0, 2, 1)
-    ring.hand(1,0,1,1)
-    ring.hand(1,0,1,-1)
-    ring.hand(1,1,-1,1)
-    ring.hand(1,1,-1,-1)
     G(0, 2, 1)
-    ring.t3(1,1)
+    ring.t3(1,0)
     ring.t0(2)
     G(0, 0, 1)
-    ring.hand(1,1,1,1)
-    ring.hand(1,1,1,-1)
-    L(0, 2, 1)
     G(0, 3, 1)
-    L(0, 1, 1)
-    L(0, 3, 1)
-    ring.hand(1,0,2,1)
-    ring.hand(1,0,2,-1)
-    L(0, 0, 1)
     G(0, 1, 1)
     ring.hand(1,1,2,1)
     ring.hand(1,1,2,-1)
+    L(0, 3, 1)
+    L(0, 1, 1)
+    ring.hand(1,0,2,1)
+    ring.hand(1,0,2,-1)
+    ring.t1(2,1,1)
+    ring.t1(2,1,-1)
     ring.t1(2,0,-1)
     ring.t1(2,0,1)
-    ring.t1(2,1,-1)
-    ring.t1(2,1,1)
+    ring.hand(2,0,0,1)
+    ring.hand(2,0,0,-1)
     ring.hand(2,1,0,-1)
     ring.hand(2,1,0,1)
-    ring.hand(2,0,0,-1)
-    ring.hand(2,0,0,1)
     for copy in ins[3:]:
         copy.wait()
     ring.t6(1)
+    E(1, 2, 1)
+    ring.t3(2,1)
+    ring.hand(2,1,-1,1)
+    ring.hand(2,1,-1,-1)
     L(1, 0, 1)
-    E(1, 3, 1)
-    ring.t3(2,0)
     ring.hand(2,0,1,1)
     ring.hand(2,0,1,-1)
-    L(1, 2, 2)
+    ring.hand(2,1,1,1)
+    ring.hand(2,1,1,-1)
+    E(1, 1, 1)
+    ring.t3(2,0)
     ring.hand(2,0,-1,1)
     ring.hand(2,0,-1,-1)
-    ring.hand(2,1,1,1)
-    ring.hand(2,1,1,-1)
-    E(1, 0, 1)
-    ring.t3(2,1)
     rs.s1(0)
-    E(1, 2, 1)
-    ring.hand(2,1,-1,1)
-    ring.hand(2,1,-1,-1)
-    E(1, 1, 1)
-    G(1, 2, 1)
+    L(1, 1, 2)
+    ring.hand(2,1,2,1)
+    ring.hand(2,1,2,-1)
+    L(1, 3, 1)
+    E(1, 3, 1)
     ring.hand(2,0,2,1)
     ring.hand(2,0,2,-1)
-    G(1, 0, 1)
+    E(1, 0, 1)
+    G(1, 2, 1)
+    rs.a1(0,0,1)
+    rs.a1(0,0,-1)
     G(1, 3, 1)
-    ring.hand(2,1,2,1)
-    ring.hand(2,1,2,-1)
-    G(1, 1, 1)
-    rs.s1(1)
-    L(1, 1, 1)
-    rs.a1(0,0,-1)
-    rs.a1(0,0,1)
+    ring.t6(2)
     rs.a1(0,1,1)
     rs.a1(0,1,-1)
-    ring.t6(2)
     L(2, 3, 1)
-    E(2, 3, 1)
+    L(2, 0, 1)
     L(2, 2, 1)
-    L(2, 0, 2)
+    L(2, 1, 1)
     later.ready()
     hidden.start()
-    rs.a1(1,1,1)
-    rs.a1(1,0,1)
-    rs.a1(1,0,-1)
-    rs.a1(1,1,-1)
+    G(1, 0, 1)
     later_block(2)
     later_block(1)
     later_block(-1)
     later.far()
+    G(1, 1, 1)
+    rs.s1(1)
+    E(2, 1, 2)
+    rs.a2(0,0)
+    E(2, 3, 1)
     E(2, 0, 1)
     rs.a2(0,1)
-    rs.a2(0,0)
-    E(2, 1, 2)
     earlier.ready()
     reload.start()
+    G(2, 1, 1)
+    G(2, 3, 1)
+    G(2, 2, 1)
     G(2, 0, 1)
-    G(2, 2, 1)
-    G(2, 1, 1)
     later.near(1)
     later.near(-1)
-    rs.a2(1,1)
-    rs.a2(1,0)
+    rs.s1(2)
+    reload.wait()
+    earlier_block(2)
     rs.a3(0,0,1)
     rs.a3(0,0,-1)
     rs.a3(0,1,1)
     rs.a3(0,1,-1)
-    G(2, 3, 1)
-    rs.s1(2)
-    reload.wait()
-    earlier_block(2)
-    rs.a3(1,0,1)
-    rs.a3(1,0,-1)
-    rs.a3(1,1,1)
-    rs.a3(1,1,-1)
-    rs.a4(0,0)
-    rs.a4(0,1)
-    earlier_block(-1)
+    rs.a1(1,0,1)
+    rs.a1(1,0,-1)
+    rs.a1(1,1,1)
+    rs.a1(1,1,-1)
     earlier.far()
     rs.a1(2,0,1)
     rs.a1(2,0,-1)
     rs.a1(2,1,1)
     rs.a1(2,1,-1)
-    rs.a4(1,0)
-    rs.a4(1,1)
     earlier_block(1)
+    rs.a4(0,0)
+    rs.a4(0,1)
+    earlier_block(-1)
     earlier_block(0)
     earlier.near(1)
     earlier.near(-1)
     gain_step(0)
+    rs.a2(1,0)
+    gain_step(1)
+    rs.a2(1,1)
+    rs.a2(2,1)
+    rs.a2(2,0)
     later_block(0)
-    gain_step(1)
-    rs.a2(2,0)
-    rs.a2(2,1)
-    later_end()
     gain_step(2)
+    rs.a3(1,0,1)
+    rs.a3(1,0,-1)
+    rs.a3(1,1,-1)
+    rs.a3(1,1,1)
+    rs.a3(2,1,-1)
+    rs.a3(2,1,1)
     rs.a3(2,0,-1)
     rs.a3(2,0,1)
-    rs.a3(2,1,-1)
-    rs.a3(2,1,1)
+    later_end()
     gain_step(3)
+    rs.a4(1,0)
+    rs.a4(1,1)
     rs.a4(2,0)
     rs.a4(2,1)
     earlier_end()
@@ -800,13 +801,16 @@
 
 
 def deliver_body(*refs):
-    n = (len(refs) - 2) // 3
-    srcs, outs, bufs = refs[:n], refs[n : 2 * n], refs[2 * n : 3 * n]
+    n = (len(refs) - 5) // 3
+    srcs, (gain_sum, gain_total) = refs[:n], refs[n : n + 2]
+    outs, gain_new = refs[n + 2 : 2 * n + 2], refs[2 * n + 2]
+    bufs = refs[2 * n + 3 : 3 * n + 3]
     in_sem, out_sem = refs[-2:]
     ins = [pltpu.make_async_copy(a, b, in_sem.at[i]) for i, (a, b) in enumerate(zip(srcs, bufs))]
     for copy in ins:
         copy.start()
     puts = [pltpu.make_async_copy(a, b, out_sem.at[i]) for i, (a, b) in enumerate(zip(bufs, outs))]
+    gain_new[...] = gain_sum[...] + gain_total[...].reshape(gain_sum.shape)
     for copy, put in zip(ins, puts):
         copy.wait()
         put.start()
@@ -814,29 +818,32 @@
         put.wait()
 
 
-def deliver(arrays):
+def deliver(arrays, gain_sum, gain_total):
     any_ = pl.BlockSpec(memory_space=pl.ANY)
+    vm = pl.BlockSpec(memory_space=pltpu.VMEM)
     n = len(arrays)
     return pl.pallas_call(
         deliver_body,
-        out_shape=[jax.ShapeDtypeStruct(a.shape, a.dtype) for a in arrays],
-        in_specs=[any_] * n,
-        out_specs=[any_] * n,
+        out_shape=[jax.ShapeDtypeStruct(a.shape, a.dtype) for a in (*arrays, gain_sum)],
+        in_specs=[any_] * n + [vm] * 2,
+        out_specs=[any_] * n + [vm],
         scratch_shapes=[pltpu.VMEM(a.shape, a.dtype) for a in arrays]
         + [pltpu.SemaphoreType.DMA((n,)), pltpu.SemaphoreType.DMA((n,))],
         compiler_params=pltpu.CompilerParams(vmem_limit_bytes=64 * 1024 * 1024 - 65536),
         name="deliver",
-    )(*arrays)
+    )(*arrays, gain_sum, gain_total)
 
 
 def local(later_in, earlier_in, cot, gate_w, up_w, down_w, gain, gate_sum, up_sum, down_sum, gain_sum):
     *parts, gain_total = run(
         later_in, earlier_in, cot, gate_w.T, up_w.T, down_w.T, gain, gate_sum.T, up_sum.T, down_sum.T
     )
-    later_out, hidden, earlier_grad, gate_new, up_new, down_new = deliver(parts)
+    later_out, hidden, earlier_grad, gate_new, up_new, down_new, gain_new = deliver(
+        parts, gain_sum, gain_total
+    )
     return (
         later_out, hidden.T, earlier_grad,
-        gate_new.T, up_new.T, down_new.T, gain_sum + gain_total[0],
+        gate_new.T, up_new.T, down_new.T, gain_new,
     )
 
 

time: 128 us -> 129 us (level)
  Pallas kernels: 125 us -> 127 us
  other arithmetic: 1.32 us -> 0 us
    add x1 -> x0, other arithmetic: 1.32 us -> none  [local(): gain_sum + gain_total[0]]
    pallas_call x1, Pallas kernels: 3.26 us -> 4.57 us  [deliver(): pl.pallas_call(deliver_body, out_shape=[jax.ShapeDtypeStruct(a.shape, a.d...]
where the time goes in v8:
time: 129 us; the launch traced here: 128 us
  Pallas kernels  127 us (98%)
    pallas_call x1, Pallas kernels, run(): pl.pallas_call(sublayer, out_shape=[jax.ShapeDtypeStruct((tokens // 8, wi...  122 us
    pallas_call x1, Pallas kernels, deliver(): pl.pallas_call(deliver_body, out_shape=[jax.ShapeDtypeStruct(a.shape, a.d...  4.57 us

profile of v8, /device:TPU:0, one launch (start us, length us, event | category | flops | bytes accessed | tf_op | source)
XLA Modules:
  0.0 127.6 jit_solution(6506840227648550804)
XLA Ops:
  0.6 122.2 %sublayer.1 = (bf16[128,2048]{1,0:T(8,128)(2,1)}, bf16[704,1024]{1,0:T(8,128)(2,1)}, bf16[128,2048]{1,0:T(8,128)(2,1)}, f32[704,128]{1,0:T(8,128)}, f32[704,128]...) custom-call(bf16[1024,2048]{1,0:T(8,128)(2,1)} %later_in.1, bf16[1024,2048]{1,0:T(8,128)(2,1)} %earlier_in.1, ...), custom_call_target="tpu_custom_call" | custom-call | tf_op jit(solution)/shard_map/sublayer/pallas_call | solution.py:747
  122.8 4.6 %deliver.1 = (bf16[128,2048]{1,0:T(8,128)(2,1)}, bf16[704,1024]{1,0:T(8,128)(2,1)}, bf16[128,2048]{1,0:T(8,128)(2,1)}, f32[704,128]{1,0:T(8,128)}, f32[704,128]{...) custom-call(bf16[128,2048]{1,0:T(8,128)(2,1)} %get-tuple-element.21.refs_0_, ...), custom_call_target="tpu_custom_call" | custom-call | tf_op jit(solution)/shard_map/deliver/pallas_call | solution.py:825
